TPU v7x, 32 devices: a whole 2x2x4 slice. The times are simulated.
32 devices in a mesh: grp: 2 (over x), sp: 4 (over y, core), tp: 4 (over z).
Axes of the slice: x: 2, y: 2, z: 4, core: 2. Of those that a mesh axis runs over, the one named last changes fastest.
Arguments:
- resid_in: bfloat16 [4096, 2048], P(('grp', 'sp', 'tp')), parts along dimension 0, may hold values from -6 to 6
- pool_input: bfloat16 [4096, 1024], P(('grp', 'sp'), 'tp'), parts along dimension 0, may hold values from -6 to 6
- pool_weight: bfloat16 [4, 256, 256], replicated, may hold values from -0.375 to 0.375
- pool_scale: float32 [1024], replicated, may hold values from 0.2 to 0.8
- out_weight: bfloat16 [1024, 2048], replicated, may hold values from -0.1875 to 0.1875
- mix_gain: float32 [2048], replicated, may hold values from 0.1 to 1.9
- ffn_gain: float32 [2048], replicated, may hold values from 0.1 to 1.9
- w_gate: bfloat16 [32, 2048, 1024], P('sp', None, 'tp'), may hold values from -0.375 to 0.375
- w_up: bfloat16 [32, 2048, 1024], P('sp', None, 'tp'), may hold values from -0.375 to 0.375
- w_down: bfloat16 [32, 1024, 2048], P('sp', 'tp'), may hold values from -0.1875 to 0.1875
- routes: int32 [4096, 2], P(('grp', 'sp', 'tp')), parts along dimension 0, may hold values from 0 to 31, all different within a row; in each aligned block of 128 rows (0 to 127, 128 to 255, ...) at most 9 rows name the same one
- route_weight: float32 [4096, 2], P(('grp', 'sp', 'tp')), parts along dimension 0, may hold values from 0.1 to 1
- post_gain: float32 [2048], replicated, may hold values from 0.1 to 1.9
Outputs:
- layer_out: bfloat16 [4096, 2048], P(('grp', 'sp', 'tp')), parts along dimension 0
There are 2 independent parts, one for each index of `grp`. A program takes and returns all parts, laid end to end along the dimension named above; an argument that names none is the same for every part. Nothing has to cross between parts.
Inputs may be any that keep to these rules, and one draw needn't show every extreme that they name: `routes`: each row names 2 different experts. The rows of one device name any one expert at most 9 times, and in every draw some device's rows name some expert exactly 9 times.
All inputs are finite; a program needn't handle non-finite values.
Results may differ from a plain program's by a relative error of at most 0.011.
Values may be sent and summed in bfloat16 or wider, within the bound.
No kernel may reach another device: no remote copies, remote signals or barrier semaphores. Data moves between devices by JAX's collectives and lax.ppermute only.
A program may use at most 128 MiB of HBM per device.

v0:
```python
import jax
import jax.numpy as jnp
from jax import lax
from jax.experimental import pallas as pl
from jax.experimental.pallas import tpu as pltpu
from jax.sharding import PartitionSpec as P


GROUPS = 4
GROUP_DIM = 256
TOP = 2
CAP = 9


pool_windows = (2, 4, 8, 16)
reach_back = 15
norm_eps = 1e-06
clamp_limit = 7.0
glu_alpha = 1.702


def passed_along(x, axis, by):
    size = lax.axis_size(axis)
    pairs = [(i, i + by) for i in range(size) if 0 <= i + by < size]
    return lax.ppermute(x, axis, pairs)


def rotated(x, axis, by):
    size = lax.axis_size(axis)
    return lax.ppermute(x, axis, [(i, (i + by) % size) for i in range(size)])


def rms_scale(values, gain_vec):
    inverse = lax.rsqrt(jnp.mean(values * values, axis=-1, keepdims=True) + norm_eps)
    return values * inverse * gain_vec


def clamped_unit(gate_pre, upward):
    gate_clip = jnp.minimum(gate_pre, clamp_limit)
    linear = jnp.clip(upward, -clamp_limit, clamp_limit)
    return gate_clip * jax.nn.sigmoid(glu_alpha * gate_clip) * (linear + 1.0)


def mixed_window(pool_input):
    seg_rows, channels = pool_input.shape
    last_rows = pool_input[seg_rows - reach_back :]
    before = passed_along(last_rows, "sp", 1)
    extended = jnp.concatenate([before, pool_input], axis=0).astype(jnp.float32)
    first_chan = lax.axis_index("tp") * channels
    chan_group = (first_chan + lax.iota(jnp.int32, channels)) // GROUP_DIM
    positions = lax.axis_index("sp") * seg_rows + lax.iota(jnp.int32, seg_rows)
    window = jnp.zeros((channels,), jnp.int32)
    for group_level, win_len in enumerate(pool_windows):
        window = jnp.where(chan_group == group_level, win_len, window)
    running = jnp.zeros((seg_rows, channels), jnp.float32)
    window_sum = running
    for offset in range(pool_windows[-1]):
        running = running + extended[reach_back - offset : reach_back - offset + seg_rows]
        if offset + 1 in pool_windows:
            window_sum = jnp.where(window[None, :] == offset + 1, running, window_sum)
    divisor = jnp.minimum(positions[:, None] + 1, window[None, :]).astype(jnp.float32)
    return (window_sum / divisor - extended[reach_back:]).astype(jnp.bfloat16)


def reached(i, d, n):
    return i ^ d if n & (n - 1) == 0 else (i + d) % n


def offset_to(target, i, n):
    return target ^ i if n & (n - 1) == 0 else (target - i) % n


def moved(x, axis, d, back=False):
    size = lax.axis_size(axis)
    pairs = [(i, reached(i, d, size)) for i in range(size)]
    return lax.ppermute(x, axis, [(b, a) for a, b in pairs] if back else pairs)


LANES = 128
IN_VMEM = pl.BlockSpec(memory_space=pltpu.VMEM)


def load_body(*refs):
    half = len(refs) // 2
    sources, targets, done = refs[:half], refs[half:-1], refs[-1]
    copies = [
        pltpu.make_async_copy(source.at[e], target.at[e], done.at[i, e])
        for i, (source, target) in enumerate(zip(sources, targets))
        for e in range(source.shape[0])
    ]
    for copy in copies:
        copy.start()
    for copy in copies:
        copy.wait()


LOAD_LIMIT = 28


def load(*weights):
    return pl.pallas_call(
        load_body,
        in_specs=[pl.BlockSpec(memory_space=pltpu.HBM)] * len(weights),
        out_specs=[IN_VMEM] * len(weights),
        out_shape=[pltpu.VMEM(w.shape, w.dtype) for w in weights],
        scratch_shapes=[pltpu.SemaphoreType.DMA((len(weights), weights[0].shape[0]))],
        compiler_params=pltpu.CompilerParams(vmem_limit_bytes=LOAD_LIMIT << 20),
        name="load",
    )(*weights)


def pick_body(at, slot, block, *outs):
    rows = outs[0].shape[0]
    tokens = slot.shape[2]
    ids = lax.broadcasted_iota(jnp.int32, (len(outs) * rows, tokens), 0)
    hit = ids == slot[at, 0:1, :]
    for k in range(1, slot.shape[1]):
        hit = hit | (ids == slot[at, k : k + 1, :])
    chosen = jnp.where(hit, 1.0, 0.0).astype(jnp.bfloat16)
    for j in range(0, block.shape[1], 2 * LANES):
        cols = slice(j, j + 2 * LANES)
        taken = jnp.dot(chosen, block[:, cols], preferred_element_type=jnp.float32)
        for d, out in enumerate(outs):
            out[:, cols] = taken[d * rows : (d + 1) * rows].astype(out.dtype)


def pick(at, slot, block, n_sp, slot_rows):
    shape = jax.ShapeDtypeStruct((slot_rows, block.shape[1]), block.dtype)
    return pl.pallas_call(
        lambda *refs: pick_body(at, *refs),
        in_specs=[IN_VMEM] * 2,
        out_specs=[IN_VMEM] * n_sp,
        out_shape=[shape] * n_sp,
        compiler_params=pltpu.CompilerParams(vmem_limit_bytes=6 << 20),
        name="pick",
    )(slot, block)


def shares_of(at, slot, weight, d, rows):
    ids = lax.broadcasted_iota(jnp.int32, (slot.shape[1], rows), 1) + d * rows
    share = jnp.zeros((slot.shape[1], rows), jnp.float32)
    for k in range(slot.shape[2]):
        share = share + jnp.where(ids == slot[at, :, k : k + 1], weight[at, :, k : k + 1], 0.0)
    return share.astype(jnp.bfloat16)


def combine_body(at, slot, weight, *refs):
    backs, out = refs[:-1], refs[-1]
    rows = backs[0].shape[0]
    share = [shares_of(at, slot, weight, d, rows) for d in range(len(backs))]
    for j in range(0, out.shape[1], 2 * LANES):
        cols = slice(j, j + 2 * LANES)
        total = None
        for d, back in enumerate(backs):
            term = jnp.dot(share[d], back[:, cols], preferred_element_type=jnp.float32)
            total = term if total is None else total + term
        out[:, cols] = total.astype(out.dtype)


def combine(at, slot, weight, backs):
    shape = jax.ShapeDtypeStruct((slot.shape[1], backs[0].shape[1]), jnp.bfloat16)
    return pl.pallas_call(
        lambda *refs: combine_body(at, *refs),
        in_specs=[IN_VMEM] * (2 + len(backs)),
        out_specs=IN_VMEM,
        out_shape=shape,
        compiler_params=pltpu.CompilerParams(vmem_limit_bytes=6 << 20),
        name="combine",
    )(slot, weight, *backs)


def finish_body(at, n_back, slot, weight, resid, gain, *refs):
    backs, parts, (out, mix) = refs[:n_back], refs[n_back:-2], refs[-2:]
    rows, width = backs[0].shape[0], out.shape[1]
    share = [shares_of(at, slot, weight, d, rows) for d in range(n_back)]
    square = jnp.zeros((out.shape[0], LANES), jnp.float32)
    for j in range(0, width, 2 * LANES):
        cols = slice(j, j + 2 * LANES)
        total = parts[0][:, cols].astype(jnp.float32) if parts else 0.0
        for part in parts[1:]:
            total = total + part[:, cols].astype(jnp.float32)
        for d, back in enumerate(backs):
            total = total + jnp.dot(share[d], back[:, cols], preferred_element_type=jnp.float32)
        mix[:, cols] = total
        square = square + total[:, :LANES] * total[:, :LANES]
        square = square + total[:, LANES:] * total[:, LANES:]
    mean = jnp.sum(square, axis=1, keepdims=True) / width
    inverse = lax.rsqrt(mean + norm_eps)
    for j in range(0, width, 2 * LANES):
        cols = slice(j, j + 2 * LANES)
        scaled = mix[:, cols] * inverse * gain[:, cols]
        out[:, cols] = (resid[:, cols].astype(jnp.float32) + scaled).astype(out.dtype)


def finish(at, slot, weight, resid, gain, backs, parts):
    return pl.pallas_call(
        lambda *refs: finish_body(at, len(backs), *refs),
        in_specs=[IN_VMEM] * (4 + len(backs) + len(parts)),
        out_specs=IN_VMEM,
        out_shape=jax.ShapeDtypeStruct(resid.shape, resid.dtype),
        scratch_shapes=[pltpu.VMEM(resid.shape, jnp.float32)],
        compiler_params=pltpu.CompilerParams(vmem_limit_bytes=6 << 20),
        name="finish",
    )(slot, weight, resid, gain.reshape(1, -1), *backs, *parts)


def experts_body(n_src, *refs):
    xs, (wg, wu, wd) = refs[:n_src], refs[n_src : n_src + 3]
    outs, (into, outof) = refs[n_src + 3 : 2 * n_src + 3], refs[2 * n_src + 3 :]
    count, width = wg.shape[0], xs[0].shape[1]
    tiles, left = divmod(xs[0].shape[0] // count, 8)
    whole = count * tiles * 8
    for s, x in enumerate(xs):
        for j in range(width // LANES):
            cols = slice(j * LANES, (j + 1) * LANES)
            into[j, s * left * count : (s + 1) * left * count, :] = x[whole:, cols].astype(
                jnp.float32
            )

    def one(e, carry):
        own = [pl.ds(pl.multiple_of((e * tiles + i) * 8, 8), 8) for i in range(tiles)]
        apart = pl.ds(e, n_src * left, stride=count)
        taken = [x[at, :].astype(jnp.float32) for x in xs for at in own]
        taken.append(jnp.concatenate([into[j, apart, :] for j in range(width // LANES)], axis=1))
        taken = jnp.concatenate(taken, axis=0).astype(jnp.bfloat16)
        gate_pre = jnp.dot(taken, wg[e], preferred_element_type=jnp.float32)
        upward = jnp.dot(taken, wu[e], preferred_element_type=jnp.float32)
        activated = clamped_unit(gate_pre, upward).astype(jnp.bfloat16)
        result = jnp.dot(activated, wd[e], preferred_element_type=jnp.float32)
        row = 0
        for out in outs:
            for at in own:
                out[at, :] = result[row : row + 8].astype(out.dtype)
                row += 8
        for j in range(width // LANES):
            outof[j, apart, :] = result[row:, j * LANES : (j + 1) * LANES]
        return carry

    lax.fori_loop(0, count, one, 0, unroll=EXPERT_UNROLL)
    for s, out in enumerate(outs):
        for j in range(width // LANES):
            cols = slice(j * LANES, (j + 1) * LANES)
            out[whole:, cols] = outof[j, s * left * count : (s + 1) * left * count, :].astype(
                out.dtype
            )


EXPERT_UNROLL = 2


def experts(xs, w_gate, w_up, w_down):
    count, width, hidden = w_gate.shape
    rows, n_src = xs[0].shape[0], len(xs)
    left = rows // count % 8
    scratch = pltpu.VMEM((width // LANES, n_src * left * count, LANES), jnp.float32)
    flops = 6 * n_src * rows * width * hidden
    moved_bytes = 3 * count * width * hidden * 2 + 4 * n_src * rows * width
    return pl.pallas_call(
        lambda *refs: experts_body(n_src, *refs),
        in_specs=[IN_VMEM] * (n_src + 3),
        out_specs=[IN_VMEM] * n_src,
        out_shape=[jax.ShapeDtypeStruct((rows, width), jnp.bfloat16)] * n_src,
        scratch_shapes=[scratch, scratch],
        cost_estimate=pl.CostEstimate(flops=flops, bytes_accessed=moved_bytes, transcendentals=0),
        compiler_params=pltpu.CompilerParams(vmem_limit_bytes=6 << 20),
        name="experts",
    )(*xs, w_gate, w_up, w_down)


def per_device(
    resid_in,
    pool_input,
    pool_weight,
    pool_scale,
    out_weight,
    mix_gain,
    ffn_gain,
    w_gate,
    w_up,
    w_down,
    routes,
    route_weight,
    post_gain,
):
    n_sp = lax.axis_size("sp")
    n_tp = lax.axis_size("tp")
    tok_rows, width = resid_in.shape
    channels = pool_input.shape[1]
    local_experts = w_gate.shape[0]
    n_experts = local_experts * n_sp
    assert n_experts <= 256
    slot_rows = local_experts * CAP
    slot_total = n_sp * slot_rows

    fields = jnp.concatenate([routes.astype(jnp.bfloat16).T, route_weight.astype(jnp.bfloat16).T])
    n_fields = fields.size
    field_rows = -(-n_fields // (8 * channels)) * 8
    fields = jnp.pad(fields.reshape(-1), (0, field_rows * channels - n_fields))
    fields = jnp.broadcast_to(fields.reshape(1, field_rows, channels), (n_tp, field_rows, channels))
    mixed_rows = mixed_window(pool_input).reshape(n_tp, tok_rows, channels)
    sent = jnp.concatenate([mixed_rows, fields], axis=1)
    got = lax.all_to_all(sent, "tp", split_axis=0, concat_axis=0, tiled=True)
    token_mixed = got[:, :tok_rows].transpose(1, 0, 2).reshape(tok_rows, n_tp * channels)
    fields = got[:, tok_rows:].reshape(n_tp, -1)[:, :n_fields].reshape(n_tp, 2 * TOP, tok_rows)

    pooled = jnp.einsum(
        "tgc,gcd->tgd",
        token_mixed.reshape(tok_rows, GROUPS, GROUP_DIM),
        pool_weight,
        preferred_element_type=jnp.float32,
    )
    pooled = (
        (pooled * pool_scale.reshape(GROUPS, GROUP_DIM)).astype(jnp.bfloat16).reshape(tok_rows, -1)
    )
    mix_out = jnp.dot(pooled, out_weight, preferred_element_type=jnp.float32)
    residual = (resid_in.astype(jnp.float32) + rms_scale(mix_out, mix_gain)).astype(jnp.bfloat16)
    normed = rms_scale(residual.astype(jnp.float32), ffn_gain).astype(jnp.bfloat16)

    order = [0] + [k for pair in zip(range(1, n_tp), range(n_tp - 1, 0, -1)) for k in pair]
    order = list(dict.fromkeys(order))
    blocks = {}
    for k in order:
        blocks[k] = rotated(normed, "tp", k) if k else normed

    here = lax.axis_index("tp")
    sp_here = lax.axis_index("sp")
    fields = jnp.take(fields, (here - jnp.array(order)) % n_tp, axis=0)
    route = fields[:, :TOP].astype(jnp.int32)
    weight = fields[:, TOP:].astype(jnp.float32)
    onehot = route[..., None] == lax.iota(jnp.int32, n_experts)
    named = jnp.sum(onehot.astype(jnp.float32), axis=1)
    earlier = lax.iota(jnp.int32, tok_rows)[:, None] > lax.iota(jnp.int32, tok_rows)[None, :]
    rank = jnp.einsum(
        "ut,bte->bue",
        earlier.astype(jnp.bfloat16),
        named.astype(jnp.bfloat16),
        preferred_element_type=jnp.float32,
    )
    slot_rank = jnp.sum(rank[:, None] * onehot, axis=-1).astype(jnp.int32)

    if local_experts % 8 == 0 and CAP % 8 and n_sp <= 4:
        owner = offset_to(route // local_experts, sp_here, n_sp)
        expert = route % local_experts
        whole = CAP // 8 * 8
        in_tile = expert * whole + slot_rank
        apart = (local_experts - expert) * whole + (slot_rank - whole) * local_experts + expert
        slot = owner * slot_rows + jnp.where(slot_rank < whole, in_tile, expert * whole + apart)
        by_row = slot.transpose(0, 2, 1)
        weight = weight.transpose(0, 2, 1)
        size = max(1, n_tp // 2)
        weights = load(w_gate, w_up, w_down)
        arrived, backs, parts = [], {}, []
        for at, k in enumerate(order):
            rows = pick(at, slot, blocks[k], n_sp, slot_rows)
            arrived.append([moved(x, "sp", d) if d else x for d, x in enumerate(rows)])
        for first in range(0, n_tp, size):
            group = arrived[first : first + size]
            terms = experts([x for xs in group for x in xs], *weights)
            for at in range(first, first + size):
                back = terms[(at - first) * n_sp : (at - first + 1) * n_sp]
                backs[at] = [moved(x, "sp", d, True) if d else x for d, x in enumerate(back)]
        for at, k in enumerate(order):
            if k:
                part = combine(at, by_row, weight, backs[at])
                parts.append(rotated(part, "tp", -k))
        return finish(0, by_row, weight, residual, post_gain, backs[0], parts)
    else:
        slot_index = route * CAP + slot_rank
        picker = slot_index[..., None] == lax.iota(jnp.int32, slot_total)
        token_pick = jnp.sum(picker.astype(jnp.float32), axis=1).astype(jnp.bfloat16)
        token_weight = jnp.sum(jnp.where(picker, weight[..., None], 0.0), axis=1)
        token_weight = token_weight.astype(jnp.bfloat16)
        arrived = []
        for at, k in enumerate(order):
            rows = lax.dot_general(
                token_pick[at],
                blocks[k],
                (((0,), (0,)), ((), ())),
                preferred_element_type=jnp.float32,
            )
            rows = rows.astype(jnp.bfloat16).reshape(n_sp, slot_rows, width)
            arrived.append(lax.all_to_all(rows, "sp", split_axis=0, concat_axis=0, tiled=True))
        arrived = jnp.stack(arrived).reshape(n_tp, n_sp, local_experts, CAP, width)
        f32 = {"preferred_element_type": jnp.float32}
        gate_pre = jnp.einsum("sklcd,ldf->sklcf", arrived, w_gate, **f32)
        upward = jnp.einsum("sklcd,ldf->sklcf", arrived, w_up, **f32)
        activated = clamped_unit(gate_pre, upward).astype(jnp.bfloat16)
        terms = jnp.einsum("sklcf,lfd->sklcd", activated, w_down, **f32)
        terms = terms.astype(jnp.bfloat16).reshape(n_tp, n_sp, slot_rows, width)
        parts = {}
        for at, k in enumerate(order):
            back = lax.all_to_all(terms[at], "sp", split_axis=0, concat_axis=0, tiled=True)
            part = jnp.dot(token_weight[at], back.reshape(slot_total, width), **f32)
            part = part.astype(jnp.bfloat16)
            parts[k] = rotated(part, "tp", -k) if k else part
    expert_mix = sum(parts[k].astype(jnp.float32) for k in order)
    return (residual.astype(jnp.float32) + rms_scale(expert_mix, post_gain)).astype(jnp.bfloat16)


def solution(mesh):
    in_specs = (
        P(("grp", "sp", "tp"), None),
        P(("grp", "sp"), "tp"),
        P(),
        P(),
        P(),
        P(),
        P(),
        P("sp", None, "tp"),
        P("sp", None, "tp"),
        P("sp", "tp", None),
        P(("grp", "sp", "tp"), None),
        P(("grp", "sp", "tp"), None),
        P(),
    )
    out_specs = P(("grp", "sp", "tp"), None)

    return jax.shard_map(
        per_device, mesh=mesh, in_specs=in_specs, out_specs=out_specs, check_vma=False
    )
```

profile of v0, /device:TPU:0, one launch (start us, length us, event | category | flops | bytes accessed | tf_op | source)
XLA Modules:
  0.0 196.1 jit_solution(4153755031348712463)
XLA Ops:
  0.8 2.4 %collective-permute-start = (bf16[15,256]{1,0:T(8,128)(2,1)S(1)}, bf16[15,256]{1,0:T(8,128)(2,1)S(1)}, u32[]{:S(2)}, u32[]{:S(2)}) collective-permute-start(bf16[15,256]{1,0:T(8,128)(2,1)S(1)} %slice.67), channel_id=1, source_target_pairs={{0,4},{4,8},{8,12},{1,5},{5,9},{9,13},{2,6},{6,10},{10,14},{3,7},{... | collective-permute-start | bytes 23048 | tf_op jit(solution)/shard_map/ppermute | solution.py:25
  7.3 5.7 %all-to-all-start = ((bf16[4,136,256]{2,1,0:T(8,128)(2,1)}), bf16[4,136,256]{2,1,0:T(8,128)(2,1)S(1)}, u32[]{:S(2)}, u32[]{:S(2)}) async-start(bf16[4,136,256]{2,1,0:T(8,128)(2,1)} %pad_maximum_fusion), calls=%async_computation | async-start | bytes 557056 | tf_op jit(solution)/shard_map/all_to_all | solution.py:302
  13.0 10.0 %all-to-all-done = bf16[4,136,256]{2,1,0:T(8,128)(2,1)S(1)} async-done(((bf16[4,136,256]{2,1,0:T(8,128)(2,1)}), bf16[4,136,256]{2,1,0:T(8,128)(2,1)S(1)}, u32[]{:S(2)}, u32[]{:S(2)}) %all-to-all-start) | async-done | bytes 278560 | tf_op jit(solution)/shard_map/all_to_all | solution.py:302
  24.5 3.0 %multiply_reduce_fusion = (f32[128]{0:T(128)S(1)}, f32[128,2048]{1,0:T(8,128)S(1)}) fusion(bf16[128,1024]{0,1:T(8,128)(2,1)S(1)} %bitcast.38, bf16[1024,2048]{1,0:T(8,128)(2,1)} %param.18), kind=kOutput, calls=%fused_computation.11 | convolution fusion | flops 537395072 | bytes 5505536 | tf_op jit(solution)/shard_map/dot_general | solution.py:315
  28.2 1.7 collective-permute-start.15
  32.2 1.3 fusion.11
  34.2 8.7 %collective-permute-done.15.refs_1_ = bf16[128,2048]{1,0:T(8,128)(2,1)S(1)} collective-permute-done((bf16[128,2048]{1,0:T(8,128)(2,1)S(1)}, bf16[128,2048]{1,0:T(8,128)(2,1)S(1)}, u32[]{:S(2)}, u32[]{:S(2)}) %collective-permute-start.15) | collective-permute-done | bytes 524320 | tf_op jit(solution)/shard_map/ppermute | solution.py:30
  43.5 32.0 %collective-permute-done.19.refs_1_ = bf16[128,2048]{1,0:T(8,128)(2,1)S(1)} collective-permute-done((bf16[128,2048]{1,0:T(8,128)(2,1)S(1)}, bf16[128,2048]{1,0:T(8,128)(2,1)S(1)}, u32[]{:S(2)}, u32[]{:S(2)}) %collective-permute-start.19) | collective-permute-done | bytes 524320 | tf_op jit(solution)/shard_map/ppermute | solution.py:30
  76.1 2.1 %collective-permute-start.21 = (bf16[72,2048]{1,0:T(8,128)(2,1)S(1)}, bf16[72,2048]{1,0:T(8,128)(2,1)S(1)}, u32[]{:S(2)}, u32[]{:S(2)}) collective-permute-start(bf16[72,2048]{1,0:T(8,128)(2,1)S(1)} %get-tuple-element.65), channel_id=1, source_target_pairs={{0,8},{4,12},{8,0},{12,4},{1,9},{5,13},{9,1},{13,5},{2,10},{6,14},... | collective-permute-start | bytes 884744 | tf_op jit(solution)/shard_map/ppermute | solution.py:76
  78.7 1.5 collective-permute-start.2
  80.2 4.6 %collective-permute-done.18.refs_3_ = bf16[72,2048]{1,0:T(8,128)(2,1)S(1)} collective-permute-done((bf16[72,2048]{1,0:T(8,128)(2,1)S(1)}, bf16[72,2048]{1,0:T(8,128)(2,1)S(1)}, u32[]{:S(2)}, u32[]{:S(2)}) %collective-permute-start.18) | collective-permute-done | bytes 294944 | tf_op jit(solution)/shard_map/ppermute | solution.py:76
  84.9 5.7 %collective-permute-done.21.refs_6_ = bf16[72,2048]{1,0:T(8,128)(2,1)S(1)} collective-permute-done((bf16[72,2048]{1,0:T(8,128)(2,1)S(1)}, bf16[72,2048]{1,0:T(8,128)(2,1)S(1)}, u32[]{:S(2)}, u32[]{:S(2)}) %collective-permute-start.21) | collective-permute-done | bytes 294944 | tf_op jit(solution)/shard_map/ppermute | solution.py:76
  90.6 1.2 collective-permute-start.6
  91.8 8.4 %load.1 = (bf16[8,2048,256]{2,1,0:T(8,128)(2,1)S(1)}, bf16[8,2048,256]{2,1,0:T(8,128)(2,1)S(1)}, bf16[8,256,2048]{2,1,0:T(8,128)(2,1)S(1)}) custom-call(bf16[8,2048,256]{2,1,0:T(8,128)(2,1)} %refs_0_.1, bf16[8,2048,256]{2,1,0:T(8,128)(2,1)} %refs_1_.1, bf16[8,256,2048]{2,1,0:T(8,128)(2,1)} %refs_2_.1), custom_call_target="tpu_custom_call" | custom-call | tf_op jit(solution)/shard_map/load/pallas_call | solution.py:101
  100.8 6.4 %experts.3 = (bf16[72,2048]{1,0:T(8,128)(2,1)S(1)}, bf16[72,2048]{1,0:T(8,128)(2,1)S(1)}, bf16[72,2048]{1,0:T(8,128)(2,1)S(1)}, bf16[72,2048]{1,0:T(8,128)(2,1)}...) custom-call(bf16[72,2048]{1,0:T(8,128)(2,1)S(1)} %get-tuple-element., ...), custom_call_target="tpu_custom_call" | custom-call | flops 1811939328 | bytes 29884416 | tf_op jit(solution)/shard_map/experts/pallas_call | solution.py:258
  107.6 2.5 %collective-permute-done.3.refs_3_ = bf16[72,2048]{1,0:T(8,128)(2,1)S(1)} collective-permute-done((bf16[72,2048]{1,0:T(8,128)(2,1)S(1)}, bf16[72,2048]{1,0:T(8,128)(2,1)S(1)}, u32[]{:S(2)}, u32[]{:S(2)}) %collective-permute-start.3) | collective-permute-done | bytes 294944 | tf_op jit(solution)/shard_map/ppermute | solution.py:76
  111.0 4.8 %collective-permute-done.6.refs_6_ = bf16[72,2048]{1,0:T(8,128)(2,1)S(1)} collective-permute-done((bf16[72,2048]{1,0:T(8,128)(2,1)S(1)}, bf16[72,2048]{1,0:T(8,128)(2,1)S(1)}, u32[]{:S(2)}, u32[]{:S(2)}) %collective-permute-start.6) | collective-permute-done | bytes 294944 | tf_op jit(solution)/shard_map/ppermute | solution.py:76
  116.3 6.5 %collective-permute-done.7.refs_7_ = bf16[72,2048]{1,0:T(8,128)(2,1)S(1)} collective-permute-done((bf16[72,2048]{1,0:T(8,128)(2,1)S(1)}, bf16[72,2048]{1,0:T(8,128)(2,1)S(1)}, u32[]{:S(2)}, u32[]{:S(2)}) %collective-permute-start.7) | collective-permute-done | bytes 294944 | tf_op jit(solution)/shard_map/ppermute | solution.py:76
  122.8 6.7 %experts.2 = (bf16[72,2048]{1,0:T(8,128)(2,1)S(1)}, bf16[72,2048]{1,0:T(8,128)(2,1)S(1)}, bf16[72,2048]{1,0:T(8,128)(2,1)S(1)}, bf16[72,2048]{1,0:T(8,128)(2,1)}...) custom-call(bf16[72,2048]{1,0:T(8,128)(2,1)S(1)} %get-tuple-element., ...), custom_call_target="tpu_custom_call" | custom-call | flops 1811939328 | bytes 29884416 | tf_op jit(solution)/shard_map/experts/pallas_call | solution.py:258
  130.4 1.3 collective-permute-start.11
  131.7 3.7 %collective-permute-done.29.refs_5_ = bf16[72,2048]{1,0:T(8,128)(2,1)S(1)} collective-permute-done((bf16[72,2048]{1,0:T(8,128)(2,1)S(1)}, bf16[72,2048]{1,0:T(8,128)(2,1)S(1)}, u32[]{:S(2)}, u32[]{:S(2)}) %collective-permute-start.29) | collective-permute-done | bytes 294944 | tf_op jit(solution)/shard_map/ppermute | solution.py:76
  137.7 3.4 %collective-permute-done.24.refs_4_ = bf16[72,2048]{1,0:T(8,128)(2,1)S(1)} collective-permute-done((bf16[72,2048]{1,0:T(8,128)(2,1)S(1)}, bf16[72,2048]{1,0:T(8,128)(2,1)S(1)}, u32[]{:S(2)}, u32[]{:S(2)}) %collective-permute-start.24) | collective-permute-done | bytes 294944 | tf_op jit(solution)/shard_map/ppermute | solution.py:76
  143.8 4.4 %collective-permute-done.25.refs_5_ = bf16[72,2048]{1,0:T(8,128)(2,1)} collective-permute-done((bf16[72,2048]{1,0:T(8,128)(2,1)}, bf16[72,2048]{1,0:T(8,128)(2,1)}, u32[]{:S(2)}, u32[]{:S(2)}) %collective-permute-start.25) | collective-permute-done | bytes 294944 | tf_op jit(solution)/shard_map/ppermute | solution.py:76
  150.1 1.8 combine.4
  151.9 1.9 collective-permute-done.12.refs_4_
  153.9 6.9 %collective-permute-done.13.refs_5_ = bf16[72,2048]{1,0:T(8,128)(2,1)} collective-permute-done((bf16[72,2048]{1,0:T(8,128)(2,1)}, bf16[72,2048]{1,0:T(8,128)(2,1)}, u32[]{:S(2)}, u32[]{:S(2)}) %collective-permute-start.13) | collective-permute-done | bytes 294944 | tf_op jit(solution)/shard_map/ppermute | solution.py:76
  160.8 1.9 combine.3
  162.9 3.9 %collective-permute-done.10.refs_7_ = bf16[72,2048]{1,0:T(8,128)(2,1)} collective-permute-done((bf16[72,2048]{1,0:T(8,128)(2,1)}, bf16[72,2048]{1,0:T(8,128)(2,1)}, u32[]{:S(2)}, u32[]{:S(2)}) %collective-permute-start.10) | collective-permute-done | bytes 294944 | tf_op jit(solution)/shard_map/ppermute | solution.py:76
  166.8 8.9 %collective-permute-done.9.refs_6_ = bf16[72,2048]{1,0:T(8,128)(2,1)S(1)} collective-permute-done((bf16[72,2048]{1,0:T(8,128)(2,1)}, bf16[72,2048]{1,0:T(8,128)(2,1)S(1)}, u32[]{:S(2)}, u32[]{:S(2)}) %collective-permute-start.9) | collective-permute-done | bytes 294944 | tf_op jit(solution)/shard_map/ppermute | solution.py:76
  175.8 6.4 %collective-permute-done.30.refs_10_ = bf16[128,2048]{1,0:T(8,128)(2,1)S(1)} collective-permute-done((bf16[128,2048]{1,0:T(8,128)(2,1)S(1)}, bf16[128,2048]{1,0:T(8,128)(2,1)S(1)}, u32[]{:S(2)}, u32[]{:S(2)}) %collective-permute-start.30) | collective-permute-done | bytes 524320 | tf_op jit(solution)/shard_map/ppermute | solution.py:30
  182.2 11.1 %collective-permute-done.14.refs_8_ = bf16[128,2048]{1,0:T(8,128)(2,1)S(1)} collective-permute-done((bf16[128,2048]{1,0:T(8,128)(2,1)S(1)}, bf16[128,2048]{1,0:T(8,128)(2,1)S(1)}, u32[]{:S(2)}, u32[]{:S(2)}) %collective-permute-start.14) | collective-permute-done | bytes 524320 | tf_op jit(solution)/shard_map/ppermute | solution.py:30
  193.3 2.8 %finish.1 = bf16[128,2048]{1,0:T(8,128)(2,1)} custom-call(s32[4,128,2]{2,1,0:T(8,128)S(1)} %bitcast.31, f32[4,128,2]{2,1,0:T(8,128)S(1)} %bitcast.35, bf16[128,2048]{1,0:T(8,128)(2,1)S(1)} %get-tuple-element.76.refs_2_, f32[1,2048]{1,0:T(1,128)S(1)} %bitcast.36, bf16[72,2048]{1,0:T(8,128)(2,1)S(1)} %get-tuple-element.51.refs_4_, ...), custom_call_target="tpu_custom_call" | custom-call | tf_op jit(solution)/shard_map/finish/pallas_call | solution.py:196
  (123 shorter events, 21.7 us)
Async XLA Ops:
  0.8 3.9 %collective-permute-start = (bf16[15,256]{1,0:T(8,128)(2,1)S(1)}, bf16[15,256]{1,0:T(8,128)(2,1)S(1)}, u32[]{:S(2)}, u32[]{:S(2)}) collective-permute-start(bf16[15,256]{1,0:T(8,128)(2,1)S(1)} %slice.67), channel_id=1, source_target_pairs={{0,4},{4,8},{8,12},{1,5},{5,9},{9,13},{2,6},{6,10},{10,14},{3,7},{... | collective-permute-start | bytes 23048 | tf_op jit(solution)/shard_map/ppermute | solution.py:25
  7.3 15.8 %all-to-all-start = ((bf16[4,136,256]{2,1,0:T(8,128)(2,1)}), bf16[4,136,256]{2,1,0:T(8,128)(2,1)S(1)}, u32[]{:S(2)}, u32[]{:S(2)}) async-start(bf16[4,136,256]{2,1,0:T(8,128)(2,1)} %pad_maximum_fusion), calls=%async_computation | async-start | bytes 557056 | tf_op jit(solution)/shard_map/all_to_all | solution.py:302
  28.2 14.8 %collective-permute-start.15 = (bf16[128,2048]{1,0:T(8,128)(2,1)S(1)}, bf16[128,2048]{1,0:T(8,128)(2,1)S(1)}, u32[]{:S(2)}, u32[]{:S(2)}) collective-permute-start(bf16[128,2048]{1,0:T(8,128)(2,1)S(1)} %fusion.4.refs_1_), channel_id=1, source_target_pairs={{0,3},{1,0},{2,1},{3,2},{4,7},{5,4},{6,5},{7,6},{8,11},{9,8},{10,9... | collective-permute-start | bytes 1572872 | tf_op jit(solution)/shard_map/ppermute | solution.py:30
  29.9 45.6 %collective-permute-start.19 = (bf16[128,2048]{1,0:T(8,128)(2,1)S(1)}, bf16[128,2048]{1,0:T(8,128)(2,1)S(1)}, u32[]{:S(2)}, u32[]{:S(2)}) collective-permute-start(bf16[128,2048]{1,0:T(8,128)(2,1)S(1)} %fusion.4.refs_1_), channel_id=1, source_target_pairs={{0,2},{1,3},{2,0},{3,1},{4,6},{5,7},{6,4},{7,5},{8,10},{9,11},{10,... | collective-permute-start | bytes 1572872 | tf_op jit(solution)/shard_map/ppermute | solution.py:30
  29.9 46.2 %collective-permute-start.4 = (bf16[128,2048]{1,0:T(8,128)(2,1)S(1)}, bf16[128,2048]{1,0:T(8,128)(2,1)S(1)}, u32[]{:S(2)}, u32[]{:S(2)}) collective-permute-start(bf16[128,2048]{1,0:T(8,128)(2,1)S(1)} %fusion.4.refs_1_), channel_id=1, source_target_pairs={{0,1},{1,2},{2,3},{3,0},{4,5},{5,6},{6,7},{7,4},{8,9},{9,10},{10,1... | collective-permute-start | bytes 1572872 | tf_op jit(solution)/shard_map/ppermute | solution.py:30
  34.1 41.9 %collective-permute-start.1 = (bf16[72,2048]{1,0:T(8,128)(2,1)S(1)}, bf16[72,2048]{1,0:T(8,128)(2,1)S(1)}, u32[]{:S(2)}, u32[]{:S(2)}) collective-permute-start(bf16[72,2048]{1,0:T(8,128)(2,1)S(1)} %get-tuple-element.41), channel_id=1, source_target_pairs={{0,4},{4,0},{8,12},{12,8},{1,5},{5,1},{9,13},{13,9},{2,6},{6,2},{1... | collective-permute-start | bytes 884744 | tf_op jit(solution)/shard_map/ppermute | solution.py:76
  43.4 34.9 %collective-permute-start.16 = (bf16[72,2048]{1,0:T(8,128)(2,1)S(1)}, bf16[72,2048]{1,0:T(8,128)(2,1)S(1)}, u32[]{:S(2)}, u32[]{:S(2)}) collective-permute-start(bf16[72,2048]{1,0:T(8,128)(2,1)S(1)} %get-tuple-element.60), channel_id=1, source_target_pairs={{0,4},{4,0},{8,12},{12,8},{1,5},{5,1},{9,13},{13,9},{2,6},{6,2},{1... | collective-permute-start | bytes 884744 | tf_op jit(solution)/shard_map/ppermute | solution.py:76
  43.5 35.3 %collective-permute-start.17 = (bf16[72,2048]{1,0:T(8,128)(2,1)S(1)}, bf16[72,2048]{1,0:T(8,128)(2,1)S(1)}, u32[]{:S(2)}, u32[]{:S(2)}) collective-permute-start(bf16[72,2048]{1,0:T(8,128)(2,1)S(1)} %get-tuple-element.61), channel_id=1, source_target_pairs={{0,8},{4,12},{8,0},{12,4},{1,9},{5,13},{9,1},{13,5},{2,10},{6,14},... | collective-permute-start | bytes 884744 | tf_op jit(solution)/shard_map/ppermute | solution.py:76
  75.5 9.3 %collective-permute-start.18 = (bf16[72,2048]{1,0:T(8,128)(2,1)S(1)}, bf16[72,2048]{1,0:T(8,128)(2,1)S(1)}, u32[]{:S(2)}, u32[]{:S(2)}) collective-permute-start(bf16[72,2048]{1,0:T(8,128)(2,1)S(1)} %get-tuple-element.62), channel_id=1, source_target_pairs={{0,12},{4,8},{8,4},{12,0},{1,13},{5,9},{9,5},{13,1},{2,14},{6,10},... | collective-permute-start | bytes 884744 | tf_op jit(solution)/shard_map/ppermute | solution.py:76
  76.0 8.8 %collective-permute-start.20 = (bf16[72,2048]{1,0:T(8,128)(2,1)S(1)}, bf16[72,2048]{1,0:T(8,128)(2,1)S(1)}, u32[]{:S(2)}, u32[]{:S(2)}) collective-permute-start(bf16[72,2048]{1,0:T(8,128)(2,1)S(1)} %get-tuple-element.64), channel_id=1, source_target_pairs={{0,4},{4,0},{8,12},{12,8},{1,5},{5,1},{9,13},{13,9},{2,6},{6,2},{1... | collective-permute-start | bytes 884744 | tf_op jit(solution)/shard_map/ppermute | solution.py:76
  76.1 14.5 %collective-permute-start.21 = (bf16[72,2048]{1,0:T(8,128)(2,1)S(1)}, bf16[72,2048]{1,0:T(8,128)(2,1)S(1)}, u32[]{:S(2)}, u32[]{:S(2)}) collective-permute-start(bf16[72,2048]{1,0:T(8,128)(2,1)S(1)} %get-tuple-element.65), channel_id=1, source_target_pairs={{0,8},{4,12},{8,0},{12,4},{1,9},{5,13},{9,1},{13,5},{2,10},{6,14},... | collective-permute-start | bytes 884744 | tf_op jit(solution)/shard_map/ppermute | solution.py:76
  78.2 21.9 %collective-permute-start.22 = (bf16[72,2048]{1,0:T(8,128)(2,1)S(1)}, bf16[72,2048]{1,0:T(8,128)(2,1)S(1)}, u32[]{:S(2)}, u32[]{:S(2)}) collective-permute-start(bf16[72,2048]{1,0:T(8,128)(2,1)S(1)} %get-tuple-element.66), channel_id=1, source_target_pairs={{0,12},{4,8},{8,4},{12,0},{1,13},{5,9},{9,5},{13,1},{2,14},{6,10},... | collective-permute-start | bytes 884744 | tf_op jit(solution)/shard_map/ppermute | solution.py:76
  78.7 28.5 %collective-permute-start.2 = (bf16[72,2048]{1,0:T(8,128)(2,1)S(1)}, bf16[72,2048]{1,0:T(8,128)(2,1)S(1)}, u32[]{:S(2)}, u32[]{:S(2)}) collective-permute-start(bf16[72,2048]{1,0:T(8,128)(2,1)S(1)} %get-tuple-element.42), channel_id=1, source_target_pairs={{0,8},{4,12},{8,0},{12,4},{1,9},{5,13},{9,1},{13,5},{2,10},{6,14},... | collective-permute-start | bytes 884744 | tf_op jit(solution)/shard_map/ppermute | solution.py:76
  84.9 25.3 %collective-permute-start.3 = (bf16[72,2048]{1,0:T(8,128)(2,1)S(1)}, bf16[72,2048]{1,0:T(8,128)(2,1)S(1)}, u32[]{:S(2)}, u32[]{:S(2)}) collective-permute-start(bf16[72,2048]{1,0:T(8,128)(2,1)S(1)} %get-tuple-element.43), channel_id=1, source_target_pairs={{0,12},{4,8},{8,4},{12,0},{1,13},{5,9},{9,5},{13,1},{2,14},{6,10},... | collective-permute-start | bytes 884744 | tf_op jit(solution)/shard_map/ppermute | solution.py:76
  84.9 25.3 %collective-permute-start.5 = (bf16[72,2048]{1,0:T(8,128)(2,1)S(1)}, bf16[72,2048]{1,0:T(8,128)(2,1)S(1)}, u32[]{:S(2)}, u32[]{:S(2)}) collective-permute-start(bf16[72,2048]{1,0:T(8,128)(2,1)S(1)} %get-tuple-element.45), channel_id=1, source_target_pairs={{0,4},{4,0},{8,12},{12,8},{1,5},{5,1},{9,13},{13,9},{2,6},{6,2},{1... | collective-permute-start | bytes 884744 | tf_op jit(solution)/shard_map/ppermute | solution.py:76
  90.6 25.3 %collective-permute-start.6 = (bf16[72,2048]{1,0:T(8,128)(2,1)S(1)}, bf16[72,2048]{1,0:T(8,128)(2,1)S(1)}, u32[]{:S(2)}, u32[]{:S(2)}) collective-permute-start(bf16[72,2048]{1,0:T(8,128)(2,1)S(1)} %get-tuple-element.46), channel_id=1, source_target_pairs={{0,8},{4,12},{8,0},{12,4},{1,9},{5,13},{9,1},{13,5},{2,10},{6,14},... | collective-permute-start | bytes 884744 | tf_op jit(solution)/shard_map/ppermute | solution.py:76
  100.2 22.6 %collective-permute-start.7 = (bf16[72,2048]{1,0:T(8,128)(2,1)S(1)}, bf16[72,2048]{1,0:T(8,128)(2,1)S(1)}, u32[]{:S(2)}, u32[]{:S(2)}) collective-permute-start(bf16[72,2048]{1,0:T(8,128)(2,1)S(1)} %get-tuple-element.47), channel_id=1, source_target_pairs={{0,12},{4,8},{8,4},{12,0},{1,13},{5,9},{9,5},{13,1},{2,14},{6,10},... | collective-permute-start | bytes 884744 | tf_op jit(solution)/shard_map/ppermute | solution.py:76
  107.2 22.3 %collective-permute-start.27 = (bf16[72,2048]{1,0:T(8,128)(2,1)S(1)}, bf16[72,2048]{1,0:T(8,128)(2,1)S(1)}, u32[]{:S(2)}, u32[]{:S(2)}) collective-permute-start(bf16[72,2048]{1,0:T(8,128)(2,1)S(1)} %get-tuple-element.72), channel_id=1, source_target_pairs={{4,0},{0,4},{12,8},{8,12},{5,1},{1,5},{13,9},{9,13},{6,2},{2,6},{1... | collective-permute-start | bytes 884744 | tf_op jit(solution)/shard_map/ppermute | solution.py:76
  110.1 20.3 %collective-permute-start.28 = (bf16[72,2048]{1,0:T(8,128)(2,1)S(1)}, bf16[72,2048]{1,0:T(8,128)(2,1)S(1)}, u32[]{:S(2)}, u32[]{:S(2)}) collective-permute-start(bf16[72,2048]{1,0:T(8,128)(2,1)S(1)} %get-tuple-element.73), channel_id=1, source_target_pairs={{8,0},{12,4},{0,8},{4,12},{9,1},{13,5},{1,9},{5,13},{10,2},{14,6},... | collective-permute-start | bytes 884744 | tf_op jit(solution)/shard_map/ppermute | solution.py:76
  110.1 25.3 %collective-permute-start.29 = (bf16[72,2048]{1,0:T(8,128)(2,1)S(1)}, bf16[72,2048]{1,0:T(8,128)(2,1)S(1)}, u32[]{:S(2)}, u32[]{:S(2)}) collective-permute-start(bf16[72,2048]{1,0:T(8,128)(2,1)S(1)} %get-tuple-element.74), channel_id=1, source_target_pairs={{12,0},{8,4},{4,8},{0,12},{13,1},{9,5},{5,9},{1,13},{14,2},{10,6},... | collective-permute-start | bytes 884744 | tf_op jit(solution)/shard_map/ppermute | solution.py:76
  115.9 20.3 %collective-permute-start.23 = (bf16[72,2048]{1,0:T(8,128)(2,1)S(1)}, bf16[72,2048]{1,0:T(8,128)(2,1)S(1)}, u32[]{:S(2)}, u32[]{:S(2)}) collective-permute-start(bf16[72,2048]{1,0:T(8,128)(2,1)S(1)} %get-tuple-element.68), channel_id=1, source_target_pairs={{4,0},{0,4},{12,8},{8,12},{5,1},{1,5},{13,9},{9,13},{6,2},{2,6},{1... | collective-permute-start | bytes 884744 | tf_op jit(solution)/shard_map/ppermute | solution.py:76
  122.8 18.4 %collective-permute-start.24 = (bf16[72,2048]{1,0:T(8,128)(2,1)S(1)}, bf16[72,2048]{1,0:T(8,128)(2,1)S(1)}, u32[]{:S(2)}, u32[]{:S(2)}) collective-permute-start(bf16[72,2048]{1,0:T(8,128)(2,1)S(1)} %get-tuple-element.69), channel_id=1, source_target_pairs={{8,0},{12,4},{0,8},{4,12},{9,1},{13,5},{1,9},{5,13},{10,2},{14,6},... | collective-permute-start | bytes 884744 | tf_op jit(solution)/shard_map/ppermute | solution.py:76
  129.5 18.6 %collective-permute-start.25 = (bf16[72,2048]{1,0:T(8,128)(2,1)}, bf16[72,2048]{1,0:T(8,128)(2,1)}, u32[]{:S(2)}, u32[]{:S(2)}) collective-permute-start(bf16[72,2048]{1,0:T(8,128)(2,1)} %get-tuple-element.70), channel_id=1, source_target_pairs={{12,0},{8,4},{4,8},{0,12},{13,1},{9,5},{5,9},{1,13},{14,2},{10,6},... | collective-permute-start | bytes 884744 | tf_op jit(solution)/shard_map/ppermute | solution.py:76
  130.4 21.4 %collective-permute-start.11 = (bf16[72,2048]{1,0:T(8,128)(2,1)}, bf16[72,2048]{1,0:T(8,128)(2,1)}, u32[]{:S(2)}, u32[]{:S(2)}) collective-permute-start(bf16[72,2048]{1,0:T(8,128)(2,1)} %get-tuple-element.56), channel_id=1, source_target_pairs={{4,0},{0,4},{12,8},{8,12},{5,1},{1,5},{13,9},{9,13},{6,2},{2,6},{1... | collective-permute-start | bytes 884744 | tf_op jit(solution)/shard_map/ppermute | solution.py:76
  136.1 17.8 %collective-permute-start.12 = (bf16[72,2048]{1,0:T(8,128)(2,1)}, bf16[72,2048]{1,0:T(8,128)(2,1)}, u32[]{:S(2)}, u32[]{:S(2)}) collective-permute-start(bf16[72,2048]{1,0:T(8,128)(2,1)} %get-tuple-element.57), channel_id=1, source_target_pairs={{8,0},{12,4},{0,8},{4,12},{9,1},{13,5},{1,9},{5,13},{10,2},{14,6},... | collective-permute-start | bytes 884744 | tf_op jit(solution)/shard_map/ppermute | solution.py:76
  136.8 24.0 %collective-permute-start.13 = (bf16[72,2048]{1,0:T(8,128)(2,1)}, bf16[72,2048]{1,0:T(8,128)(2,1)}, u32[]{:S(2)}, u32[]{:S(2)}) collective-permute-start(bf16[72,2048]{1,0:T(8,128)(2,1)} %get-tuple-element.58), channel_id=1, source_target_pairs={{12,0},{8,4},{4,8},{0,12},{13,1},{9,5},{5,9},{1,13},{14,2},{10,6},... | collective-permute-start | bytes 884744 | tf_op jit(solution)/shard_map/ppermute | solution.py:76
  141.9 25.0 %collective-permute-start.10 = (bf16[72,2048]{1,0:T(8,128)(2,1)}, bf16[72,2048]{1,0:T(8,128)(2,1)}, u32[]{:S(2)}, u32[]{:S(2)}) collective-permute-start(bf16[72,2048]{1,0:T(8,128)(2,1)} %get-tuple-element.54), channel_id=1, source_target_pairs={{12,0},{8,4},{4,8},{0,12},{13,1},{9,5},{5,9},{1,13},{14,2},{10,6},... | collective-permute-start | bytes 884744 | tf_op jit(solution)/shard_map/ppermute | solution.py:76
  148.2 34.0 %collective-permute-start.30 = (bf16[128,2048]{1,0:T(8,128)(2,1)S(1)}, bf16[128,2048]{1,0:T(8,128)(2,1)S(1)}, u32[]{:S(2)}, u32[]{:S(2)}) collective-permute-start(bf16[128,2048]{1,0:T(8,128)(2,1)S(1)} %combine.5), channel_id=1, source_target_pairs={{0,2},{1,3},{2,0},{3,1},{4,6},{5,7},{6,4},{7,5},{8,10},{9,11},{10,... | collective-permute-start | bytes 1572872 | tf_op jit(solution)/shard_map/ppermute | solution.py:30
  151.9 30.3 %collective-permute-start.26 = (bf16[128,2048]{1,0:T(8,128)(2,1)S(1)}, bf16[128,2048]{1,0:T(8,128)(2,1)S(1)}, u32[]{:S(2)}, u32[]{:S(2)}) collective-permute-start(bf16[128,2048]{1,0:T(8,128)(2,1)S(1)} %combine.4), channel_id=1, source_target_pairs={{0,1},{1,2},{2,3},{3,0},{4,5},{5,6},{6,7},{7,4},{8,9},{9,10},{10,1... | collective-permute-start | bytes 1572872 | tf_op jit(solution)/shard_map/ppermute | solution.py:30
  162.7 30.5 %collective-permute-start.14 = (bf16[128,2048]{1,0:T(8,128)(2,1)S(1)}, bf16[128,2048]{1,0:T(8,128)(2,1)S(1)}, u32[]{:S(2)}, u32[]{:S(2)}) collective-permute-start(bf16[128,2048]{1,0:T(8,128)(2,1)S(1)} %combine.3), channel_id=1, source_target_pairs={{0,3},{1,0},{2,1},{3,2},{4,7},{5,4},{6,5},{7,6},{8,11},{9,8},{10,9... | collective-permute-start | bytes 1572872 | tf_op jit(solution)/shard_map/ppermute | solution.py:30
  162.8 4.0 %collective-permute-start.8 = (bf16[72,2048]{1,0:T(8,128)(2,1)}, bf16[72,2048]{1,0:T(8,128)(2,1)S(1)}, u32[]{:S(2)}, u32[]{:S(2)}) collective-permute-start(bf16[72,2048]{1,0:T(8,128)(2,1)} %copy-done.10), channel_id=1, source_target_pairs={{4,0},{0,4},{12,8},{8,12},{5,1},{1,5},{13,9},{9,13},{6,2},{2,6},{1... | collective-permute-start | bytes 884744 | tf_op jit(solution)/shard_map/ppermute | solution.py:76
  166.8 8.9 %collective-permute-start.9 = (bf16[72,2048]{1,0:T(8,128)(2,1)}, bf16[72,2048]{1,0:T(8,128)(2,1)S(1)}, u32[]{:S(2)}, u32[]{:S(2)}) collective-permute-start(bf16[72,2048]{1,0:T(8,128)(2,1)} %copy-done.9), channel_id=1, source_target_pairs={{8,0},{12,4},{0,8},{4,12},{9,1},{13,5},{1,9},{5,13},{10,2},{14,6},... | collective-permute-start | bytes 884744 | tf_op jit(solution)/shard_map/ppermute | solution.py:76
  (16 other events, 289.5 us)
where the time goes:
time: 197 us; the launch traced here: 196 us
  waiting for transfers between devices  126 us (64%)
  Pallas kernels  30.7 us (16%)
  starting transfers between devices  21.1 us (11%)
  local copies, waits for them, and re-layouts  8.51 us (4%)
  other arithmetic  6.2 us (3%)
  matrix products  3.38 us (2%)
    ppermute x6, waiting for transfers between devices, rotated(): return lax.ppermute(x, axis, [(i, (i + by) % size) for i in range(size)])  58.2 us
    ppermute x24, waiting for transfers between devices, moved(): return lax.ppermute(x, axis, [(b, a) for a, b in pairs] if back else pairs)  57.5 us
    pallas_call x2, Pallas kernels, experts(): pl.pallas_call(lambda *refs: experts_body(n_src, *refs), in_specs=[IN_VME...  13.1 us
    ppermute x24, starting transfers between devices, moved(): return lax.ppermute(x, axis, [(b, a) for a, b in pairs] if back else pairs)  10.6 us
    all_to_all x1, waiting for transfers between devices, per_device(): got = lax.all_to_all(sent, 'tp', split_axis=0, concat_axis=0, tiled=True)  10 us
    pallas_call x1, Pallas kernels, load(): pl.pallas_call(load_body, in_specs=[pl.BlockSpec(memory_space=pltpu.HBM)]...  8.38 us
    all_to_all x1, starting transfers between devices, per_device(): got = lax.all_to_all(sent, 'tp', split_axis=0, concat_axis=0, tiled=True)  5.69 us
    unnamed x34, local copies, waits for them, and re-layouts  5.07 us
  transfers between devices with their start and end apart: 32, of which 17 were waited for; matrix products, arithmetic and copies ran while one was open for 2% of the time, Pallas kernels for 14%

commit v1 on v0

--- a/solution.py
+++ b/solution.py
@@ -347,16 +347,16 @@
         slot = owner * slot_rows + jnp.where(slot_rank < whole, in_tile, expert * whole + apart)
         by_row = slot.transpose(0, 2, 1)
         weight = weight.transpose(0, 2, 1)
-        size = max(1, n_tp // 2)
+        slot, by_row, weight = lax.optimization_barrier((slot, by_row, weight))
         weights = load(w_gate, w_up, w_down)
         arrived, backs, parts = [], {}, []
         for at, k in enumerate(order):
             rows = pick(at, slot, blocks[k], n_sp, slot_rows)
             arrived.append([moved(x, "sp", d) if d else x for d, x in enumerate(rows)])
-        for first in range(0, n_tp, size):
-            group = arrived[first : first + size]
+        for first, stop in groups_of(n_tp):
+            group = arrived[first:stop]
             terms = experts([x for xs in group for x in xs], *weights)
-            for at in range(first, first + size):
+            for at in range(first, stop):
                 back = terms[(at - first) * n_sp : (at - first + 1) * n_sp]
                 backs[at] = [moved(x, "sp", d, True) if d else x for d, x in enumerate(back)]
         for at, k in enumerate(order):
@@ -397,6 +397,11 @@
     return (residual.astype(jnp.float32) + rms_scale(expert_mix, post_gain)).astype(jnp.bfloat16)
 
 
+def groups_of(n_tp):
+    first = min(2, n_tp)
+    return [(0, first)] + [(at, at + 1) for at in range(first, n_tp)]
+
+
 def solution(mesh):
     in_specs = (
         P(("grp", "sp", "tp"), None),

time: 197 us -> 182 us (0.924)
  waiting for transfers between devices: 126 us -> 98 us
  starting transfers between devices: 21.1 us -> 38.8 us
  local copies, waits for them, and re-layouts: 8.51 us -> 2.79 us
    ppermute x24, waiting for transfers between devices: 57.5 us -> 32.3 us  [moved(): return lax.ppermute(x, axis, [(b, a) for a, b in pairs] if back else pairs)]
    ppermute x6, starting transfers between devices: 2.51 us -> 15 us  [rotated(): return lax.ppermute(x, axis, [(i, (i + by) % size) for i in range(size)])]
    ppermute x24, starting transfers between devices: 10.6 us -> 15.8 us  [moved(): return lax.ppermute(x, axis, [(b, a) for a, b in pairs] if back else pairs)]
    unnamed x34 -> x18, local copies, waits for them, and re-layouts: 5.07 us -> 0.05 us
    pallas_call x2 -> x3, Pallas kernels: 13.1 us -> 16.8 us  [experts(): pl.pallas_call(lambda *refs: experts_body(n_src, *refs), in_specs=[IN_VME...]
    ppermute x6, waiting for transfers between devices: 58.2 us -> 55.7 us  [rotated(): return lax.ppermute(x, axis, [(i, (i + by) % size) for i in range(size)])]
    pallas_call x3, Pallas kernels: 4.49 us -> 2.4 us  [combine(): pl.pallas_call(lambda *refs: combine_body(at, *refs), in_specs=[IN_VMEM]...]
  transfers between devices with their start and end apart: 32 -> 32, of which waited for: 17 -> 12; matrix products, arithmetic and copies ran while one was open for 2% -> 1% of each run, Pallas kernels for 14% -> 16%
where the time goes in v1:
time: 182 us; the launch traced here: 180 us
  waiting for transfers between devices  98 us (54%)
  starting transfers between devices  38.8 us (21%)
  Pallas kernels  31.3 us (17%)
  other arithmetic  5.25 us (3%)
  matrix products  3.38 us (2%)
  local copies, waits for them, and re-layouts  2.79 us (2%)
    ppermute x6, waiting for transfers between devices, rotated(): return lax.ppermute(x, axis, [(i, (i + by) % size) for i in range(size)])  55.7 us
    ppermute x24, waiting for transfers between devices, moved(): return lax.ppermute(x, axis, [(b, a) for a, b in pairs] if back else pairs)  32.3 us
    pallas_call x3, Pallas kernels, experts(): pl.pallas_call(lambda *refs: experts_body(n_src, *refs), in_specs=[IN_VME...  16.8 us
    ppermute x24, starting transfers between devices, moved(): return lax.ppermute(x, axis, [(b, a) for a, b in pairs] if back else pairs)  15.8 us
    ppermute x6, starting transfers between devices, rotated(): return lax.ppermute(x, axis, [(i, (i + by) % size) for i in range(size)])  15 us
    all_to_all x1, waiting for transfers between devices, per_device(): got = lax.all_to_all(sent, 'tp', split_axis=0, concat_axis=0, tiled=True)  10 us
    pallas_call x1, Pallas kernels, load(): pl.pallas_call(load_body, in_specs=[pl.BlockSpec(memory_space=pltpu.HBM)]...  8.39 us
    all_to_all x1, starting transfers between devices, per_device(): got = lax.all_to_all(sent, 'tp', split_axis=0, concat_axis=0, tiled=True)  5.69 us
  transfers between devices with their start and end apart: 32, of which 12 were waited for; matrix products, arithmetic and copies ran while one was open for 1% of the time, Pallas kernels for 16%

profile of v1, /device:TPU:0, one launch (start us, length us, event | category | flops | bytes accessed | tf_op | source)
XLA Modules:
  0.0 180.0 jit_solution(14655708414124697465)
XLA Ops:
  0.8 2.4 %collective-permute-start = (bf16[15,256]{1,0:T(8,128)(2,1)S(1)}, bf16[15,256]{1,0:T(8,128)(2,1)S(1)}, u32[]{:S(2)}, u32[]{:S(2)}) collective-permute-start(bf16[15,256]{1,0:T(8,128)(2,1)S(1)} %slice.67), channel_id=1, source_target_pairs={{0,4},{4,8},{8,12},{1,5},{5,9},{9,13},{2,6},{6,10},{10,14},{3,7},{... | collective-permute-start | bytes 23048 | tf_op jit(solution)/shard_map/ppermute | solution.py:25
  7.2 5.7 %all-to-all-start = ((bf16[4,136,256]{2,1,0:T(8,128)(2,1)}), bf16[4,136,256]{2,1,0:T(8,128)(2,1)S(1)}, u32[]{:S(2)}, u32[]{:S(2)}) async-start(bf16[4,136,256]{2,1,0:T(8,128)(2,1)} %pad_maximum_fusion), calls=%async_computation | async-start | bytes 557056 | tf_op jit(solution)/shard_map/all_to_all | solution.py:302
  13.0 10.0 %all-to-all-done = bf16[4,136,256]{2,1,0:T(8,128)(2,1)S(1)} async-done(((bf16[4,136,256]{2,1,0:T(8,128)(2,1)}), bf16[4,136,256]{2,1,0:T(8,128)(2,1)S(1)}, u32[]{:S(2)}, u32[]{:S(2)}) %all-to-all-start) | async-done | bytes 278560 | tf_op jit(solution)/shard_map/all_to_all | solution.py:302
  24.9 3.0 %multiply_reduce_fusion = (f32[128]{0:T(128)S(1)}, f32[128,2048]{1,0:T(8,128)S(1)}) fusion(bf16[128,1024]{0,1:T(8,128)(2,1)S(1)} %bitcast.38, bf16[1024,2048]{1,0:T(8,128)(2,1)} %param.18), kind=kOutput, calls=%fused_computation.11 | convolution fusion | flops 537395072 | bytes 5505536 | tf_op jit(solution)/shard_map/dot_general | solution.py:315
  28.6 3.8 %collective-permute-start.15 = (bf16[128,2048]{1,0:T(8,128)(2,1)S(1)}, bf16[128,2048]{1,0:T(8,128)(2,1)S(1)}, u32[]{:S(2)}, u32[]{:S(2)}) collective-permute-start(bf16[128,2048]{1,0:T(8,128)(2,1)S(1)} %fusion.4.refs_1_), channel_id=1, source_target_pairs={{0,3},{1,0},{2,1},{3,2},{4,7},{5,4},{6,5},{7,6},{8,11},{9,8},{10,9... | collective-permute-start | bytes 1572872 | tf_op jit(solution)/shard_map/ppermute | solution.py:30
  34.4 10.8 %collective-permute-done.4.refs_1_ = bf16[128,2048]{1,0:T(8,128)(2,1)S(1)} collective-permute-done((bf16[128,2048]{1,0:T(8,128)(2,1)S(1)}, bf16[128,2048]{1,0:T(8,128)(2,1)S(1)}, u32[]{:S(2)}, u32[]{:S(2)}) %collective-permute-start.4) | collective-permute-done | bytes 524320 | tf_op jit(solution)/shard_map/ppermute | solution.py:30
  45.9 2.0 %collective-permute-start.6 = (bf16[72,2048]{1,0:T(8,128)(2,1)S(1)}, bf16[72,2048]{1,0:T(8,128)(2,1)S(1)}, u32[]{:S(2)}, u32[]{:S(2)}) collective-permute-start(bf16[72,2048]{1,0:T(8,128)(2,1)S(1)} %get-tuple-element.52), channel_id=1, source_target_pairs={{0,8},{4,12},{8,0},{12,4},{1,9},{5,13},{9,1},{13,5},{2,10},{6,14},... | collective-permute-start | bytes 884744 | tf_op jit(solution)/shard_map/ppermute | solution.py:76
  47.9 7.0 %collective-permute-done.15.refs_1_ = bf16[128,2048]{1,0:T(8,128)(2,1)S(1)} collective-permute-done((bf16[128,2048]{1,0:T(8,128)(2,1)S(1)}, bf16[128,2048]{1,0:T(8,128)(2,1)S(1)}, u32[]{:S(2)}, u32[]{:S(2)}) %collective-permute-start.15) | collective-permute-done | bytes 524320 | tf_op jit(solution)/shard_map/ppermute | solution.py:30
  55.5 21.0 %collective-permute-done.23.refs_1_ = bf16[128,2048]{1,0:T(8,128)(2,1)S(1)} collective-permute-done((bf16[128,2048]{1,0:T(8,128)(2,1)S(1)}, bf16[128,2048]{1,0:T(8,128)(2,1)S(1)}, u32[]{:S(2)}, u32[]{:S(2)}) %collective-permute-start.23) | collective-permute-done | bytes 524320 | tf_op jit(solution)/shard_map/ppermute | solution.py:30
  77.6 1.6 collective-permute-start.24
  79.2 8.4 %load.1 = (bf16[8,2048,256]{2,1,0:T(8,128)(2,1)S(1)}, bf16[8,2048,256]{2,1,0:T(8,128)(2,1)S(1)}, bf16[8,256,2048]{2,1,0:T(8,128)(2,1)S(1)}) custom-call(bf16[8,2048,256]{2,1,0:T(8,128)(2,1)} %refs_0_.1, bf16[8,2048,256]{2,1,0:T(8,128)(2,1)} %refs_1_.1, bf16[8,256,2048]{2,1,0:T(8,128)(2,1)} %refs_2_.1), custom_call_target="tpu_custom_call" | custom-call | tf_op jit(solution)/shard_map/load/pallas_call | solution.py:101
  87.6 5.7 %experts.3 = (bf16[72,2048]{1,0:T(8,128)(2,1)S(1)}, bf16[72,2048]{1,0:T(8,128)(2,1)S(1)}, bf16[72,2048]{1,0:T(8,128)(2,1)S(1)}, bf16[72,2048]{1,0:T(8,128)(2,1)S...) custom-call(bf16[72,2048]{1,0:T(8,128)(2,1)S(1)} %get-tuple-element., ...), custom_call_target="tpu_custom_call" | custom-call | flops 1811939328 | bytes 29884416 | tf_op jit(solution)/shard_map/experts/pallas_call | solution.py:258
  93.3 1.5 collective-permute-start.26
  95.6 5.5 %experts.4 = (bf16[72,2048]{1,0:T(8,128)(2,1)S(1)}, bf16[72,2048]{1,0:T(8,128)(2,1)S(1)}, bf16[72,2048]{1,0:T(8,128)(2,1)S(1)}, bf16[72,2048]{1,0:T(8,128)(2,1)S(1)}) custom-call(bf16[72,2048]{1,0:T(8,128)(2,1)S(1)} %get-tuple-element.65.refs_0_, bf16[72,2048]{1,0:T(8,128)(2,1)S(1)} %collective-permute-done.16.refs_1_, ...), custom_call_target="tpu_custom_call" | custom-call | flops 905969664 | bytes 27525120 | tf_op jit(solution)/shard_map/experts/pallas_call | solution.py:258
  101.1 1.4 collective-permute-start.13
  103.2 1.4 collective-permute-start.20
  104.7 5.5 %experts.5 = (bf16[72,2048]{1,0:T(8,128)(2,1)S(1)}, bf16[72,2048]{1,0:T(8,128)(2,1)S(1)}, bf16[72,2048]{1,0:T(8,128)(2,1)S(1)}, bf16[72,2048]{1,0:T(8,128)(2,1)S(1)}) custom-call(bf16[72,2048]{1,0:T(8,128)(2,1)S(1)} %get-tuple-element.73.refs_0_, bf16[72,2048]{1,0:T(8,128)(2,1)S(1)} %collective-permute-done.24.refs_1_, ...), custom_call_target="tpu_custom_call" | custom-call | flops 905969664 | bytes 27525120 | tf_op jit(solution)/shard_map/experts/pallas_call | solution.py:258
  110.2 1.2 collective-permute-start.21
  111.4 3.9 %collective-permute-done.13.refs_5_ = bf16[72,2048]{1,0:T(8,128)(2,1)S(1)} collective-permute-done((bf16[72,2048]{1,0:T(8,128)(2,1)S(1)}, bf16[72,2048]{1,0:T(8,128)(2,1)S(1)}, u32[]{:S(2)}, u32[]{:S(2)}) %collective-permute-start.13) | collective-permute-done | bytes 294944 | tf_op jit(solution)/shard_map/ppermute | solution.py:76
  115.3 2.0 %collective-permute-start.28 = (bf16[72,2048]{1,0:T(8,128)(2,1)S(1)}, bf16[72,2048]{1,0:T(8,128)(2,1)S(1)}, u32[]{:S(2)}, u32[]{:S(2)}) collective-permute-start(bf16[72,2048]{1,0:T(8,128)(2,1)S(1)} %get-tuple-element.79), channel_id=1, source_target_pairs={{8,0},{12,4},{0,8},{4,12},{9,1},{13,5},{1,9},{5,13},{10,2},{14,6},... | collective-permute-start | bytes 884744 | tf_op jit(solution)/shard_map/ppermute | solution.py:76
  117.3 1.1 collective-permute-start.29
  118.4 5.1 %collective-permute-done.20.refs_4_ = bf16[72,2048]{1,0:T(8,128)(2,1)S(1)} collective-permute-done((bf16[72,2048]{1,0:T(8,128)(2,1)S(1)}, bf16[72,2048]{1,0:T(8,128)(2,1)S(1)}, u32[]{:S(2)}, u32[]{:S(2)}) %collective-permute-start.20) | collective-permute-done | bytes 294944 | tf_op jit(solution)/shard_map/ppermute | solution.py:76
  124.4 3.5 %collective-permute-done.21.refs_5_ = bf16[72,2048]{1,0:T(8,128)(2,1)S(1)} collective-permute-done((bf16[72,2048]{1,0:T(8,128)(2,1)S(1)}, bf16[72,2048]{1,0:T(8,128)(2,1)S(1)}, u32[]{:S(2)}, u32[]{:S(2)}) %collective-permute-start.21) | collective-permute-done | bytes 294944 | tf_op jit(solution)/shard_map/ppermute | solution.py:76
  127.9 1.8 collective-permute-start.14
  130.6 3.5 %collective-permute-start.22 = (bf16[128,2048]{1,0:T(8,128)(2,1)S(1)}, bf16[128,2048]{1,0:T(8,128)(2,1)S(1)}, u32[]{:S(2)}, u32[]{:S(2)}) collective-permute-start(bf16[128,2048]{1,0:T(8,128)(2,1)S(1)} %combine.4), channel_id=1, source_target_pairs={{0,1},{1,2},{2,3},{3,0},{4,5},{5,6},{6,7},{7,4},{8,9},{9,10},{10,1... | collective-permute-start | bytes 1572872 | tf_op jit(solution)/shard_map/ppermute | solution.py:30
  134.1 2.2 %collective-permute-done.28.refs_4_ = bf16[72,2048]{1,0:T(8,128)(2,1)S(1)} collective-permute-done((bf16[72,2048]{1,0:T(8,128)(2,1)S(1)}, bf16[72,2048]{1,0:T(8,128)(2,1)S(1)}, u32[]{:S(2)}, u32[]{:S(2)}) %collective-permute-start.28) | collective-permute-done | bytes 294944 | tf_op jit(solution)/shard_map/ppermute | solution.py:76
  136.2 4.4 %collective-permute-done.29.refs_5_ = bf16[72,2048]{1,0:T(8,128)(2,1)S(1)} collective-permute-done((bf16[72,2048]{1,0:T(8,128)(2,1)S(1)}, bf16[72,2048]{1,0:T(8,128)(2,1)S(1)}, u32[]{:S(2)}, u32[]{:S(2)}) %collective-permute-start.29) | collective-permute-done | bytes 294944 | tf_op jit(solution)/shard_map/ppermute | solution.py:76
  141.4 5.8 %collective-permute-start.30 = (bf16[128,2048]{1,0:T(8,128)(2,1)S(1)}, bf16[128,2048]{1,0:T(8,128)(2,1)S(1)}, u32[]{:S(2)}, u32[]{:S(2)}) collective-permute-start(bf16[128,2048]{1,0:T(8,128)(2,1)S(1)} %combine.5), channel_id=1, source_target_pairs={{0,2},{1,3},{2,0},{3,1},{4,6},{5,7},{6,4},{7,5},{8,10},{9,11},{10,... | collective-permute-start | bytes 1572872 | tf_op jit(solution)/shard_map/ppermute | solution.py:30
  148.1 9.0 %collective-permute-done.9.refs_6_ = bf16[72,2048]{1,0:T(8,128)(2,1)S(1)} collective-permute-done((bf16[72,2048]{1,0:T(8,128)(2,1)S(1)}, bf16[72,2048]{1,0:T(8,128)(2,1)S(1)}, u32[]{:S(2)}, u32[]{:S(2)}) %collective-permute-start.9) | collective-permute-done | bytes 294944 | tf_op jit(solution)/shard_map/ppermute | solution.py:76
  157.1 4.1 %collective-permute-done.10.refs_7_ = bf16[72,2048]{1,0:T(8,128)(2,1)S(1)} collective-permute-done((bf16[72,2048]{1,0:T(8,128)(2,1)S(1)}, bf16[72,2048]{1,0:T(8,128)(2,1)S(1)}, u32[]{:S(2)}, u32[]{:S(2)}) %collective-permute-start.10) | collective-permute-done | bytes 294944 | tf_op jit(solution)/shard_map/ppermute | solution.py:76
  161.2 16.9 %collective-permute-done.30.refs_10_ = bf16[128,2048]{1,0:T(8,128)(2,1)S(1)} collective-permute-done((bf16[128,2048]{1,0:T(8,128)(2,1)S(1)}, bf16[128,2048]{1,0:T(8,128)(2,1)S(1)}, u32[]{:S(2)}, u32[]{:S(2)}) %collective-permute-start.30) | collective-permute-done | bytes 524320 | tf_op jit(solution)/shard_map/ppermute | solution.py:30
  178.1 1.8 %finish.1 = bf16[128,2048]{1,0:T(8,128)(2,1)} custom-call(s32[4,128,2]{2,1,0:T(8,128)S(1)} %bitcast.31, f32[4,128,2]{2,1,0:T(8,128)S(1)} %bitcast.35, bf16[128,2048]{1,0:T(8,128)(2,1)S(1)} %get-tuple-element.82.refs_2_, f32[1,2048]{1,0:T(1,128)S(1)} %bitcast.36, bf16[72,2048]{1,0:T(8,128)(2,1)S(1)} %get-tuple-element.57.refs_4_, ...), custom_call_target="tpu_custom_call" | custom-call | tf_op jit(solution)/shard_map/finish/pallas_call | solution.py:196
  (108 shorter events, 16.4 us)
Async XLA Ops:
  0.8 3.9 %collective-permute-start = (bf16[15,256]{1,0:T(8,128)(2,1)S(1)}, bf16[15,256]{1,0:T(8,128)(2,1)S(1)}, u32[]{:S(2)}, u32[]{:S(2)}) collective-permute-start(bf16[15,256]{1,0:T(8,128)(2,1)S(1)} %slice.67), channel_id=1, source_target_pairs={{0,4},{4,8},{8,12},{1,5},{5,9},{9,13},{2,6},{6,10},{10,14},{3,7},{... | collective-permute-start | bytes 23048 | tf_op jit(solution)/shard_map/ppermute | solution.py:25
  7.2 15.8 %all-to-all-start = ((bf16[4,136,256]{2,1,0:T(8,128)(2,1)}), bf16[4,136,256]{2,1,0:T(8,128)(2,1)S(1)}, u32[]{:S(2)}, u32[]{:S(2)}) async-start(bf16[4,136,256]{2,1,0:T(8,128)(2,1)} %pad_maximum_fusion), calls=%async_computation | async-start | bytes 557056 | tf_op jit(solution)/shard_map/all_to_all | solution.py:302
  28.5 16.7 %collective-permute-start.4 = (bf16[128,2048]{1,0:T(8,128)(2,1)S(1)}, bf16[128,2048]{1,0:T(8,128)(2,1)S(1)}, u32[]{:S(2)}, u32[]{:S(2)}) collective-permute-start(bf16[128,2048]{1,0:T(8,128)(2,1)S(1)} %fusion.4.refs_1_), channel_id=1, source_target_pairs={{0,1},{1,2},{2,3},{3,0},{4,5},{5,6},{6,7},{7,4},{8,9},{9,10},{10,1... | collective-permute-start | bytes 1572872 | tf_op jit(solution)/shard_map/ppermute | solution.py:30
  28.6 26.3 %collective-permute-start.15 = (bf16[128,2048]{1,0:T(8,128)(2,1)S(1)}, bf16[128,2048]{1,0:T(8,128)(2,1)S(1)}, u32[]{:S(2)}, u32[]{:S(2)}) collective-permute-start(bf16[128,2048]{1,0:T(8,128)(2,1)S(1)} %fusion.4.refs_1_), channel_id=1, source_target_pairs={{0,3},{1,0},{2,1},{3,2},{4,7},{5,4},{6,5},{7,6},{8,11},{9,8},{10,9... | collective-permute-start | bytes 1572872 | tf_op jit(solution)/shard_map/ppermute | solution.py:30
  34.1 11.6 %collective-permute-start.1 = (bf16[72,2048]{1,0:T(8,128)(2,1)S(1)}, bf16[72,2048]{1,0:T(8,128)(2,1)S(1)}, u32[]{:S(2)}, u32[]{:S(2)}) collective-permute-start(bf16[72,2048]{1,0:T(8,128)(2,1)S(1)} %get-tuple-element.47), channel_id=1, source_target_pairs={{0,4},{4,0},{8,12},{12,8},{1,5},{5,1},{9,13},{13,9},{2,6},{6,2},{1... | collective-permute-start | bytes 884744 | tf_op jit(solution)/shard_map/ppermute | solution.py:76
  34.2 42.3 %collective-permute-start.23 = (bf16[128,2048]{1,0:T(8,128)(2,1)S(1)}, bf16[128,2048]{1,0:T(8,128)(2,1)S(1)}, u32[]{:S(2)}, u32[]{:S(2)}) collective-permute-start(bf16[128,2048]{1,0:T(8,128)(2,1)S(1)} %fusion.4.refs_1_), channel_id=1, source_target_pairs={{0,2},{1,3},{2,0},{3,1},{4,6},{5,7},{6,4},{7,5},{8,10},{9,11},{10,... | collective-permute-start | bytes 1572872 | tf_op jit(solution)/shard_map/ppermute | solution.py:30
  34.3 11.6 %collective-permute-start.2 = (bf16[72,2048]{1,0:T(8,128)(2,1)S(1)}, bf16[72,2048]{1,0:T(8,128)(2,1)S(1)}, u32[]{:S(2)}, u32[]{:S(2)}) collective-permute-start(bf16[72,2048]{1,0:T(8,128)(2,1)S(1)} %get-tuple-element.48), channel_id=1, source_target_pairs={{0,8},{4,12},{8,0},{12,4},{1,9},{5,13},{9,1},{13,5},{2,10},{6,14},... | collective-permute-start | bytes 884744 | tf_op jit(solution)/shard_map/ppermute | solution.py:76
  45.2 10.2 %collective-permute-start.3 = (bf16[72,2048]{1,0:T(8,128)(2,1)S(1)}, bf16[72,2048]{1,0:T(8,128)(2,1)S(1)}, u32[]{:S(2)}, u32[]{:S(2)}) collective-permute-start(bf16[72,2048]{1,0:T(8,128)(2,1)S(1)} %get-tuple-element.49), channel_id=1, source_target_pairs={{0,12},{4,8},{8,4},{12,0},{1,13},{5,9},{9,5},{13,1},{2,14},{6,10},... | collective-permute-start | bytes 884744 | tf_op jit(solution)/shard_map/ppermute | solution.py:76
  45.7 30.8 %collective-permute-start.5 = (bf16[72,2048]{1,0:T(8,128)(2,1)S(1)}, bf16[72,2048]{1,0:T(8,128)(2,1)S(1)}, u32[]{:S(2)}, u32[]{:S(2)}) collective-permute-start(bf16[72,2048]{1,0:T(8,128)(2,1)S(1)} %get-tuple-element.51), channel_id=1, source_target_pairs={{0,4},{4,0},{8,12},{12,8},{1,5},{5,1},{9,13},{13,9},{2,6},{6,2},{1... | collective-permute-start | bytes 884744 | tf_op jit(solution)/shard_map/ppermute | solution.py:76
  45.9 31.7 %collective-permute-start.6 = (bf16[72,2048]{1,0:T(8,128)(2,1)S(1)}, bf16[72,2048]{1,0:T(8,128)(2,1)S(1)}, u32[]{:S(2)}, u32[]{:S(2)}) collective-permute-start(bf16[72,2048]{1,0:T(8,128)(2,1)S(1)} %get-tuple-element.52), channel_id=1, source_target_pairs={{0,8},{4,12},{8,0},{12,4},{1,9},{5,13},{9,1},{13,5},{2,10},{6,14},... | collective-permute-start | bytes 884744 | tf_op jit(solution)/shard_map/ppermute | solution.py:76
  54.9 24.3 %collective-permute-start.7 = (bf16[72,2048]{1,0:T(8,128)(2,1)S(1)}, bf16[72,2048]{1,0:T(8,128)(2,1)S(1)}, u32[]{:S(2)}, u32[]{:S(2)}) collective-permute-start(bf16[72,2048]{1,0:T(8,128)(2,1)S(1)} %get-tuple-element.53), channel_id=1, source_target_pairs={{0,12},{4,8},{8,4},{12,0},{1,13},{5,9},{9,5},{13,1},{2,14},{6,10},... | collective-permute-start | bytes 884744 | tf_op jit(solution)/shard_map/ppermute | solution.py:76
  55.4 37.9 %collective-permute-start.16 = (bf16[72,2048]{1,0:T(8,128)(2,1)S(1)}, bf16[72,2048]{1,0:T(8,128)(2,1)S(1)}, u32[]{:S(2)}, u32[]{:S(2)}) collective-permute-start(bf16[72,2048]{1,0:T(8,128)(2,1)S(1)} %get-tuple-element.66), channel_id=1, source_target_pairs={{0,4},{4,0},{8,12},{12,8},{1,5},{5,1},{9,13},{13,9},{2,6},{6,2},{1... | collective-permute-start | bytes 884744 | tf_op jit(solution)/shard_map/ppermute | solution.py:76
  76.5 18.3 %collective-permute-start.17 = (bf16[72,2048]{1,0:T(8,128)(2,1)S(1)}, bf16[72,2048]{1,0:T(8,128)(2,1)S(1)}, u32[]{:S(2)}, u32[]{:S(2)}) collective-permute-start(bf16[72,2048]{1,0:T(8,128)(2,1)S(1)} %get-tuple-element.67), channel_id=1, source_target_pairs={{0,8},{4,12},{8,0},{12,4},{1,9},{5,13},{9,1},{13,5},{2,10},{6,14},... | collective-permute-start | bytes 884744 | tf_op jit(solution)/shard_map/ppermute | solution.py:76
  76.5 19.0 %collective-permute-start.18 = (bf16[72,2048]{1,0:T(8,128)(2,1)S(1)}, bf16[72,2048]{1,0:T(8,128)(2,1)S(1)}, u32[]{:S(2)}, u32[]{:S(2)}) collective-permute-start(bf16[72,2048]{1,0:T(8,128)(2,1)S(1)} %get-tuple-element.68), channel_id=1, source_target_pairs={{0,12},{4,8},{8,4},{12,0},{1,13},{5,9},{9,5},{13,1},{2,14},{6,10},... | collective-permute-start | bytes 884744 | tf_op jit(solution)/shard_map/ppermute | solution.py:76
  77.6 23.5 %collective-permute-start.24 = (bf16[72,2048]{1,0:T(8,128)(2,1)S(1)}, bf16[72,2048]{1,0:T(8,128)(2,1)S(1)}, u32[]{:S(2)}, u32[]{:S(2)}) collective-permute-start(bf16[72,2048]{1,0:T(8,128)(2,1)S(1)} %get-tuple-element.74), channel_id=1, source_target_pairs={{0,4},{4,0},{8,12},{12,8},{1,5},{5,1},{9,13},{13,9},{2,6},{6,2},{1... | collective-permute-start | bytes 884744 | tf_op jit(solution)/shard_map/ppermute | solution.py:76
  79.2 23.3 %collective-permute-start.25 = (bf16[72,2048]{1,0:T(8,128)(2,1)S(1)}, bf16[72,2048]{1,0:T(8,128)(2,1)S(1)}, u32[]{:S(2)}, u32[]{:S(2)}) collective-permute-start(bf16[72,2048]{1,0:T(8,128)(2,1)S(1)} %get-tuple-element.75), channel_id=1, source_target_pairs={{0,8},{4,12},{8,0},{12,4},{1,9},{5,13},{9,1},{13,5},{2,10},{6,14},... | collective-permute-start | bytes 884744 | tf_op jit(solution)/shard_map/ppermute | solution.py:76
  93.3 9.9 %collective-permute-start.26 = (bf16[72,2048]{1,0:T(8,128)(2,1)S(1)}, bf16[72,2048]{1,0:T(8,128)(2,1)S(1)}, u32[]{:S(2)}, u32[]{:S(2)}) collective-permute-start(bf16[72,2048]{1,0:T(8,128)(2,1)S(1)} %get-tuple-element.76), channel_id=1, source_target_pairs={{0,12},{4,8},{8,4},{12,0},{1,13},{5,9},{9,5},{13,1},{2,14},{6,10},... | collective-permute-start | bytes 884744 | tf_op jit(solution)/shard_map/ppermute | solution.py:76
  94.8 15.4 %collective-permute-start.11 = (bf16[72,2048]{1,0:T(8,128)(2,1)S(1)}, bf16[72,2048]{1,0:T(8,128)(2,1)S(1)}, u32[]{:S(2)}, u32[]{:S(2)}) collective-permute-start(bf16[72,2048]{1,0:T(8,128)(2,1)S(1)} %get-tuple-element.62), channel_id=1, source_target_pairs={{4,0},{0,4},{12,8},{8,12},{5,1},{1,5},{13,9},{9,13},{6,2},{2,6},{1... | collective-permute-start | bytes 884744 | tf_op jit(solution)/shard_map/ppermute | solution.py:76
  95.5 15.9 %collective-permute-start.12 = (bf16[72,2048]{1,0:T(8,128)(2,1)S(1)}, bf16[72,2048]{1,0:T(8,128)(2,1)S(1)}, u32[]{:S(2)}, u32[]{:S(2)}) collective-permute-start(bf16[72,2048]{1,0:T(8,128)(2,1)S(1)} %get-tuple-element.63), channel_id=1, source_target_pairs={{8,0},{12,4},{0,8},{4,12},{9,1},{13,5},{1,9},{5,13},{10,2},{14,6},... | collective-permute-start | bytes 884744 | tf_op jit(solution)/shard_map/ppermute | solution.py:76
  101.1 14.2 %collective-permute-start.13 = (bf16[72,2048]{1,0:T(8,128)(2,1)S(1)}, bf16[72,2048]{1,0:T(8,128)(2,1)S(1)}, u32[]{:S(2)}, u32[]{:S(2)}) collective-permute-start(bf16[72,2048]{1,0:T(8,128)(2,1)S(1)} %get-tuple-element.64), channel_id=1, source_target_pairs={{12,0},{8,4},{4,8},{0,12},{13,1},{9,5},{5,9},{1,13},{14,2},{10,6},... | collective-permute-start | bytes 884744 | tf_op jit(solution)/shard_map/ppermute | solution.py:76
  102.5 14.8 %collective-permute-start.19 = (bf16[72,2048]{1,0:T(8,128)(2,1)S(1)}, bf16[72,2048]{1,0:T(8,128)(2,1)S(1)}, u32[]{:S(2)}, u32[]{:S(2)}) collective-permute-start(bf16[72,2048]{1,0:T(8,128)(2,1)S(1)} %get-tuple-element.70), channel_id=1, source_target_pairs={{4,0},{0,4},{12,8},{8,12},{5,1},{1,5},{13,9},{9,13},{6,2},{2,6},{1... | collective-permute-start | bytes 884744 | tf_op jit(solution)/shard_map/ppermute | solution.py:76
  103.2 20.3 %collective-permute-start.20 = (bf16[72,2048]{1,0:T(8,128)(2,1)S(1)}, bf16[72,2048]{1,0:T(8,128)(2,1)S(1)}, u32[]{:S(2)}, u32[]{:S(2)}) collective-permute-start(bf16[72,2048]{1,0:T(8,128)(2,1)S(1)} %get-tuple-element.71), channel_id=1, source_target_pairs={{8,0},{12,4},{0,8},{4,12},{9,1},{13,5},{1,9},{5,13},{10,2},{14,6},... | collective-permute-start | bytes 884744 | tf_op jit(solution)/shard_map/ppermute | solution.py:76
  110.2 17.7 %collective-permute-start.21 = (bf16[72,2048]{1,0:T(8,128)(2,1)S(1)}, bf16[72,2048]{1,0:T(8,128)(2,1)S(1)}, u32[]{:S(2)}, u32[]{:S(2)}) collective-permute-start(bf16[72,2048]{1,0:T(8,128)(2,1)S(1)} %get-tuple-element.72), channel_id=1, source_target_pairs={{12,0},{8,4},{4,8},{0,12},{13,1},{9,5},{5,9},{1,13},{14,2},{10,6},... | collective-permute-start | bytes 884744 | tf_op jit(solution)/shard_map/ppermute | solution.py:76
  111.4 19.1 %collective-permute-start.27 = (bf16[72,2048]{1,0:T(8,128)(2,1)S(1)}, bf16[72,2048]{1,0:T(8,128)(2,1)S(1)}, u32[]{:S(2)}, u32[]{:S(2)}) collective-permute-start(bf16[72,2048]{1,0:T(8,128)(2,1)S(1)} %get-tuple-element.78), channel_id=1, source_target_pairs={{4,0},{0,4},{12,8},{8,12},{5,1},{1,5},{13,9},{9,13},{6,2},{2,6},{1... | collective-permute-start | bytes 884744 | tf_op jit(solution)/shard_map/ppermute | solution.py:76
  115.3 20.9 %collective-permute-start.28 = (bf16[72,2048]{1,0:T(8,128)(2,1)S(1)}, bf16[72,2048]{1,0:T(8,128)(2,1)S(1)}, u32[]{:S(2)}, u32[]{:S(2)}) collective-permute-start(bf16[72,2048]{1,0:T(8,128)(2,1)S(1)} %get-tuple-element.79), channel_id=1, source_target_pairs={{8,0},{12,4},{0,8},{4,12},{9,1},{13,5},{1,9},{5,13},{10,2},{14,6},... | collective-permute-start | bytes 884744 | tf_op jit(solution)/shard_map/ppermute | solution.py:76
  117.3 23.3 %collective-permute-start.29 = (bf16[72,2048]{1,0:T(8,128)(2,1)S(1)}, bf16[72,2048]{1,0:T(8,128)(2,1)S(1)}, u32[]{:S(2)}, u32[]{:S(2)}) collective-permute-start(bf16[72,2048]{1,0:T(8,128)(2,1)S(1)} %get-tuple-element.80), channel_id=1, source_target_pairs={{12,0},{8,4},{4,8},{0,12},{13,1},{9,5},{5,9},{1,13},{14,2},{10,6},... | collective-permute-start | bytes 884744 | tf_op jit(solution)/shard_map/ppermute | solution.py:76
  123.6 24.5 %collective-permute-start.8 = (bf16[72,2048]{1,0:T(8,128)(2,1)S(1)}, bf16[72,2048]{1,0:T(8,128)(2,1)S(1)}, u32[]{:S(2)}, u32[]{:S(2)}) collective-permute-start(bf16[72,2048]{1,0:T(8,128)(2,1)S(1)} %get-tuple-element.58), channel_id=1, source_target_pairs={{4,0},{0,4},{12,8},{8,12},{5,1},{1,5},{13,9},{9,13},{6,2},{2,6},{1... | collective-permute-start | bytes 884744 | tf_op jit(solution)/shard_map/ppermute | solution.py:76
  127.9 33.3 %collective-permute-start.14 = (bf16[128,2048]{1,0:T(8,128)(2,1)S(1)}, bf16[128,2048]{1,0:T(8,128)(2,1)S(1)}, u32[]{:S(2)}, u32[]{:S(2)}) collective-permute-start(bf16[128,2048]{1,0:T(8,128)(2,1)S(1)} %combine.3), channel_id=1, source_target_pairs={{0,3},{1,0},{2,1},{3,2},{4,7},{5,4},{6,5},{7,6},{8,11},{9,8},{10,9... | collective-permute-start | bytes 1572872 | tf_op jit(solution)/shard_map/ppermute | solution.py:30
  130.6 30.7 %collective-permute-start.22 = (bf16[128,2048]{1,0:T(8,128)(2,1)S(1)}, bf16[128,2048]{1,0:T(8,128)(2,1)S(1)}, u32[]{:S(2)}, u32[]{:S(2)}) collective-permute-start(bf16[128,2048]{1,0:T(8,128)(2,1)S(1)} %combine.4), channel_id=1, source_target_pairs={{0,1},{1,2},{2,3},{3,0},{4,5},{5,6},{6,7},{7,4},{8,9},{9,10},{10,1... | collective-permute-start | bytes 1572872 | tf_op jit(solution)/shard_map/ppermute | solution.py:30
  141.4 36.7 %collective-permute-start.30 = (bf16[128,2048]{1,0:T(8,128)(2,1)S(1)}, bf16[128,2048]{1,0:T(8,128)(2,1)S(1)}, u32[]{:S(2)}, u32[]{:S(2)}) collective-permute-start(bf16[128,2048]{1,0:T(8,128)(2,1)S(1)} %combine.5), channel_id=1, source_target_pairs={{0,2},{1,3},{2,0},{3,1},{4,6},{5,7},{6,4},{7,5},{8,10},{9,11},{10,... | collective-permute-start | bytes 1572872 | tf_op jit(solution)/shard_map/ppermute | solution.py:30
  147.2 9.9 %collective-permute-start.9 = (bf16[72,2048]{1,0:T(8,128)(2,1)S(1)}, bf16[72,2048]{1,0:T(8,128)(2,1)S(1)}, u32[]{:S(2)}, u32[]{:S(2)}) collective-permute-start(bf16[72,2048]{1,0:T(8,128)(2,1)S(1)} %get-tuple-element.59), channel_id=1, source_target_pairs={{8,0},{12,4},{0,8},{4,12},{9,1},{13,5},{1,9},{5,13},{10,2},{14,6},... | collective-permute-start | bytes 884744 | tf_op jit(solution)/shard_map/ppermute | solution.py:76
  148.1 13.2 %collective-permute-start.10 = (bf16[72,2048]{1,0:T(8,128)(2,1)S(1)}, bf16[72,2048]{1,0:T(8,128)(2,1)S(1)}, u32[]{:S(2)}, u32[]{:S(2)}) collective-permute-start(bf16[72,2048]{1,0:T(8,128)(2,1)S(1)} %get-tuple-element.60), channel_id=1, source_target_pairs={{12,0},{8,4},{4,8},{0,12},{13,1},{9,5},{5,9},{1,13},{14,2},{10,6},... | collective-permute-start | bytes 884744 | tf_op jit(solution)/shard_map/ppermute | solution.py:76
  (8 other events, 266.1 us)

commit v2 on v1

--- a/solution.py
+++ b/solution.py
@@ -144,8 +144,8 @@
     return share.astype(jnp.bfloat16)
 
 
-def combine_body(at, slot, weight, *refs):
-    backs, out = refs[:-1], refs[-1]
+def combine_body(at, n_back, slot, weight, *refs):
+    backs, joined, out = refs[:n_back], refs[n_back:-1], refs[-1]
     rows = backs[0].shape[0]
     share = [shares_of(at, slot, weight, d, rows) for d in range(len(backs))]
     for j in range(0, out.shape[1], 2 * LANES):
@@ -154,19 +154,21 @@
         for d, back in enumerate(backs):
             term = jnp.dot(share[d], back[:, cols], preferred_element_type=jnp.float32)
             total = term if total is None else total + term
+        for other in joined:
+            total = total + other[:, cols].astype(jnp.float32)
         out[:, cols] = total.astype(out.dtype)
 
 
-def combine(at, slot, weight, backs):
+def combine(at, slot, weight, backs, joined):
     shape = jax.ShapeDtypeStruct((slot.shape[1], backs[0].shape[1]), jnp.bfloat16)
     return pl.pallas_call(
-        lambda *refs: combine_body(at, *refs),
-        in_specs=[IN_VMEM] * (2 + len(backs)),
+        lambda *refs: combine_body(at, len(backs), *refs),
+        in_specs=[IN_VMEM] * (2 + len(backs) + len(joined)),
         out_specs=IN_VMEM,
         out_shape=shape,
         compiler_params=pltpu.CompilerParams(vmem_limit_bytes=6 << 20),
         name="combine",
-    )(slot, weight, *backs)
+    )(slot, weight, *backs, *joined)
 
 
 def finish_body(at, n_back, slot, weight, resid, gain, *refs):
@@ -316,11 +318,13 @@
     residual = (resid_in.astype(jnp.float32) + rms_scale(mix_out, mix_gain)).astype(jnp.bfloat16)
     normed = rms_scale(residual.astype(jnp.float32), ffn_gain).astype(jnp.bfloat16)
 
-    order = [0] + [k for pair in zip(range(1, n_tp), range(n_tp - 1, 0, -1)) for k in pair]
-    order = list(dict.fromkeys(order))
-    blocks = {}
+    far = n_tp // 2
+    order = list(range(far + 1)) + list(range(n_tp - 1, far, -1))
+    blocks = {0: normed, n_tp: normed}
     for k in order:
-        blocks[k] = rotated(normed, "tp", k) if k else normed
+        if k:
+            by = 1 if k <= far else -1
+            blocks[k] = rotated(blocks[k - by], "tp", by)
 
     here = lax.axis_index("tp")
     sp_here = lax.axis_index("sp")
@@ -349,7 +353,7 @@
         weight = weight.transpose(0, 2, 1)
         slot, by_row, weight = lax.optimization_barrier((slot, by_row, weight))
         weights = load(w_gate, w_up, w_down)
-        arrived, backs, parts = [], {}, []
+        arrived, backs, parts = [], {}, {}
         for at, k in enumerate(order):
             rows = pick(at, slot, blocks[k], n_sp, slot_rows)
             arrived.append([moved(x, "sp", d) if d else x for d, x in enumerate(rows)])
@@ -359,11 +363,14 @@
             for at in range(first, stop):
                 back = terms[(at - first) * n_sp : (at - first + 1) * n_sp]
                 backs[at] = [moved(x, "sp", d, True) if d else x for d, x in enumerate(back)]
-        for at, k in enumerate(order):
-            if k:
-                part = combine(at, by_row, weight, backs[at])
-                parts.append(rotated(part, "tp", -k))
-        return finish(0, by_row, weight, residual, post_gain, backs[0], parts)
+        for at in return_order(n_tp)[:-1]:
+            k = order[at]
+            by = -1 if k <= far else 1
+            inner = k < far or k > far + 1
+            joined = [parts.pop(k - by)] if inner else []
+            part = combine(at, by_row, weight, backs[at], joined)
+            parts[k] = rotated(part, "tp", by)
+        return finish(0, by_row, weight, residual, post_gain, backs[0], list(parts.values()))
     else:
         slot_index = route * CAP + slot_rank
         picker = slot_index[..., None] == lax.iota(jnp.int32, slot_total)
@@ -402,6 +409,11 @@
     return [(0, first)] + [(at, at + 1) for at in range(first, n_tp)]
 
 
+def return_order(n_tp):
+    far = n_tp // 2
+    return list(range(far, 1, -1)) + list(range(n_tp - 1, far, -1)) + list(range(min(2, n_tp)))[::-1]
+
+
 def solution(mesh):
     in_specs = (
         P(("grp", "sp", "tp"), None),

time: 182 us -> 181 us (level)
  starting transfers between devices: 38.8 us -> 29.2 us
  waiting for transfers between devices: 98 us -> 106 us
    ppermute x24, waiting for transfers between devices: 32.3 us -> 64.9 us  [moved(): return lax.ppermute(x, axis, [(b, a) for a, b in pairs] if back else pairs)]
    ppermute x6, waiting for transfers between devices: 55.7 us -> 30.8 us  [rotated(): return lax.ppermute(x, axis, [(i, (i + by) % size) for i in range(size)])]
    ppermute x6, starting transfers between devices: 15 us -> 4.52 us  [rotated(): return lax.ppermute(x, axis, [(i, (i + by) % size) for i in range(size)])]
  transfers between devices with their start and end apart: 32 -> 32, of which waited for: 12 -> 15; matrix products, arithmetic and copies ran while one was open for 1% -> 3% of each run, Pallas kernels for 16% -> 16%
where the time goes in v2:
time: 181 us; the launch traced here: 180 us
  waiting for transfers between devices  106 us (59%)
  Pallas kernels  31.2 us (17%)
  starting transfers between devices  29.2 us (16%)
  other arithmetic  6.25 us (3%)
  local copies, waits for them, and re-layouts  4.07 us (2%)
  matrix products  3.39 us (2%)
    ppermute x24, waiting for transfers between devices, moved(): return lax.ppermute(x, axis, [(b, a) for a, b in pairs] if back else pairs)  64.9 us
    ppermute x6, waiting for transfers between devices, rotated(): return lax.ppermute(x, axis, [(i, (i + by) % size) for i in range(size)])  30.8 us
    pallas_call x3, Pallas kernels, experts(): pl.pallas_call(lambda *refs: experts_body(n_src, *refs), in_specs=[IN_VME...  16.7 us
    ppermute x24, starting transfers between devices, moved(): return lax.ppermute(x, axis, [(b, a) for a, b in pairs] if back else pairs)  16.6 us
    all_to_all x1, waiting for transfers between devices, per_device(): got = lax.all_to_all(sent, 'tp', split_axis=0, concat_axis=0, tiled=True)  10 us
    pallas_call x1, Pallas kernels, load(): pl.pallas_call(load_body, in_specs=[pl.BlockSpec(memory_space=pltpu.HBM)]...  8.39 us
    all_to_all x1, starting transfers between devices, per_device(): got = lax.all_to_all(sent, 'tp', split_axis=0, concat_axis=0, tiled=True)  5.69 us
    ppermute x6, starting transfers between devices, rotated(): return lax.ppermute(x, axis, [(i, (i + by) % size) for i in range(size)])  4.52 us
  transfers between devices with their start and end apart: 32, of which 15 were waited for; matrix products, arithmetic and copies ran while one was open for 3% of the time, Pallas kernels for 16%

profile of v2, /device:TPU:0, one launch (start us, length us, event | category | flops | bytes accessed | tf_op | source)
XLA Modules:
  0.0 180.3 jit_solution(12200680450715543546)
XLA Ops:
  0.8 2.4 %collective-permute-start = (bf16[15,256]{1,0:T(8,128)(2,1)S(1)}, bf16[15,256]{1,0:T(8,128)(2,1)S(1)}, u32[]{:S(2)}, u32[]{:S(2)}) collective-permute-start(bf16[15,256]{1,0:T(8,128)(2,1)S(1)} %slice.67), channel_id=1, source_target_pairs={{0,4},{4,8},{8,12},{1,5},{5,9},{9,13},{2,6},{6,10},{10,14},{3,7},{... | collective-permute-start | bytes 23048 | tf_op jit(solution)/shard_map/ppermute | solution.py:25
  7.2 5.7 %all-to-all-start = ((bf16[4,136,256]{2,1,0:T(8,128)(2,1)}), bf16[4,136,256]{2,1,0:T(8,128)(2,1)S(1)}, u32[]{:S(2)}, u32[]{:S(2)}) async-start(bf16[4,136,256]{2,1,0:T(8,128)(2,1)} %pad_maximum_fusion), calls=%async_computation | async-start | bytes 557056 | tf_op jit(solution)/shard_map/all_to_all | solution.py:304
  13.0 10.0 %all-to-all-done = bf16[4,136,256]{2,1,0:T(8,128)(2,1)S(1)} async-done(((bf16[4,136,256]{2,1,0:T(8,128)(2,1)}), bf16[4,136,256]{2,1,0:T(8,128)(2,1)S(1)}, u32[]{:S(2)}, u32[]{:S(2)}) %all-to-all-start) | async-done | bytes 278560 | tf_op jit(solution)/shard_map/all_to_all | solution.py:304
  24.5 3.0 %multiply_reduce_fusion = (f32[128]{0:T(128)S(1)}, f32[128,2048]{1,0:T(8,128)S(1)}) fusion(bf16[128,1024]{0,1:T(8,128)(2,1)S(1)} %bitcast.38, bf16[1024,2048]{1,0:T(8,128)(2,1)} %param.18), kind=kOutput, calls=%fused_computation.11 | convolution fusion | flops 537395072 | bytes 5505536 | tf_op jit(solution)/shard_map/dot_general | solution.py:317
  28.2 3.8 %collective-permute-start.11 = (bf16[128,2048]{1,0:T(8,128)(2,1)S(1)}, bf16[128,2048]{1,0:T(8,128)(2,1)S(1)}, u32[]{:S(2)}, u32[]{:S(2)}) collective-permute-start(bf16[128,2048]{1,0:T(8,128)(2,1)S(1)} %fusion.4.refs_1_), channel_id=1, source_target_pairs={{0,3},{1,0},{2,1},{3,2},{4,7},{5,4},{6,5},{7,6},{8,11},{9,8},{10,9... | collective-permute-start | bytes 1572872 | tf_op jit(solution)/shard_map/ppermute | solution.py:30
  32.5 12.3 %collective-permute-done.4.refs_1_ = bf16[128,2048]{1,0:T(8,128)(2,1)S(1)} collective-permute-done((bf16[128,2048]{1,0:T(8,128)(2,1)S(1)}, bf16[128,2048]{1,0:T(8,128)(2,1)S(1)}, u32[]{:S(2)}, u32[]{:S(2)}) %collective-permute-start.4) | collective-permute-done | bytes 524320 | tf_op jit(solution)/shard_map/ppermute | solution.py:30
  46.8 1.3 fusion.11
  48.3 18.5 %collective-permute-done.22.refs_1_ = bf16[128,2048]{1,0:T(8,128)(2,1)S(1)} collective-permute-done((bf16[128,2048]{1,0:T(8,128)(2,1)S(1)}, bf16[128,2048]{1,0:T(8,128)(2,1)S(1)}, u32[]{:S(2)}, u32[]{:S(2)}) %collective-permute-start.22) | collective-permute-done | bytes 524320 | tf_op jit(solution)/shard_map/ppermute | solution.py:30
  67.4 1.8 collective-permute-start.25
  70.6 1.5 collective-permute-start.3
  72.1 5.2 %collective-permute-done.24.refs_2_ = bf16[72,2048]{1,0:T(8,128)(2,1)S(1)} collective-permute-done((bf16[72,2048]{1,0:T(8,128)(2,1)S(1)}, bf16[72,2048]{1,0:T(8,128)(2,1)S(1)}, u32[]{:S(2)}, u32[]{:S(2)}) %collective-permute-start.24) | collective-permute-done | bytes 294944 | tf_op jit(solution)/shard_map/ppermute | solution.py:76
  77.2 8.4 %load.1 = (bf16[8,2048,256]{2,1,0:T(8,128)(2,1)S(1)}, bf16[8,2048,256]{2,1,0:T(8,128)(2,1)S(1)}, bf16[8,256,2048]{2,1,0:T(8,128)(2,1)S(1)}) custom-call(bf16[8,2048,256]{2,1,0:T(8,128)(2,1)} %refs_0_.1, bf16[8,2048,256]{2,1,0:T(8,128)(2,1)} %refs_1_.1, bf16[8,256,2048]{2,1,0:T(8,128)(2,1)} %refs_2_.1), custom_call_target="tpu_custom_call" | custom-call | tf_op jit(solution)/shard_map/load/pallas_call | solution.py:101
  85.7 5.5 %experts.5 = (bf16[72,2048]{1,0:T(8,128)(2,1)S(1)}, bf16[72,2048]{1,0:T(8,128)(2,1)S(1)}, bf16[72,2048]{1,0:T(8,128)(2,1)S(1)}, bf16[72,2048]{1,0:T(8,128)(2,1)S(1)}) custom-call(bf16[72,2048]{1,0:T(8,128)(2,1)S(1)} %get-tuple-element.73.refs_0_, bf16[72,2048]{1,0:T(8,128)(2,1)S(1)} %collective-permute-done.23.refs_1_, ...), custom_call_target="tpu_custom_call" | custom-call | flops 905969664 | bytes 27525120 | tf_op jit(solution)/shard_map/experts/pallas_call | solution.py:260
  91.2 1.9 %collective-permute-start.14 = (bf16[72,2048]{1,0:T(8,128)(2,1)S(1)}, bf16[72,2048]{1,0:T(8,128)(2,1)S(1)}, u32[]{:S(2)}, u32[]{:S(2)}) collective-permute-start(bf16[72,2048]{1,0:T(8,128)(2,1)S(1)} %get-tuple-element.64), channel_id=1, source_target_pairs={{0,12},{4,8},{8,4},{12,0},{1,13},{5,9},{9,5},{13,1},{2,14},{6,10},... | collective-permute-start | bytes 884744 | tf_op jit(solution)/shard_map/ppermute | solution.py:76
  93.4 1.7 collective-permute-done.3.refs_3_
  95.7 1.6 collective-permute-start.28
  97.8 4.7 %collective-permute-done.13.refs_2_ = bf16[72,2048]{1,0:T(8,128)(2,1)S(1)} collective-permute-done((bf16[72,2048]{1,0:T(8,128)(2,1)S(1)}, bf16[72,2048]{1,0:T(8,128)(2,1)S(1)}, u32[]{:S(2)}, u32[]{:S(2)}) %collective-permute-start.13) | collective-permute-done | bytes 294944 | tf_op jit(solution)/shard_map/ppermute | solution.py:76
  102.5 5.2 %collective-permute-done.14.refs_3_ = bf16[72,2048]{1,0:T(8,128)(2,1)S(1)} collective-permute-done((bf16[72,2048]{1,0:T(8,128)(2,1)S(1)}, bf16[72,2048]{1,0:T(8,128)(2,1)S(1)}, u32[]{:S(2)}, u32[]{:S(2)}) %collective-permute-start.14) | collective-permute-done | bytes 294944 | tf_op jit(solution)/shard_map/ppermute | solution.py:76
  108.4 1.6 collective-permute-start.7
  110.0 5.5 %experts.4 = (bf16[72,2048]{1,0:T(8,128)(2,1)S(1)}, bf16[72,2048]{1,0:T(8,128)(2,1)S(1)}, bf16[72,2048]{1,0:T(8,128)(2,1)S(1)}, bf16[72,2048]{1,0:T(8,128)(2,1)S(1)}) custom-call(bf16[72,2048]{1,0:T(8,128)(2,1)S(1)} %get-tuple-element.61.refs_0_, bf16[72,2048]{1,0:T(8,128)(2,1)S(1)} %collective-permute-done.12.refs_1_, ...), custom_call_target="tpu_custom_call" | custom-call | flops 905969664 | bytes 27525120 | tf_op jit(solution)/shard_map/experts/pallas_call | solution.py:260
  115.6 4.8 %collective-permute-done.28.refs_5_ = bf16[72,2048]{1,0:T(8,128)(2,1)S(1)} collective-permute-done((bf16[72,2048]{1,0:T(8,128)(2,1)S(1)}, bf16[72,2048]{1,0:T(8,128)(2,1)S(1)}, u32[]{:S(2)}, u32[]{:S(2)}) %collective-permute-start.28) | collective-permute-done | bytes 294944 | tf_op jit(solution)/shard_map/ppermute | solution.py:76
  122.1 5.7 %collective-permute-done.6.refs_6_ = bf16[72,2048]{1,0:T(8,128)(2,1)S(1)} collective-permute-done((bf16[72,2048]{1,0:T(8,128)(2,1)S(1)}, bf16[72,2048]{1,0:T(8,128)(2,1)S(1)}, u32[]{:S(2)}, u32[]{:S(2)}) %collective-permute-start.6) | collective-permute-done | bytes 294944 | tf_op jit(solution)/shard_map/ppermute | solution.py:76
  127.8 5.2 %collective-permute-done.7.refs_7_ = bf16[72,2048]{1,0:T(8,128)(2,1)S(1)} collective-permute-done((bf16[72,2048]{1,0:T(8,128)(2,1)S(1)}, bf16[72,2048]{1,0:T(8,128)(2,1)S(1)}, u32[]{:S(2)}, u32[]{:S(2)}) %collective-permute-start.7) | collective-permute-done | bytes 294944 | tf_op jit(solution)/shard_map/ppermute | solution.py:76
  133.0 5.7 %experts.3 = (bf16[72,2048]{1,0:T(8,128)(2,1)S(1)}, bf16[72,2048]{1,0:T(8,128)(2,1)S(1)}, bf16[72,2048]{1,0:T(8,128)(2,1)S(1)}, bf16[72,2048]{1,0:T(8,128)(2,1)S...) custom-call(bf16[72,2048]{1,0:T(8,128)(2,1)S(1)} %get-tuple-element., ...), custom_call_target="tpu_custom_call" | custom-call | flops 1811939328 | bytes 29884416 | tf_op jit(solution)/shard_map/experts/pallas_call | solution.py:260
  140.0 1.7 collective-permute-start.20
  141.8 7.2 %collective-permute-done.17.refs_5_ = bf16[72,2048]{1,0:T(8,128)(2,1)S(1)} collective-permute-done((bf16[72,2048]{1,0:T(8,128)(2,1)S(1)}, bf16[72,2048]{1,0:T(8,128)(2,1)S(1)}, u32[]{:S(2)}, u32[]{:S(2)}) %collective-permute-start.17) | collective-permute-done | bytes 294944 | tf_op jit(solution)/shard_map/ppermute | solution.py:76
  149.9 6.0 %collective-permute-done.20.refs_4_ = bf16[72,2048]{1,0:T(8,128)(2,1)S(1)} collective-permute-done((bf16[72,2048]{1,0:T(8,128)(2,1)S(1)}, bf16[72,2048]{1,0:T(8,128)(2,1)S(1)}, u32[]{:S(2)}, u32[]{:S(2)}) %collective-permute-start.20) | collective-permute-done | bytes 294944 | tf_op jit(solution)/shard_map/ppermute | solution.py:76
  155.9 5.8 %collective-permute-done.21.refs_5_ = bf16[72,2048]{1,0:T(8,128)(2,1)S(1)} collective-permute-done((bf16[72,2048]{1,0:T(8,128)(2,1)S(1)}, bf16[72,2048]{1,0:T(8,128)(2,1)S(1)}, u32[]{:S(2)}, u32[]{:S(2)}) %collective-permute-start.21) | collective-permute-done | bytes 294944 | tf_op jit(solution)/shard_map/ppermute | solution.py:76
  163.1 1.9 %collective-permute-start.9 = (bf16[72,2048]{1,0:T(8,128)(2,1)S(1)}, bf16[72,2048]{1,0:T(8,128)(2,1)S(1)}, u32[]{:S(2)}, u32[]{:S(2)}) collective-permute-start(bf16[72,2048]{1,0:T(8,128)(2,1)S(1)} %get-tuple-element.59), channel_id=1, source_target_pairs={{8,0},{12,4},{0,8},{4,12},{9,1},{13,5},{1,9},{5,13},{10,2},{14,6},... | collective-permute-start | bytes 884744 | tf_op jit(solution)/shard_map/ppermute | solution.py:76
  164.9 6.8 %collective-permute-done.10.refs_7_ = bf16[72,2048]{1,0:T(8,128)(2,1)S(1)} collective-permute-done((bf16[72,2048]{1,0:T(8,128)(2,1)S(1)}, bf16[72,2048]{1,0:T(8,128)(2,1)S(1)}, u32[]{:S(2)}, u32[]{:S(2)}) %collective-permute-start.10) | collective-permute-done | bytes 294944 | tf_op jit(solution)/shard_map/ppermute | solution.py:76
  171.7 6.7 %collective-permute-done.9.refs_6_ = bf16[72,2048]{1,0:T(8,128)(2,1)S(1)} collective-permute-done((bf16[72,2048]{1,0:T(8,128)(2,1)S(1)}, bf16[72,2048]{1,0:T(8,128)(2,1)S(1)}, u32[]{:S(2)}, u32[]{:S(2)}) %collective-permute-start.9) | collective-permute-done | bytes 294944 | tf_op jit(solution)/shard_map/ppermute | solution.py:76
  178.4 1.8 %finish.1 = bf16[128,2048]{1,0:T(8,128)(2,1)} custom-call(s32[4,128,2]{2,1,0:T(8,128)S(1)} %bitcast.31, f32[4,128,2]{2,1,0:T(8,128)S(1)} %bitcast.35, bf16[128,2048]{1,0:T(8,128)(2,1)S(1)} %get-tuple-element.82.refs_2_, f32[1,2048]{1,0:T(1,128)S(1)} %bitcast.36, bf16[72,2048]{1,0:T(8,128)(2,1)S(1)} %get-tuple-element.57.refs_4_, ...), custom_call_target="tpu_custom_call" | custom-call | tf_op jit(solution)/shard_map/finish/pallas_call | solution.py:198
  (107 shorter events, 19.0 us)
Async XLA Ops:
  0.8 3.9 %collective-permute-start = (bf16[15,256]{1,0:T(8,128)(2,1)S(1)}, bf16[15,256]{1,0:T(8,128)(2,1)S(1)}, u32[]{:S(2)}, u32[]{:S(2)}) collective-permute-start(bf16[15,256]{1,0:T(8,128)(2,1)S(1)} %slice.67), channel_id=1, source_target_pairs={{0,4},{4,8},{8,12},{1,5},{5,9},{9,13},{2,6},{6,10},{10,14},{3,7},{... | collective-permute-start | bytes 23048 | tf_op jit(solution)/shard_map/ppermute | solution.py:25
  7.2 15.8 %all-to-all-start = ((bf16[4,136,256]{2,1,0:T(8,128)(2,1)}), bf16[4,136,256]{2,1,0:T(8,128)(2,1)S(1)}, u32[]{:S(2)}, u32[]{:S(2)}) async-start(bf16[4,136,256]{2,1,0:T(8,128)(2,1)} %pad_maximum_fusion), calls=%async_computation | async-start | bytes 557056 | tf_op jit(solution)/shard_map/all_to_all | solution.py:304
  28.2 16.7 %collective-permute-start.4 = (bf16[128,2048]{1,0:T(8,128)(2,1)S(1)}, bf16[128,2048]{1,0:T(8,128)(2,1)S(1)}, u32[]{:S(2)}, u32[]{:S(2)}) collective-permute-start(bf16[128,2048]{1,0:T(8,128)(2,1)S(1)} %fusion.4.refs_1_), channel_id=1, source_target_pairs={{0,1},{1,2},{2,3},{3,0},{4,5},{5,6},{6,7},{7,4},{8,9},{9,10},{10,1... | collective-permute-start | bytes 1572872 | tf_op jit(solution)/shard_map/ppermute | solution.py:30
  28.2 41.8 %collective-permute-start.11 = (bf16[128,2048]{1,0:T(8,128)(2,1)S(1)}, bf16[128,2048]{1,0:T(8,128)(2,1)S(1)}, u32[]{:S(2)}, u32[]{:S(2)}) collective-permute-start(bf16[128,2048]{1,0:T(8,128)(2,1)S(1)} %fusion.4.refs_1_), channel_id=1, source_target_pairs={{0,3},{1,0},{2,1},{3,2},{4,7},{5,4},{6,5},{7,6},{8,11},{9,8},{10,9... | collective-permute-start | bytes 1572872 | tf_op jit(solution)/shard_map/ppermute | solution.py:30
  44.9 21.9 %collective-permute-start.22 = (bf16[128,2048]{1,0:T(8,128)(2,1)S(1)}, bf16[128,2048]{1,0:T(8,128)(2,1)S(1)}, u32[]{:S(2)}, u32[]{:S(2)}) collective-permute-start(bf16[128,2048]{1,0:T(8,128)(2,1)S(1)} %collective-permute-done.4.refs_1_), channel_id=1, source_target_pairs={{0,1},{1,2},{2,3},{3,0},{4,5},{5,6},{6,7},{7,4},{8,9},{9,10},{10,1... | collective-permute-start | bytes 1572872 | tf_op jit(solution)/shard_map/ppermute | solution.py:30
  67.2 3.4 %collective-permute-start.23 = (bf16[72,2048]{1,0:T(8,128)(2,1)S(1)}, bf16[72,2048]{1,0:T(8,128)(2,1)S(1)}, u32[]{:S(2)}, u32[]{:S(2)}) collective-permute-start(bf16[72,2048]{1,0:T(8,128)(2,1)S(1)} %get-tuple-element.74), channel_id=1, source_target_pairs={{0,4},{4,0},{8,12},{12,8},{1,5},{5,1},{9,13},{13,9},{2,6},{6,2},{1... | collective-permute-start | bytes 884744 | tf_op jit(solution)/shard_map/ppermute | solution.py:76
  67.3 9.9 %collective-permute-start.24 = (bf16[72,2048]{1,0:T(8,128)(2,1)S(1)}, bf16[72,2048]{1,0:T(8,128)(2,1)S(1)}, u32[]{:S(2)}, u32[]{:S(2)}) collective-permute-start(bf16[72,2048]{1,0:T(8,128)(2,1)S(1)} %get-tuple-element.75), channel_id=1, source_target_pairs={{0,8},{4,12},{8,0},{12,4},{1,9},{5,13},{9,1},{13,5},{2,10},{6,14},... | collective-permute-start | bytes 884744 | tf_op jit(solution)/shard_map/ppermute | solution.py:76
  67.4 18.3 %collective-permute-start.25 = (bf16[72,2048]{1,0:T(8,128)(2,1)S(1)}, bf16[72,2048]{1,0:T(8,128)(2,1)S(1)}, u32[]{:S(2)}, u32[]{:S(2)}) collective-permute-start(bf16[72,2048]{1,0:T(8,128)(2,1)S(1)} %get-tuple-element.76), channel_id=1, source_target_pairs={{0,12},{4,8},{8,4},{12,0},{1,13},{5,9},{9,5},{13,1},{2,14},{6,10},... | collective-permute-start | bytes 884744 | tf_op jit(solution)/shard_map/ppermute | solution.py:76
  69.6 21.6 %collective-permute-start.1 = (bf16[72,2048]{1,0:T(8,128)(2,1)S(1)}, bf16[72,2048]{1,0:T(8,128)(2,1)S(1)}, u32[]{:S(2)}, u32[]{:S(2)}) collective-permute-start(bf16[72,2048]{1,0:T(8,128)(2,1)S(1)} %get-tuple-element.47), channel_id=1, source_target_pairs={{0,4},{4,0},{8,12},{12,8},{1,5},{5,1},{9,13},{13,9},{2,6},{6,2},{1... | collective-permute-start | bytes 884744 | tf_op jit(solution)/shard_map/ppermute | solution.py:76
  70.0 23.1 %collective-permute-start.2 = (bf16[72,2048]{1,0:T(8,128)(2,1)S(1)}, bf16[72,2048]{1,0:T(8,128)(2,1)S(1)}, u32[]{:S(2)}, u32[]{:S(2)}) collective-permute-start(bf16[72,2048]{1,0:T(8,128)(2,1)S(1)} %get-tuple-element.48), channel_id=1, source_target_pairs={{0,8},{4,12},{8,0},{12,4},{1,9},{5,13},{9,1},{13,5},{2,10},{6,14},... | collective-permute-start | bytes 884744 | tf_op jit(solution)/shard_map/ppermute | solution.py:76
  70.6 24.5 %collective-permute-start.3 = (bf16[72,2048]{1,0:T(8,128)(2,1)S(1)}, bf16[72,2048]{1,0:T(8,128)(2,1)S(1)}, u32[]{:S(2)}, u32[]{:S(2)}) collective-permute-start(bf16[72,2048]{1,0:T(8,128)(2,1)S(1)} %get-tuple-element.49), channel_id=1, source_target_pairs={{0,12},{4,8},{8,4},{12,0},{1,13},{5,9},{9,5},{13,1},{2,14},{6,10},... | collective-permute-start | bytes 884744 | tf_op jit(solution)/shard_map/ppermute | solution.py:76
  77.2 18.5 %collective-permute-start.12 = (bf16[72,2048]{1,0:T(8,128)(2,1)S(1)}, bf16[72,2048]{1,0:T(8,128)(2,1)S(1)}, u32[]{:S(2)}, u32[]{:S(2)}) collective-permute-start(bf16[72,2048]{1,0:T(8,128)(2,1)S(1)} %get-tuple-element.62), channel_id=1, source_target_pairs={{0,4},{4,0},{8,12},{12,8},{1,5},{5,1},{9,13},{13,9},{2,6},{6,2},{1... | collective-permute-start | bytes 884744 | tf_op jit(solution)/shard_map/ppermute | solution.py:76
  85.6 16.9 %collective-permute-start.13 = (bf16[72,2048]{1,0:T(8,128)(2,1)S(1)}, bf16[72,2048]{1,0:T(8,128)(2,1)S(1)}, u32[]{:S(2)}, u32[]{:S(2)}) collective-permute-start(bf16[72,2048]{1,0:T(8,128)(2,1)S(1)} %get-tuple-element.63), channel_id=1, source_target_pairs={{0,8},{4,12},{8,0},{12,4},{1,9},{5,13},{9,1},{13,5},{2,10},{6,14},... | collective-permute-start | bytes 884744 | tf_op jit(solution)/shard_map/ppermute | solution.py:76
  91.2 16.5 %collective-permute-start.14 = (bf16[72,2048]{1,0:T(8,128)(2,1)S(1)}, bf16[72,2048]{1,0:T(8,128)(2,1)S(1)}, u32[]{:S(2)}, u32[]{:S(2)}) collective-permute-start(bf16[72,2048]{1,0:T(8,128)(2,1)S(1)} %get-tuple-element.64), channel_id=1, source_target_pairs={{0,12},{4,8},{8,4},{12,0},{1,13},{5,9},{9,5},{13,1},{2,14},{6,10},... | collective-permute-start | bytes 884744 | tf_op jit(solution)/shard_map/ppermute | solution.py:76
  93.2 15.2 %collective-permute-start.26 = (bf16[72,2048]{1,0:T(8,128)(2,1)S(1)}, bf16[72,2048]{1,0:T(8,128)(2,1)S(1)}, u32[]{:S(2)}, u32[]{:S(2)}) collective-permute-start(bf16[72,2048]{1,0:T(8,128)(2,1)S(1)} %get-tuple-element.78), channel_id=1, source_target_pairs={{4,0},{0,4},{12,8},{8,12},{5,1},{1,5},{13,9},{9,13},{6,2},{2,6},{1... | collective-permute-start | bytes 884744 | tf_op jit(solution)/shard_map/ppermute | solution.py:76
  95.1 20.4 %collective-permute-start.27 = (bf16[72,2048]{1,0:T(8,128)(2,1)S(1)}, bf16[72,2048]{1,0:T(8,128)(2,1)S(1)}, u32[]{:S(2)}, u32[]{:S(2)}) collective-permute-start(bf16[72,2048]{1,0:T(8,128)(2,1)S(1)} %get-tuple-element.79), channel_id=1, source_target_pairs={{8,0},{12,4},{0,8},{4,12},{9,1},{13,5},{1,9},{5,13},{10,2},{14,6},... | collective-permute-start | bytes 884744 | tf_op jit(solution)/shard_map/ppermute | solution.py:76
  95.7 24.6 %collective-permute-start.28 = (bf16[72,2048]{1,0:T(8,128)(2,1)S(1)}, bf16[72,2048]{1,0:T(8,128)(2,1)S(1)}, u32[]{:S(2)}, u32[]{:S(2)}) collective-permute-start(bf16[72,2048]{1,0:T(8,128)(2,1)S(1)} %get-tuple-element.80), channel_id=1, source_target_pairs={{12,0},{8,4},{4,8},{0,12},{13,1},{9,5},{5,9},{1,13},{14,2},{10,6},... | collective-permute-start | bytes 884744 | tf_op jit(solution)/shard_map/ppermute | solution.py:76
  102.5 19.3 %collective-permute-start.5 = (bf16[72,2048]{1,0:T(8,128)(2,1)S(1)}, bf16[72,2048]{1,0:T(8,128)(2,1)S(1)}, u32[]{:S(2)}, u32[]{:S(2)}) collective-permute-start(bf16[72,2048]{1,0:T(8,128)(2,1)S(1)} %get-tuple-element.51), channel_id=1, source_target_pairs={{0,4},{4,0},{8,12},{12,8},{1,5},{5,1},{9,13},{13,9},{2,6},{6,2},{1... | collective-permute-start | bytes 884744 | tf_op jit(solution)/shard_map/ppermute | solution.py:76
  107.7 20.0 %collective-permute-start.6 = (bf16[72,2048]{1,0:T(8,128)(2,1)S(1)}, bf16[72,2048]{1,0:T(8,128)(2,1)S(1)}, u32[]{:S(2)}, u32[]{:S(2)}) collective-permute-start(bf16[72,2048]{1,0:T(8,128)(2,1)S(1)} %get-tuple-element.52), channel_id=1, source_target_pairs={{0,8},{4,12},{8,0},{12,4},{1,9},{5,13},{9,1},{13,5},{2,10},{6,14},... | collective-permute-start | bytes 884744 | tf_op jit(solution)/shard_map/ppermute | solution.py:76
  108.4 24.6 %collective-permute-start.7 = (bf16[72,2048]{1,0:T(8,128)(2,1)S(1)}, bf16[72,2048]{1,0:T(8,128)(2,1)S(1)}, u32[]{:S(2)}, u32[]{:S(2)}) collective-permute-start(bf16[72,2048]{1,0:T(8,128)(2,1)S(1)} %get-tuple-element.53), channel_id=1, source_target_pairs={{0,12},{4,8},{8,4},{12,0},{1,13},{5,9},{9,5},{13,1},{2,14},{6,10},... | collective-permute-start | bytes 884744 | tf_op jit(solution)/shard_map/ppermute | solution.py:76
  115.5 24.5 %collective-permute-start.15 = (bf16[72,2048]{1,0:T(8,128)(2,1)S(1)}, bf16[72,2048]{1,0:T(8,128)(2,1)S(1)}, u32[]{:S(2)}, u32[]{:S(2)}) collective-permute-start(bf16[72,2048]{1,0:T(8,128)(2,1)S(1)} %get-tuple-element.66), channel_id=1, source_target_pairs={{4,0},{0,4},{12,8},{8,12},{5,1},{1,5},{13,9},{9,13},{6,2},{2,6},{1... | collective-permute-start | bytes 884744 | tf_op jit(solution)/shard_map/ppermute | solution.py:76
  120.4 21.3 %collective-permute-start.16 = (bf16[72,2048]{1,0:T(8,128)(2,1)S(1)}, bf16[72,2048]{1,0:T(8,128)(2,1)S(1)}, u32[]{:S(2)}, u32[]{:S(2)}) collective-permute-start(bf16[72,2048]{1,0:T(8,128)(2,1)S(1)} %get-tuple-element.67), channel_id=1, source_target_pairs={{8,0},{12,4},{0,8},{4,12},{9,1},{13,5},{1,9},{5,13},{10,2},{14,6},... | collective-permute-start | bytes 884744 | tf_op jit(solution)/shard_map/ppermute | solution.py:76
  121.8 39.9 %collective-permute-start.29 = (bf16[128,2048]{1,0:T(8,128)(2,1)S(1)}, bf16[128,2048]{1,0:T(8,128)(2,1)S(1)}, u32[]{:S(2)}, u32[]{:S(2)}) collective-permute-start(bf16[128,2048]{1,0:T(8,128)(2,1)S(1)} %combine.4), channel_id=1, source_target_pairs={{0,3},{1,0},{2,1},{3,2},{4,7},{5,4},{6,5},{7,6},{8,11},{9,8},{10,9... | collective-permute-start | bytes 1572872 | tf_op jit(solution)/shard_map/ppermute | solution.py:30
  138.7 11.2 %collective-permute-start.19 = (bf16[72,2048]{1,0:T(8,128)(2,1)S(1)}, bf16[72,2048]{1,0:T(8,128)(2,1)S(1)}, u32[]{:S(2)}, u32[]{:S(2)}) collective-permute-start(bf16[72,2048]{1,0:T(8,128)(2,1)S(1)} %get-tuple-element.70), channel_id=1, source_target_pairs={{4,0},{0,4},{12,8},{8,12},{5,1},{1,5},{13,9},{9,13},{6,2},{2,6},{1... | collective-permute-start | bytes 884744 | tf_op jit(solution)/shard_map/ppermute | solution.py:76
  140.0 9.0 %collective-permute-start.17 = (bf16[72,2048]{1,0:T(8,128)(2,1)S(1)}, bf16[72,2048]{1,0:T(8,128)(2,1)S(1)}, u32[]{:S(2)}, u32[]{:S(2)}) collective-permute-start(bf16[72,2048]{1,0:T(8,128)(2,1)S(1)} %get-tuple-element.68), channel_id=1, source_target_pairs={{12,0},{8,4},{4,8},{0,12},{13,1},{9,5},{5,9},{1,13},{14,2},{10,6},... | collective-permute-start | bytes 884744 | tf_op jit(solution)/shard_map/ppermute | solution.py:76
  140.0 15.9 %collective-permute-start.20 = (bf16[72,2048]{1,0:T(8,128)(2,1)S(1)}, bf16[72,2048]{1,0:T(8,128)(2,1)S(1)}, u32[]{:S(2)}, u32[]{:S(2)}) collective-permute-start(bf16[72,2048]{1,0:T(8,128)(2,1)S(1)} %get-tuple-element.71), channel_id=1, source_target_pairs={{8,0},{12,4},{0,8},{4,12},{9,1},{13,5},{1,9},{5,13},{10,2},{14,6},... | collective-permute-start | bytes 884744 | tf_op jit(solution)/shard_map/ppermute | solution.py:76
  141.7 20.0 %collective-permute-start.21 = (bf16[72,2048]{1,0:T(8,128)(2,1)S(1)}, bf16[72,2048]{1,0:T(8,128)(2,1)S(1)}, u32[]{:S(2)}, u32[]{:S(2)}) collective-permute-start(bf16[72,2048]{1,0:T(8,128)(2,1)S(1)} %get-tuple-element.72), channel_id=1, source_target_pairs={{12,0},{8,4},{4,8},{0,12},{13,1},{9,5},{5,9},{1,13},{14,2},{10,6},... | collective-permute-start | bytes 884744 | tf_op jit(solution)/shard_map/ppermute | solution.py:76
  149.8 28.6 %collective-permute-start.18 = (bf16[128,2048]{1,0:T(8,128)(2,1)S(1)}, bf16[128,2048]{1,0:T(8,128)(2,1)S(1)}, u32[]{:S(2)}, u32[]{:S(2)}) collective-permute-start(bf16[128,2048]{1,0:T(8,128)(2,1)S(1)} %combine.3), channel_id=1, source_target_pairs={{0,1},{1,2},{2,3},{3,0},{4,5},{5,6},{6,7},{7,4},{8,9},{9,10},{10,1... | collective-permute-start | bytes 1572872 | tf_op jit(solution)/shard_map/ppermute | solution.py:30
  162.5 15.9 %collective-permute-start.30 = (bf16[128,2048]{1,0:T(8,128)(2,1)S(1)}, bf16[128,2048]{1,0:T(8,128)(2,1)S(1)}, u32[]{:S(2)}, u32[]{:S(2)}) collective-permute-start(bf16[128,2048]{1,0:T(8,128)(2,1)S(1)} %combine.5), channel_id=1, source_target_pairs={{0,3},{1,0},{2,1},{3,2},{4,7},{5,4},{6,5},{7,6},{8,11},{9,8},{10,9... | collective-permute-start | bytes 1572872 | tf_op jit(solution)/shard_map/ppermute | solution.py:30
  162.8 8.9 %collective-permute-start.10 = (bf16[72,2048]{1,0:T(8,128)(2,1)S(1)}, bf16[72,2048]{1,0:T(8,128)(2,1)S(1)}, u32[]{:S(2)}, u32[]{:S(2)}) collective-permute-start(bf16[72,2048]{1,0:T(8,128)(2,1)S(1)} %get-tuple-element.60), channel_id=1, source_target_pairs={{12,0},{8,4},{4,8},{0,12},{13,1},{9,5},{5,9},{1,13},{14,2},{10,6},... | collective-permute-start | bytes 884744 | tf_op jit(solution)/shard_map/ppermute | solution.py:76
  162.8 8.9 %collective-permute-start.8 = (bf16[72,2048]{1,0:T(8,128)(2,1)S(1)}, bf16[72,2048]{1,0:T(8,128)(2,1)S(1)}, u32[]{:S(2)}, u32[]{:S(2)}) collective-permute-start(bf16[72,2048]{1,0:T(8,128)(2,1)S(1)} %get-tuple-element.58), channel_id=1, source_target_pairs={{4,0},{0,4},{12,8},{8,12},{5,1},{1,5},{13,9},{9,13},{6,2},{2,6},{1... | collective-permute-start | bytes 884744 | tf_op jit(solution)/shard_map/ppermute | solution.py:76
  163.1 15.3 %collective-permute-start.9 = (bf16[72,2048]{1,0:T(8,128)(2,1)S(1)}, bf16[72,2048]{1,0:T(8,128)(2,1)S(1)}, u32[]{:S(2)}, u32[]{:S(2)}) collective-permute-start(bf16[72,2048]{1,0:T(8,128)(2,1)S(1)} %get-tuple-element.59), channel_id=1, source_target_pairs={{8,0},{12,4},{0,8},{4,12},{9,1},{13,5},{1,9},{5,13},{10,2},{14,6},... | collective-permute-start | bytes 884744 | tf_op jit(solution)/shard_map/ppermute | solution.py:76
  (7 other events, 195.6 us)

commit v3 on v2

--- a/solution.py
+++ b/solution.py
@@ -78,16 +78,18 @@
 
 LANES = 128
 IN_VMEM = pl.BlockSpec(memory_space=pltpu.VMEM)
+IN_SMEM = pl.BlockSpec(memory_space=pltpu.SMEM)
 
 
 def load_body(*refs):
     half = len(refs) // 2
     sources, targets, done = refs[:half], refs[half:-1], refs[-1]
-    copies = [
-        pltpu.make_async_copy(source.at[e], target.at[e], done.at[i, e])
-        for i, (source, target) in enumerate(zip(sources, targets))
-        for e in range(source.shape[0])
-    ]
+    copies = []
+    for source, target in zip(sources, targets):
+        parts = range(source.shape[0]) if len(source.shape) == 3 else [...]
+        for e in parts:
+            at = done.at[len(copies)]
+            copies.append(pltpu.make_async_copy(source.at[e], target.at[e], at))
     for copy in copies:
         copy.start()
     for copy in copies:
@@ -98,12 +100,13 @@
 
 
 def load(*weights):
+    count = sum(w.shape[0] if w.ndim == 3 else 1 for w in weights)
     return pl.pallas_call(
         load_body,
         in_specs=[pl.BlockSpec(memory_space=pltpu.HBM)] * len(weights),
         out_specs=[IN_VMEM] * len(weights),
         out_shape=[pltpu.VMEM(w.shape, w.dtype) for w in weights],
-        scratch_shapes=[pltpu.SemaphoreType.DMA((len(weights), weights[0].shape[0]))],
+        scratch_shapes=[pltpu.SemaphoreType.DMA((count,))],
         compiler_params=pltpu.CompilerParams(vmem_limit_bytes=LOAD_LIMIT << 20),
         name="load",
     )(*weights)
@@ -269,7 +272,7 @@
     )(*xs, w_gate, w_up, w_down)
 
 
-def per_device(
+def plain_path(
     resid_in,
     pool_input,
     pool_weight,
@@ -327,7 +330,6 @@
             blocks[k] = rotated(blocks[k - by], "tp", by)
 
     here = lax.axis_index("tp")
-    sp_here = lax.axis_index("sp")
     fields = jnp.take(fields, (here - jnp.array(order)) % n_tp, axis=0)
     route = fields[:, :TOP].astype(jnp.int32)
     weight = fields[:, TOP:].astype(jnp.float32)
@@ -342,66 +344,285 @@
     )
     slot_rank = jnp.sum(rank[:, None] * onehot, axis=-1).astype(jnp.int32)
 
-    if local_experts % 8 == 0 and CAP % 8 and n_sp <= 4:
-        owner = offset_to(route // local_experts, sp_here, n_sp)
-        expert = route % local_experts
-        whole = CAP // 8 * 8
-        in_tile = expert * whole + slot_rank
-        apart = (local_experts - expert) * whole + (slot_rank - whole) * local_experts + expert
-        slot = owner * slot_rows + jnp.where(slot_rank < whole, in_tile, expert * whole + apart)
-        by_row = slot.transpose(0, 2, 1)
-        weight = weight.transpose(0, 2, 1)
-        slot, by_row, weight = lax.optimization_barrier((slot, by_row, weight))
-        weights = load(w_gate, w_up, w_down)
-        arrived, backs, parts = [], {}, {}
-        for at, k in enumerate(order):
-            rows = pick(at, slot, blocks[k], n_sp, slot_rows)
-            arrived.append([moved(x, "sp", d) if d else x for d, x in enumerate(rows)])
-        for first, stop in groups_of(n_tp):
-            group = arrived[first:stop]
-            terms = experts([x for xs in group for x in xs], *weights)
-            for at in range(first, stop):
-                back = terms[(at - first) * n_sp : (at - first + 1) * n_sp]
-                backs[at] = [moved(x, "sp", d, True) if d else x for d, x in enumerate(back)]
-        for at in return_order(n_tp)[:-1]:
-            k = order[at]
-            by = -1 if k <= far else 1
-            inner = k < far or k > far + 1
-            joined = [parts.pop(k - by)] if inner else []
-            part = combine(at, by_row, weight, backs[at], joined)
-            parts[k] = rotated(part, "tp", by)
-        return finish(0, by_row, weight, residual, post_gain, backs[0], list(parts.values()))
-    else:
-        slot_index = route * CAP + slot_rank
-        picker = slot_index[..., None] == lax.iota(jnp.int32, slot_total)
-        token_pick = jnp.sum(picker.astype(jnp.float32), axis=1).astype(jnp.bfloat16)
-        token_weight = jnp.sum(jnp.where(picker, weight[..., None], 0.0), axis=1)
-        token_weight = token_weight.astype(jnp.bfloat16)
-        arrived = []
-        for at, k in enumerate(order):
-            rows = lax.dot_general(
-                token_pick[at],
-                blocks[k],
-                (((0,), (0,)), ((), ())),
-                preferred_element_type=jnp.float32,
-            )
-            rows = rows.astype(jnp.bfloat16).reshape(n_sp, slot_rows, width)
-            arrived.append(lax.all_to_all(rows, "sp", split_axis=0, concat_axis=0, tiled=True))
-        arrived = jnp.stack(arrived).reshape(n_tp, n_sp, local_experts, CAP, width)
-        f32 = {"preferred_element_type": jnp.float32}
-        gate_pre = jnp.einsum("sklcd,ldf->sklcf", arrived, w_gate, **f32)
-        upward = jnp.einsum("sklcd,ldf->sklcf", arrived, w_up, **f32)
-        activated = clamped_unit(gate_pre, upward).astype(jnp.bfloat16)
-        terms = jnp.einsum("sklcf,lfd->sklcd", activated, w_down, **f32)
-        terms = terms.astype(jnp.bfloat16).reshape(n_tp, n_sp, slot_rows, width)
-        parts = {}
-        for at, k in enumerate(order):
-            back = lax.all_to_all(terms[at], "sp", split_axis=0, concat_axis=0, tiled=True)
-            part = jnp.dot(token_weight[at], back.reshape(slot_total, width), **f32)
-            part = part.astype(jnp.bfloat16)
-            parts[k] = rotated(part, "tp", -k) if k else part
+    slot_index = route * CAP + slot_rank
+    picker = slot_index[..., None] == lax.iota(jnp.int32, slot_total)
+    token_pick = jnp.sum(picker.astype(jnp.float32), axis=1).astype(jnp.bfloat16)
+    token_weight = jnp.sum(jnp.where(picker, weight[..., None], 0.0), axis=1)
+    token_weight = token_weight.astype(jnp.bfloat16)
+    arrived = []
+    for at, k in enumerate(order):
+        rows = lax.dot_general(
+            token_pick[at],
+            blocks[k],
+            (((0,), (0,)), ((), ())),
+            preferred_element_type=jnp.float32,
+        )
+        rows = rows.astype(jnp.bfloat16).reshape(n_sp, slot_rows, width)
+        arrived.append(lax.all_to_all(rows, "sp", split_axis=0, concat_axis=0, tiled=True))
+    arrived = jnp.stack(arrived).reshape(n_tp, n_sp, local_experts, CAP, width)
+    f32 = {"preferred_element_type": jnp.float32}
+    gate_pre = jnp.einsum("sklcd,ldf->sklcf", arrived, w_gate, **f32)
+    upward = jnp.einsum("sklcd,ldf->sklcf", arrived, w_up, **f32)
+    activated = clamped_unit(gate_pre, upward).astype(jnp.bfloat16)
+    terms = jnp.einsum("sklcf,lfd->sklcd", activated, w_down, **f32)
+    terms = terms.astype(jnp.bfloat16).reshape(n_tp, n_sp, slot_rows, width)
+    parts = {}
+    for at, k in enumerate(order):
+        back = lax.all_to_all(terms[at], "sp", split_axis=0, concat_axis=0, tiled=True)
+        part = jnp.dot(token_weight[at], back.reshape(slot_total, width), **f32)
+        part = part.astype(jnp.bfloat16)
+        parts[k] = rotated(part, "tp", -k) if k else part
     expert_mix = sum(parts[k].astype(jnp.float32) for k in order)
     return (residual.astype(jnp.float32) + rms_scale(expert_mix, post_gain)).astype(jnp.bfloat16)
+
+
+AHEAD = 16
+
+
+def cut_body(place, x, routes, weights, *outs):
+    chunks, tail = outs[:-1], outs[-1]
+    n_tp, rows = len(chunks), routes.shape[0]
+    top = routes.shape[1]
+    lane = lax.broadcasted_iota(jnp.int32, (rows, rows), 1)
+    fields = jnp.zeros((rows, rows), jnp.float32)
+    for k in range(top):
+        fields = jnp.where(lane == k, routes[:, k : k + 1].astype(jnp.float32), fields)
+        fields = jnp.where(lane == top + k, weights[:, k : k + 1], fields)
+    fields = fields.T[:8].astype(jnp.bfloat16)
+    for k, chunk in enumerate(chunks):
+        first = (place[0] + k) % n_tp * rows
+        before = pl.multiple_of(jnp.maximum(first - AHEAD, 0), AHEAD)
+        chunk[:AHEAD, :] = x[pl.ds(before, AHEAD), :]
+        chunk[AHEAD : AHEAD + rows, :] = x[pl.ds(pl.multiple_of(first, AHEAD), rows), :]
+        chunk[AHEAD + rows :, :] = jnp.zeros((8, chunk.shape[1]), jnp.bfloat16)
+        chunk[AHEAD + rows :, :rows] = fields
+    tail[...] = x[x.shape[0] - AHEAD :, :]
+
+
+def cut(place, x, routes, weights, n_tp):
+    rows, channels = routes.shape[0], x.shape[1]
+    chunk = jax.ShapeDtypeStruct((AHEAD + rows + 8, channels), x.dtype)
+    return pl.pallas_call(
+        cut_body,
+        in_specs=[IN_SMEM] + [IN_VMEM] * 3,
+        out_specs=[IN_VMEM] * (n_tp + 1),
+        out_shape=[chunk] * n_tp + [jax.ShapeDtypeStruct((AHEAD, channels), x.dtype)],
+        compiler_params=pltpu.CompilerParams(vmem_limit_bytes=6 << 20),
+        name="cut",
+    )(place, x, routes, weights)
+
+
+def mix_body(n_tp, place, *refs):
+    chunks, halos = refs[:n_tp], refs[n_tp : 2 * n_tp]
+    pool_w, scale, out_w, mix_gain, ffn_gain, resid = refs[2 * n_tp : 2 * n_tp + 6]
+    residual, normed, raw, pooled, mix = refs[2 * n_tp + 6 :]
+    rows, width = resid.shape
+    channels = chunks[0].shape[1]
+    tp, sp = place[0], place[1]
+    for k, chunk in enumerate(chunks):
+        source = (tp - k + n_tp) % n_tp
+        cols = pl.ds(pl.multiple_of(source * channels, LANES), channels)
+        raw[:, cols] = chunk[: AHEAD + rows, :].astype(jnp.float32)
+
+    @pl.when(tp == 0)
+    def _():
+        for j, halo in enumerate(halos):
+            raw[:AHEAD, j * channels : (j + 1) * channels] = halo[...].astype(jnp.float32)
+
+    start = (sp * n_tp + tp) * rows
+    position = start + lax.broadcasted_iota(jnp.int32, (rows, GROUP_DIM), 0) + 1
+    for g, window in enumerate(pool_windows):
+        cols = slice(g * GROUP_DIM, (g + 1) * GROUP_DIM)
+        own = raw[:, cols]
+        total, reach = own, 1
+        while reach < window:
+            total = total + pltpu.roll(total, reach, 0)
+            reach = 2 * reach
+        divisor = jnp.minimum(position, window).astype(jnp.float32)
+        mixed = (total[AHEAD:] / divisor - own[AHEAD:]).astype(jnp.bfloat16)
+        part = jnp.dot(mixed, pool_w[g], preferred_element_type=jnp.float32)
+        pooled[:, cols] = (part * scale[:, cols]).astype(jnp.bfloat16)
+
+    def columns():
+        return [slice(j, j + 2 * LANES) for j in range(0, width, 2 * LANES)]
+
+    def inverse_of(square):
+        return lax.rsqrt(jnp.sum(square, axis=1, keepdims=True) / width + norm_eps)
+
+    square = jnp.zeros((rows, LANES), jnp.float32)
+    for cols in columns():
+        part = jnp.dot(pooled[...], out_w[:, cols], preferred_element_type=jnp.float32)
+        mix[:, cols] = part
+        square = square + part[:, :LANES] * part[:, :LANES] + part[:, LANES:] * part[:, LANES:]
+    inverse = inverse_of(square)
+    square = jnp.zeros((rows, LANES), jnp.float32)
+    for cols in columns():
+        part = resid[:, cols].astype(jnp.float32) + mix[:, cols] * inverse * mix_gain[:, cols]
+        part = part.astype(jnp.bfloat16)
+        residual[:, cols] = part
+        part = part.astype(jnp.float32)
+        square = square + part[:, :LANES] * part[:, :LANES] + part[:, LANES:] * part[:, LANES:]
+    inverse = inverse_of(square)
+    for cols in columns():
+        part = residual[:, cols].astype(jnp.float32) * inverse * ffn_gain[:, cols]
+        normed[:, cols] = part.astype(normed.dtype)
+
+
+def mix_tokens(place, chunks, halos, pool_w, scale, out_w, mix_gain, ffn_gain, resid):
+    rows, width = resid.shape
+    total = out_w.shape[0]
+    return pl.pallas_call(
+        lambda *refs: mix_body(len(chunks), *refs),
+        in_specs=[IN_SMEM] + [IN_VMEM] * (2 * len(chunks) + 6),
+        out_specs=[IN_VMEM] * 2,
+        out_shape=[jax.ShapeDtypeStruct(resid.shape, resid.dtype)] * 2,
+        scratch_shapes=[
+            pltpu.VMEM((AHEAD + rows, total), jnp.float32),
+            pltpu.VMEM((rows, total), jnp.bfloat16),
+            pltpu.VMEM((rows, width), jnp.float32),
+        ],
+        compiler_params=pltpu.CompilerParams(vmem_limit_bytes=12 << 20),
+        name="mix",
+    )(
+        place,
+        *chunks,
+        *halos,
+        pool_w,
+        scale,
+        out_w,
+        mix_gain,
+        ffn_gain,
+        resid,
+    )
+
+
+def slots_body(n_sp, local, place, *refs):
+    chunks, (slot, by_row, weight) = refs[:-3], refs[-3:]
+    top, tokens = slot.shape[1], slot.shape[2]
+    n_experts = n_sp * local
+    expert = lax.broadcasted_iota(jnp.int32, (n_experts, tokens), 0)
+    row = lax.broadcasted_iota(jnp.int32, (tokens, tokens), 0)
+    lane = lax.broadcasted_iota(jnp.int32, (tokens, tokens), 1)
+    before = jnp.where(row < lane, 1.0, 0.0).astype(jnp.bfloat16)
+    whole = CAP // 8 * 8
+    for at, chunk in enumerate(chunks):
+        first = chunk.shape[0] - 8
+        fields = chunk[first:, :tokens].astype(jnp.float32)
+        hits = [
+            jnp.where(expert == fields[k : k + 1].astype(jnp.int32), 1.0, 0.0) for k in range(top)
+        ]
+        named = sum(hits).astype(jnp.bfloat16)
+        rank = jnp.dot(named, before, preferred_element_type=jnp.float32)
+        found = []
+        for k, hit in enumerate(hits):
+            mine = jnp.sum(rank * hit, axis=0, keepdims=True).astype(jnp.int32)
+            route = jnp.sum(expert.astype(jnp.float32) * hit, axis=0, keepdims=True)
+            owner = jnp.sum(
+                (expert // local).astype(jnp.float32) * hit, axis=0, keepdims=True
+            ).astype(jnp.int32)
+            inside = route.astype(jnp.int32) - owner * local
+            owner = offset_to(owner, place[1], n_sp)
+            in_tile = inside * whole + mine
+            apart = local * whole + (mine - whole) * local + inside
+            found.append(owner * local * CAP + jnp.where(mine < whole, in_tile, apart))
+            slot[at, k : k + 1, :] = found[-1]
+        rows8 = [x.astype(jnp.float32) for x in found] + [fields[top : 2 * top]]
+        rows8.append(jnp.zeros((tokens - 2 * top, tokens), jnp.float32))
+        turned = jnp.concatenate(rows8, axis=0).T
+        by_row[at] = turned[:, :top].astype(jnp.int32)
+        weight[at] = turned[:, top : 2 * top]
+
+
+def slots(place, chunks, n_sp, local, top, tokens):
+    n = len(chunks)
+    return pl.pallas_call(
+        lambda *refs: slots_body(n_sp, local, *refs),
+        in_specs=[IN_SMEM] + [IN_VMEM] * n,
+        out_specs=[IN_VMEM] * 3,
+        out_shape=[
+            jax.ShapeDtypeStruct((n, top, tokens), jnp.int32),
+            jax.ShapeDtypeStruct((n, tokens, top), jnp.int32),
+            jax.ShapeDtypeStruct((n, tokens, top), jnp.float32),
+        ],
+        compiler_params=pltpu.CompilerParams(vmem_limit_bytes=6 << 20),
+        name="slots",
+    )(place, *chunks)
+
+
+def kernel_path(
+    resid_in,
+    pool_input,
+    pool_weight,
+    pool_scale,
+    out_weight,
+    mix_gain,
+    ffn_gain,
+    w_gate,
+    w_up,
+    w_down,
+    routes,
+    route_weight,
+    post_gain,
+):
+    n_sp = lax.axis_size("sp")
+    n_tp = lax.axis_size("tp")
+    tok_rows = resid_in.shape[0]
+    local_experts = w_gate.shape[0]
+    slot_rows = local_experts * CAP
+
+    place = jnp.stack([lax.axis_index("tp"), lax.axis_index("sp")]).astype(jnp.int32)
+    *chunks, tail = cut(place, pool_input, routes, route_weight, n_tp)
+    halos = []
+    for j in range(n_tp):
+        pairs = [(s * n_tp + j, (s + 1) * n_tp) for s in range(n_sp - 1)]
+        halos.append(lax.ppermute(tail, ("sp", "tp"), pairs))
+    chunks = [rotated(x, "tp", k) if k else x for k, x in enumerate(chunks)]
+    small = [x.reshape(1, -1) for x in (pool_scale, mix_gain, ffn_gain)]
+    scale, mix_gain, ffn_gain, pool_weight, out_weight, resid_in = load(
+        *small, pool_weight, out_weight, resid_in
+    )
+    residual, normed = mix_tokens(
+        place, chunks, halos, pool_weight, scale, out_weight, mix_gain, ffn_gain, resid_in
+    )
+
+    far = n_tp // 2
+    order = list(range(far + 1)) + list(range(n_tp - 1, far, -1))
+    blocks = {0: normed, n_tp: normed}
+    for k in order:
+        if k:
+            by = 1 if k <= far else -1
+            blocks[k] = rotated(blocks[k - by], "tp", by)
+
+    slot, by_row, weight = slots(
+        place, [chunks[k] for k in order], n_sp, local_experts, TOP, tok_rows
+    )
+    weights = load(w_gate, w_up, w_down)
+    arrived, backs, parts = [], {}, {}
+    for at, k in enumerate(order):
+        rows = pick(at, slot, blocks[k], n_sp, slot_rows)
+        arrived.append([moved(x, "sp", d) if d else x for d, x in enumerate(rows)])
+    for first, stop in groups_of(n_tp):
+        group = arrived[first:stop]
+        terms = experts([x for xs in group for x in xs], *weights)
+        for at in range(first, stop):
+            back = terms[(at - first) * n_sp : (at - first + 1) * n_sp]
+            backs[at] = [moved(x, "sp", d, True) if d else x for d, x in enumerate(back)]
+    for at in return_order(n_tp)[:-1]:
+        k = order[at]
+        by = -1 if k <= far else 1
+        inner = k < far or k > far + 1
+        joined = [parts.pop(k - by)] if inner else []
+        part = combine(at, by_row, weight, backs[at], joined)
+        parts[k] = rotated(part, "tp", by)
+    return finish(0, by_row, weight, residual, post_gain, backs[0], list(parts.values()))
+
+
+def per_device(*args):
+    pool_input, w_gate, routes = args[1], args[7], args[10]
+    n_sp = lax.axis_size("sp")
+    fits = w_gate.shape[0] % 8 == 0 and CAP % 8 and n_sp <= 4 and w_gate.shape[0] * n_sp <= 256
+    fits = fits and routes.shape[0] == LANES and pool_input.shape[1] % LANES == 0
+    return kernel_path(*args) if fits else plain_path(*args)
 
 
 def groups_of(n_tp):

time: 181 us -> 173 us (0.956)
  waiting for transfers between devices: 106 us -> 91.7 us
  starting transfers between devices: 29.2 us -> 35.6 us
  other arithmetic: 6.25 us -> 0.07 us
  Pallas kernels: 31.2 us -> 36 us
  local copies, waits for them, and re-layouts: 4.07 us -> 8.87 us
  matrix products: 3.39 us -> 0 us
    ppermute x6 -> x9, starting transfers between devices: 4.52 us -> 16.7 us  [rotated(): return lax.ppermute(x, axis, [(i, (i + by) % size) for i in range(size)])]
    all_to_all x1 -> x0, waiting for transfers between devices: 10 us -> none  [per_device(): got = lax.all_to_all(sent, 'tp', split_axis=0, concat_axis=0, tiled=True)]
    unnamed x16 -> x18, local copies, waits for them, and re-layouts: 0.05 us -> 8.87 us
    ppermute x24, waiting for transfers between devices: 64.9 us -> 57 us  [moved(): return lax.ppermute(x, axis, [(b, a) for a, b in pairs] if back else pairs)]
    all_to_all x1 -> x0, starting transfers between devices: 5.69 us -> none  [per_device(): got = lax.all_to_all(sent, 'tp', split_axis=0, concat_axis=0, tiled=True)]
    ppermute x6 -> x9, waiting for transfers between devices: 30.8 us -> 34.6 us  [rotated(): return lax.ppermute(x, axis, [(i, (i + by) % size) for i in range(size)])]
    pallas_call x0 -> x3, Pallas kernels: none -> 3.66 us  [the longest x1 2 us: mix_tokens(): pl.pallas_call(lambda *refs: mix_body(len(chunks), *refs), in_specs=[IN_S...]
    dot_general x3 -> x0, matrix products: 3.39 us -> none  [the longest x1 3.01 us: per_device(): mix_out = jnp.dot(pooled, out_weight, preferred_element_type=jnp.float32)]
  transfers between devices with their start and end apart: 32 -> 37, of which waited for: 15 -> 18; matrix products, arithmetic and copies ran while one was open for 3% -> 0% of each run, Pallas kernels for 16% -> 18%
where the time goes in v3:
time: 173 us
  waiting for transfers between devices  91.7 us (53%)
  Pallas kernels  36 us (21%)
  starting transfers between devices  35.6 us (21%)
  local copies, waits for them, and re-layouts  8.87 us (5%)
    ppermute x24, waiting for transfers between devices, moved(): return lax.ppermute(x, axis, [(b, a) for a, b in pairs] if back else pairs)  57 us
    ppermute x9, waiting for transfers between devices, rotated(): return lax.ppermute(x, axis, [(i, (i + by) % size) for i in range(size)])  34.6 us
    pallas_call x3, Pallas kernels, experts(): pl.pallas_call(lambda *refs: experts_body(n_src, *refs), in_specs=[IN_VME...  16.7 us
    ppermute x9, starting transfers between devices, rotated(): return lax.ppermute(x, axis, [(i, (i + by) % size) for i in range(size)])  16.7 us
    ppermute x24, starting transfers between devices, moved(): return lax.ppermute(x, axis, [(b, a) for a, b in pairs] if back else pairs)  15.6 us
    pallas_call x2, Pallas kernels, load(): pl.pallas_call(load_body, in_specs=[pl.BlockSpec(memory_space=pltpu.HBM)]...  9.47 us
    unnamed x18, local copies, waits for them, and re-layouts  8.87 us
  transfers between devices with their start and end apart: 37, of which 18 were waited for; matrix products, arithmetic and copies ran while one was open for 0% of the time, Pallas kernels for 18%

profile of v3, /device:TPU:0, one launch (start us, length us, event | category | flops | bytes accessed | tf_op | source)
XLA Modules:
  0.0 172.6 jit_solution(14498132310542416357)
XLA Ops:
  3.3 3.1 %collective-permute-start = (bf16[152,256]{1,0:T(8,128)(2,1)S(1)}, bf16[152,256]{1,0:T(8,128)(2,1)S(1)}, u32[]{:S(2)}, u32[]{:S(2)}) collective-permute-start(bf16[152,256]{1,0:T(8,128)(2,1)S(1)} %get-tuple-element.57), channel_id=1, source_target_pairs={{0,1},{1,2},{2,3},{3,0},{4,5},{5,6},{6,7},{7,4},{8,9},{9,10},{10,1... | collective-permute-start | bytes 233480 | tf_op jit(solution)/shard_map/ppermute | solution.py:30
  6.4 2.6 %collective-permute-start.1 = (bf16[152,256]{1,0:T(8,128)(2,1)S(1)}, bf16[152,256]{1,0:T(8,128)(2,1)S(1)}, u32[]{:S(2)}, u32[]{:S(2)}) collective-permute-start(bf16[152,256]{1,0:T(8,128)(2,1)S(1)} %get-tuple-element.58), channel_id=1, source_target_pairs={{0,2},{1,3},{2,0},{3,1},{4,6},{5,7},{6,4},{7,5},{8,10},{9,11},{10,... | collective-permute-start | bytes 233480 | tf_op jit(solution)/shard_map/ppermute | solution.py:30
  8.9 1.3 collective-permute-start.2
  10.3 1.3 collective-permute-start.3
  13.7 2.2 %copy-done = bf16[1024,2048]{1,0:T(8,128)(2,1)S(1)} copy-done((bf16[1024,2048]{1,0:T(8,128)(2,1)S(1)}, bf16[1024,2048]{1,0:T(8,128)(2,1)}, u32[]{:S(2)}) %copy-start) | copy-done | bytes 4194328
  21.2 2.0 %mix.1 = (bf16[128,2048]{1,0:T(8,128)(2,1)S(1)}, bf16[128,2048]{1,0:T(8,128)(2,1)S(1)}) custom-call(s32[2]{0:T(128)S(1)} %pad_add_fusion.place.refs_0_, bf16[152,256]{1,0:T(8,128)(2,1)S(1)} %get-tuple-element.56.refs_1_, bf16[152,256]{1,0:T(8,128)(2,1)S(1)} %collective-permute-done.refs_2_, bf16[152,256]{1,0:T(8,128)(2,1)S(1)} %collective-permute-done.1.refs_3_, ...), custom_call_target="tpu_custom_call" | custom-call | tf_op jit(solution)/shard_map/mix/pallas_call | solution.py:474
  23.2 5.7 %collective-permute-start.10 = (bf16[128,2048]{1,0:T(8,128)(2,1)S(1)}, bf16[128,2048]{1,0:T(8,128)(2,1)S(1)}, u32[]{:S(2)}, u32[]{:S(2)}) collective-permute-start(bf16[128,2048]{1,0:T(8,128)(2,1)S(1)} %get-tuple-element.71.refs_1_), channel_id=1, source_target_pairs={{0,1},{1,2},{2,3},{3,0},{4,5},{5,6},{6,7},{7,4},{8,9},{9,10},{10,1... | collective-permute-start | bytes 1572872 | tf_op jit(solution)/shard_map/ppermute | solution.py:30
  28.9 17.5 %collective-permute-done.10.refs_1_ = bf16[128,2048]{1,0:T(8,128)(2,1)S(1)} collective-permute-done((bf16[128,2048]{1,0:T(8,128)(2,1)S(1)}, bf16[128,2048]{1,0:T(8,128)(2,1)S(1)}, u32[]{:S(2)}, u32[]{:S(2)}) %collective-permute-start.10) | collective-permute-done | bytes 524320 | tf_op jit(solution)/shard_map/ppermute | solution.py:30
  46.4 3.8 %collective-permute-start.17 = (bf16[128,2048]{1,0:T(8,128)(2,1)S(1)}, bf16[128,2048]{1,0:T(8,128)(2,1)S(1)}, u32[]{:S(2)}, u32[]{:S(2)}) collective-permute-start(bf16[128,2048]{1,0:T(8,128)(2,1)S(1)} %get-tuple-element.71.refs_1_), channel_id=1, source_target_pairs={{0,3},{1,0},{2,1},{3,2},{4,7},{5,4},{6,5},{7,6},{8,11},{9,8},{10,9... | collective-permute-start | bytes 1572872 | tf_op jit(solution)/shard_map/ppermute | solution.py:30
  51.2 11.8 %collective-permute-done.28.refs_1_ = bf16[128,2048]{1,0:T(8,128)(2,1)S(1)} collective-permute-done((bf16[128,2048]{1,0:T(8,128)(2,1)S(1)}, bf16[128,2048]{1,0:T(8,128)(2,1)S(1)}, u32[]{:S(2)}, u32[]{:S(2)}) %collective-permute-start.28) | collective-permute-done | bytes 524320 | tf_op jit(solution)/shard_map/ppermute | solution.py:30
  63.7 1.8 %collective-permute-start.31 = (bf16[72,2048]{1,0:T(8,128)(2,1)S(1)}, bf16[72,2048]{1,0:T(8,128)(2,1)S(1)}, u32[]{:S(2)}, u32[]{:S(2)}) collective-permute-start(bf16[72,2048]{1,0:T(8,128)(2,1)S(1)} %get-tuple-element.102), channel_id=1, source_target_pairs={{0,12},{4,8},{8,4},{12,0},{1,13},{5,9},{9,5},{13,1},{2,14},{6,10},... | collective-permute-start | bytes 884744 | tf_op jit(solution)/shard_map/ppermute | solution.py:76
  66.4 5.2 %collective-permute-done.17.refs_1_ = bf16[128,2048]{1,0:T(8,128)(2,1)S(1)} collective-permute-done((bf16[128,2048]{1,0:T(8,128)(2,1)S(1)}, bf16[128,2048]{1,0:T(8,128)(2,1)S(1)}, u32[]{:S(2)}, u32[]{:S(2)}) %collective-permute-start.17) | collective-permute-done | bytes 524320 | tf_op jit(solution)/shard_map/ppermute | solution.py:30
  74.3 8.4 %load.3 = (bf16[8,2048,256]{2,1,0:T(8,128)(2,1)S(1)}, bf16[8,2048,256]{2,1,0:T(8,128)(2,1)S(1)}, bf16[8,256,2048]{2,1,0:T(8,128)(2,1)S(1)}) custom-call(bf16[8,2048,256]{2,1,0:T(8,128)(2,1)} %refs_0_.1, bf16[8,2048,256]{2,1,0:T(8,128)(2,1)} %refs_1_.1, bf16[8,256,2048]{2,1,0:T(8,128)(2,1)} %refs_2_.1), custom_call_target="tpu_custom_call" | custom-call | tf_op jit(solution)/shard_map/load/pallas_call | solution.py:104
  82.8 5.5 %experts.5 = (bf16[72,2048]{1,0:T(8,128)(2,1)S(1)}, bf16[72,2048]{1,0:T(8,128)(2,1)S(1)}, bf16[72,2048]{1,0:T(8,128)(2,1)S(1)}, bf16[72,2048]{1,0:T(8,128)(2,1)S(1)}) custom-call(bf16[72,2048]{1,0:T(8,128)(2,1)S(1)} %get-tuple-element.99.refs_0_, bf16[72,2048]{1,0:T(8,128)(2,1)S(1)} %collective-permute-done.29.refs_1_, ...), custom_call_target="tpu_custom_call" | custom-call | flops 905969664 | bytes 27525120 | tf_op jit(solution)/shard_map/experts/pallas_call | solution.py:263
  88.3 1.4 collective-permute-start.20
  92.1 1.6 collective-permute-start.34
  94.2 4.7 %collective-permute-done.19.refs_2_ = bf16[72,2048]{1,0:T(8,128)(2,1)S(1)} collective-permute-done((bf16[72,2048]{1,0:T(8,128)(2,1)S(1)}, bf16[72,2048]{1,0:T(8,128)(2,1)S(1)}, u32[]{:S(2)}, u32[]{:S(2)}) %collective-permute-start.19) | collective-permute-done | bytes 294944 | tf_op jit(solution)/shard_map/ppermute | solution.py:76
  98.8 5.2 %collective-permute-done.20.refs_3_ = bf16[72,2048]{1,0:T(8,128)(2,1)S(1)} collective-permute-done((bf16[72,2048]{1,0:T(8,128)(2,1)S(1)}, bf16[72,2048]{1,0:T(8,128)(2,1)S(1)}, u32[]{:S(2)}, u32[]{:S(2)}) %collective-permute-start.20) | collective-permute-done | bytes 294944 | tf_op jit(solution)/shard_map/ppermute | solution.py:76
  104.7 1.6 collective-permute-start.13
  106.3 5.5 %experts.4 = (bf16[72,2048]{1,0:T(8,128)(2,1)S(1)}, bf16[72,2048]{1,0:T(8,128)(2,1)S(1)}, bf16[72,2048]{1,0:T(8,128)(2,1)S(1)}, bf16[72,2048]{1,0:T(8,128)(2,1)S(1)}) custom-call(bf16[72,2048]{1,0:T(8,128)(2,1)S(1)} %get-tuple-element.87.refs_0_, bf16[72,2048]{1,0:T(8,128)(2,1)S(1)} %collective-permute-done.18.refs_1_, ...), custom_call_target="tpu_custom_call" | custom-call | flops 905969664 | bytes 27525120 | tf_op jit(solution)/shard_map/experts/pallas_call | solution.py:263
  112.0 4.8 %collective-permute-done.34.refs_5_ = bf16[72,2048]{1,0:T(8,128)(2,1)S(1)} collective-permute-done((bf16[72,2048]{1,0:T(8,128)(2,1)S(1)}, bf16[72,2048]{1,0:T(8,128)(2,1)S(1)}, u32[]{:S(2)}, u32[]{:S(2)}) %collective-permute-start.34) | collective-permute-done | bytes 294944 | tf_op jit(solution)/shard_map/ppermute | solution.py:76
  118.2 5.9 %collective-permute-done.12.refs_6_ = bf16[72,2048]{1,0:T(8,128)(2,1)S(1)} collective-permute-done((bf16[72,2048]{1,0:T(8,128)(2,1)S(1)}, bf16[72,2048]{1,0:T(8,128)(2,1)S(1)}, u32[]{:S(2)}, u32[]{:S(2)}) %collective-permute-start.12) | collective-permute-done | bytes 294944 | tf_op jit(solution)/shard_map/ppermute | solution.py:76
  124.1 5.2 %collective-permute-done.13.refs_7_ = bf16[72,2048]{1,0:T(8,128)(2,1)S(1)} collective-permute-done((bf16[72,2048]{1,0:T(8,128)(2,1)S(1)}, bf16[72,2048]{1,0:T(8,128)(2,1)S(1)}, u32[]{:S(2)}, u32[]{:S(2)}) %collective-permute-start.13) | collective-permute-done | bytes 294944 | tf_op jit(solution)/shard_map/ppermute | solution.py:76
  129.4 5.7 %experts.3 = (bf16[72,2048]{1,0:T(8,128)(2,1)S(1)}, bf16[72,2048]{1,0:T(8,128)(2,1)S(1)}, bf16[72,2048]{1,0:T(8,128)(2,1)S(1)}, bf16[72,2048]{1,0:T(8,128)(2,1)S...) custom-call(bf16[72,2048]{1,0:T(8,128)(2,1)S(1)} %get-tuple-element., ...), custom_call_target="tpu_custom_call" | custom-call | flops 1811939328 | bytes 29884416 | tf_op jit(solution)/shard_map/experts/pallas_call | solution.py:263
  135.1 1.3 collective-permute-start.25
  137.8 4.2 %collective-permute-done.23.refs_5_ = bf16[72,2048]{1,0:T(8,128)(2,1)S(1)} collective-permute-done((bf16[72,2048]{1,0:T(8,128)(2,1)S(1)}, bf16[72,2048]{1,0:T(8,128)(2,1)S(1)}, u32[]{:S(2)}, u32[]{:S(2)}) %collective-permute-start.23) | collective-permute-done | bytes 294944 | tf_op jit(solution)/shard_map/ppermute | solution.py:76
  142.9 6.5 %collective-permute-done.26.refs_4_ = bf16[72,2048]{1,0:T(8,128)(2,1)S(1)} collective-permute-done((bf16[72,2048]{1,0:T(8,128)(2,1)S(1)}, bf16[72,2048]{1,0:T(8,128)(2,1)S(1)}, u32[]{:S(2)}, u32[]{:S(2)}) %collective-permute-start.26) | collective-permute-done | bytes 294944 | tf_op jit(solution)/shard_map/ppermute | solution.py:76
  149.4 5.2 %collective-permute-done.27.refs_5_ = bf16[72,2048]{1,0:T(8,128)(2,1)S(1)} collective-permute-done((bf16[72,2048]{1,0:T(8,128)(2,1)S(1)}, bf16[72,2048]{1,0:T(8,128)(2,1)S(1)}, u32[]{:S(2)}, u32[]{:S(2)}) %collective-permute-start.27) | collective-permute-done | bytes 294944 | tf_op jit(solution)/shard_map/ppermute | solution.py:76
  156.5 1.1 collective-permute-start.16
  157.7 8.4 %collective-permute-done.15.refs_6_ = bf16[72,2048]{1,0:T(8,128)(2,1)S(1)} collective-permute-done((bf16[72,2048]{1,0:T(8,128)(2,1)S(1)}, bf16[72,2048]{1,0:T(8,128)(2,1)S(1)}, u32[]{:S(2)}, u32[]{:S(2)}) %collective-permute-start.15) | collective-permute-done | bytes 294944 | tf_op jit(solution)/shard_map/ppermute | solution.py:76
  166.1 4.5 %collective-permute-done.16.refs_7_ = bf16[72,2048]{1,0:T(8,128)(2,1)S(1)} collective-permute-done((bf16[72,2048]{1,0:T(8,128)(2,1)S(1)}, bf16[72,2048]{1,0:T(8,128)(2,1)S(1)}, u32[]{:S(2)}, u32[]{:S(2)}) %collective-permute-start.16) | collective-permute-done | bytes 294944 | tf_op jit(solution)/shard_map/ppermute | solution.py:76
  170.7 1.8 %finish.1 = bf16[128,2048]{1,0:T(8,128)(2,1)} custom-call(s32[4,128,2]{2,1,0:T(8,128)S(1)} %get-tuple-element.60.refs_0_, f32[4,128,2]{2,1,0:T(8,128)S(1)} %get-tuple-element.61.refs_1_, bf16[128,2048]{1,0:T(8,128)(2,1)S(1)} %get-tuple-element.69.refs_2_, f32[1,2048]{1,0:T(1,128)S(1)} %bitcast.8, bf16[72,2048]{1,0:T(8,128)(2,1)S(1)} %get-tuple-element.83.refs_4_, ...), custom_call_target="tpu_custom_call" | custom-call | tf_op jit(solution)/shard_map/finish/pallas_call | solution.py:201
  (77 shorter events, 25.1 us)
Async XLA Ops:
  3.3 17.9 %collective-permute-start = (bf16[152,256]{1,0:T(8,128)(2,1)S(1)}, bf16[152,256]{1,0:T(8,128)(2,1)S(1)}, u32[]{:S(2)}, u32[]{:S(2)}) collective-permute-start(bf16[152,256]{1,0:T(8,128)(2,1)S(1)} %get-tuple-element.57), channel_id=1, source_target_pairs={{0,1},{1,2},{2,3},{3,0},{4,5},{5,6},{6,7},{7,4},{8,9},{9,10},{10,1... | collective-permute-start | bytes 233480 | tf_op jit(solution)/shard_map/ppermute | solution.py:30
  6.4 14.9 %collective-permute-start.1 = (bf16[152,256]{1,0:T(8,128)(2,1)S(1)}, bf16[152,256]{1,0:T(8,128)(2,1)S(1)}, u32[]{:S(2)}, u32[]{:S(2)}) collective-permute-start(bf16[152,256]{1,0:T(8,128)(2,1)S(1)} %get-tuple-element.58), channel_id=1, source_target_pairs={{0,2},{1,3},{2,0},{3,1},{4,6},{5,7},{6,4},{7,5},{8,10},{9,11},{10,... | collective-permute-start | bytes 233480 | tf_op jit(solution)/shard_map/ppermute | solution.py:30
  8.9 12.3 %collective-permute-start.2 = (bf16[152,256]{1,0:T(8,128)(2,1)S(1)}, bf16[152,256]{1,0:T(8,128)(2,1)S(1)}, u32[]{:S(2)}, u32[]{:S(2)}) collective-permute-start(bf16[152,256]{1,0:T(8,128)(2,1)S(1)} %get-tuple-element.59), channel_id=1, source_target_pairs={{0,3},{1,0},{2,1},{3,2},{4,7},{5,4},{6,5},{7,6},{8,11},{9,8},{10,9... | collective-permute-start | bytes 233480 | tf_op jit(solution)/shard_map/ppermute | solution.py:30
  12.4 8.8 %collective-permute-start.5 = (bf16[16,256]{1,0:T(8,128)(2,1)S(1)}, bf16[16,256]{1,0:T(8,128)(2,1)S(1)}, u32[]{:S(2)}, u32[]{:S(2)}) collective-permute-start(bf16[16,256]{1,0:T(8,128)(2,1)S(1)} %get-tuple-element.62), channel_id=1, source_target_pairs={{2,4},{6,8},{10,12},{18,20},{22,24},{26,28}} | collective-permute-start | bytes 24584 | tf_op jit(solution)/shard_map/ppermute | solution.py:578
  23.2 23.2 %collective-permute-start.10 = (bf16[128,2048]{1,0:T(8,128)(2,1)S(1)}, bf16[128,2048]{1,0:T(8,128)(2,1)S(1)}, u32[]{:S(2)}, u32[]{:S(2)}) collective-permute-start(bf16[128,2048]{1,0:T(8,128)(2,1)S(1)} %get-tuple-element.71.refs_1_), channel_id=1, source_target_pairs={{0,1},{1,2},{2,3},{3,0},{4,5},{5,6},{6,7},{7,4},{8,9},{9,10},{10,1... | collective-permute-start | bytes 1572872 | tf_op jit(solution)/shard_map/ppermute | solution.py:30
  46.4 16.6 %collective-permute-start.28 = (bf16[128,2048]{1,0:T(8,128)(2,1)S(1)}, bf16[128,2048]{1,0:T(8,128)(2,1)S(1)}, u32[]{:S(2)}, u32[]{:S(2)}) collective-permute-start(bf16[128,2048]{1,0:T(8,128)(2,1)S(1)} %collective-permute-done.10.refs_1_), channel_id=1, source_target_pairs={{0,1},{1,2},{2,3},{3,0},{4,5},{5,6},{6,7},{7,4},{8,9},{9,10},{10,1... | collective-permute-start | bytes 1572872 | tf_op jit(solution)/shard_map/ppermute | solution.py:30
  46.4 25.2 %collective-permute-start.17 = (bf16[128,2048]{1,0:T(8,128)(2,1)S(1)}, bf16[128,2048]{1,0:T(8,128)(2,1)S(1)}, u32[]{:S(2)}, u32[]{:S(2)}) collective-permute-start(bf16[128,2048]{1,0:T(8,128)(2,1)S(1)} %get-tuple-element.71.refs_1_), channel_id=1, source_target_pairs={{0,3},{1,0},{2,1},{3,2},{4,7},{5,4},{6,5},{7,6},{8,11},{9,8},{10,9... | collective-permute-start | bytes 1572872 | tf_op jit(solution)/shard_map/ppermute | solution.py:30
  63.5 8.6 %collective-permute-start.29 = (bf16[72,2048]{1,0:T(8,128)(2,1)S(1)}, bf16[72,2048]{1,0:T(8,128)(2,1)S(1)}, u32[]{:S(2)}, u32[]{:S(2)}) collective-permute-start(bf16[72,2048]{1,0:T(8,128)(2,1)S(1)} %get-tuple-element.100), channel_id=1, source_target_pairs={{0,4},{4,0},{8,12},{12,8},{1,5},{5,1},{9,13},{13,9},{2,6},{6,2},{1... | collective-permute-start | bytes 884744 | tf_op jit(solution)/shard_map/ppermute | solution.py:76
  63.6 9.9 %collective-permute-start.30 = (bf16[72,2048]{1,0:T(8,128)(2,1)S(1)}, bf16[72,2048]{1,0:T(8,128)(2,1)S(1)}, u32[]{:S(2)}, u32[]{:S(2)}) collective-permute-start(bf16[72,2048]{1,0:T(8,128)(2,1)S(1)} %get-tuple-element.101), channel_id=1, source_target_pairs={{0,8},{4,12},{8,0},{12,4},{1,9},{5,13},{9,1},{13,5},{2,10},{6,14},... | collective-permute-start | bytes 884744 | tf_op jit(solution)/shard_map/ppermute | solution.py:76
  63.7 19.0 %collective-permute-start.31 = (bf16[72,2048]{1,0:T(8,128)(2,1)S(1)}, bf16[72,2048]{1,0:T(8,128)(2,1)S(1)}, u32[]{:S(2)}, u32[]{:S(2)}) collective-permute-start(bf16[72,2048]{1,0:T(8,128)(2,1)S(1)} %get-tuple-element.102), channel_id=1, source_target_pairs={{0,12},{4,8},{8,4},{12,0},{1,13},{5,9},{9,5},{13,1},{2,14},{6,10},... | collective-permute-start | bytes 884744 | tf_op jit(solution)/shard_map/ppermute | solution.py:76
  65.9 22.4 %collective-permute-start.7 = (bf16[72,2048]{1,0:T(8,128)(2,1)S(1)}, bf16[72,2048]{1,0:T(8,128)(2,1)S(1)}, u32[]{:S(2)}, u32[]{:S(2)}) collective-permute-start(bf16[72,2048]{1,0:T(8,128)(2,1)S(1)} %get-tuple-element.73), channel_id=1, source_target_pairs={{0,4},{4,0},{8,12},{12,8},{1,5},{5,1},{9,13},{13,9},{2,6},{6,2},{1... | collective-permute-start | bytes 884744 | tf_op jit(solution)/shard_map/ppermute | solution.py:76
  71.6 18.1 %collective-permute-start.8 = (bf16[72,2048]{1,0:T(8,128)(2,1)S(1)}, bf16[72,2048]{1,0:T(8,128)(2,1)S(1)}, u32[]{:S(2)}, u32[]{:S(2)}) collective-permute-start(bf16[72,2048]{1,0:T(8,128)(2,1)S(1)} %get-tuple-element.74), channel_id=1, source_target_pairs={{0,8},{4,12},{8,0},{12,4},{1,9},{5,13},{9,1},{13,5},{2,10},{6,14},... | collective-permute-start | bytes 884744 | tf_op jit(solution)/shard_map/ppermute | solution.py:76
  72.1 19.3 %collective-permute-start.9 = (bf16[72,2048]{1,0:T(8,128)(2,1)S(1)}, bf16[72,2048]{1,0:T(8,128)(2,1)S(1)}, u32[]{:S(2)}, u32[]{:S(2)}) collective-permute-start(bf16[72,2048]{1,0:T(8,128)(2,1)S(1)} %get-tuple-element.75), channel_id=1, source_target_pairs={{0,12},{4,8},{8,4},{12,0},{1,13},{5,9},{9,5},{13,1},{2,14},{6,10},... | collective-permute-start | bytes 884744 | tf_op jit(solution)/shard_map/ppermute | solution.py:76
  73.6 18.5 %collective-permute-start.18 = (bf16[72,2048]{1,0:T(8,128)(2,1)S(1)}, bf16[72,2048]{1,0:T(8,128)(2,1)S(1)}, u32[]{:S(2)}, u32[]{:S(2)}) collective-permute-start(bf16[72,2048]{1,0:T(8,128)(2,1)S(1)} %get-tuple-element.88), channel_id=1, source_target_pairs={{0,4},{4,0},{8,12},{12,8},{1,5},{5,1},{9,13},{13,9},{2,6},{6,2},{1... | collective-permute-start | bytes 884744 | tf_op jit(solution)/shard_map/ppermute | solution.py:76
  82.7 16.1 %collective-permute-start.19 = (bf16[72,2048]{1,0:T(8,128)(2,1)S(1)}, bf16[72,2048]{1,0:T(8,128)(2,1)S(1)}, u32[]{:S(2)}, u32[]{:S(2)}) collective-permute-start(bf16[72,2048]{1,0:T(8,128)(2,1)S(1)} %get-tuple-element.89), channel_id=1, source_target_pairs={{0,8},{4,12},{8,0},{12,4},{1,9},{5,13},{9,1},{13,5},{2,10},{6,14},... | collective-permute-start | bytes 884744 | tf_op jit(solution)/shard_map/ppermute | solution.py:76
  88.3 15.8 %collective-permute-start.20 = (bf16[72,2048]{1,0:T(8,128)(2,1)S(1)}, bf16[72,2048]{1,0:T(8,128)(2,1)S(1)}, u32[]{:S(2)}, u32[]{:S(2)}) collective-permute-start(bf16[72,2048]{1,0:T(8,128)(2,1)S(1)} %get-tuple-element.90), channel_id=1, source_target_pairs={{0,12},{4,8},{8,4},{12,0},{1,13},{5,9},{9,5},{13,1},{2,14},{6,10},... | collective-permute-start | bytes 884744 | tf_op jit(solution)/shard_map/ppermute | solution.py:76
  89.7 15.0 %collective-permute-start.32 = (bf16[72,2048]{1,0:T(8,128)(2,1)S(1)}, bf16[72,2048]{1,0:T(8,128)(2,1)S(1)}, u32[]{:S(2)}, u32[]{:S(2)}) collective-permute-start(bf16[72,2048]{1,0:T(8,128)(2,1)S(1)} %get-tuple-element.104), channel_id=1, source_target_pairs={{4,0},{0,4},{12,8},{8,12},{5,1},{1,5},{13,9},{9,13},{6,2},{2,6},{1... | collective-permute-start | bytes 884744 | tf_op jit(solution)/shard_map/ppermute | solution.py:76
  91.4 20.4 %collective-permute-start.33 = (bf16[72,2048]{1,0:T(8,128)(2,1)S(1)}, bf16[72,2048]{1,0:T(8,128)(2,1)S(1)}, u32[]{:S(2)}, u32[]{:S(2)}) collective-permute-start(bf16[72,2048]{1,0:T(8,128)(2,1)S(1)} %get-tuple-element.105), channel_id=1, source_target_pairs={{8,0},{12,4},{0,8},{4,12},{9,1},{13,5},{1,9},{5,13},{10,2},{14,6},... | collective-permute-start | bytes 884744 | tf_op jit(solution)/shard_map/ppermute | solution.py:76
  92.1 24.6 %collective-permute-start.34 = (bf16[72,2048]{1,0:T(8,128)(2,1)S(1)}, bf16[72,2048]{1,0:T(8,128)(2,1)S(1)}, u32[]{:S(2)}, u32[]{:S(2)}) collective-permute-start(bf16[72,2048]{1,0:T(8,128)(2,1)S(1)} %get-tuple-element.106), channel_id=1, source_target_pairs={{12,0},{8,4},{4,8},{0,12},{13,1},{9,5},{5,9},{1,13},{14,2},{10,6},... | collective-permute-start | bytes 884744 | tf_op jit(solution)/shard_map/ppermute | solution.py:76
  98.8 19.3 %collective-permute-start.11 = (bf16[72,2048]{1,0:T(8,128)(2,1)S(1)}, bf16[72,2048]{1,0:T(8,128)(2,1)S(1)}, u32[]{:S(2)}, u32[]{:S(2)}) collective-permute-start(bf16[72,2048]{1,0:T(8,128)(2,1)S(1)} %get-tuple-element.77), channel_id=1, source_target_pairs={{0,4},{4,0},{8,12},{12,8},{1,5},{5,1},{9,13},{13,9},{2,6},{6,2},{1... | collective-permute-start | bytes 884744 | tf_op jit(solution)/shard_map/ppermute | solution.py:76
  104.1 20.0 %collective-permute-start.12 = (bf16[72,2048]{1,0:T(8,128)(2,1)S(1)}, bf16[72,2048]{1,0:T(8,128)(2,1)S(1)}, u32[]{:S(2)}, u32[]{:S(2)}) collective-permute-start(bf16[72,2048]{1,0:T(8,128)(2,1)S(1)} %get-tuple-element.78), channel_id=1, source_target_pairs={{0,8},{4,12},{8,0},{12,4},{1,9},{5,13},{9,1},{13,5},{2,10},{6,14},... | collective-permute-start | bytes 884744 | tf_op jit(solution)/shard_map/ppermute | solution.py:76
  104.7 24.6 %collective-permute-start.13 = (bf16[72,2048]{1,0:T(8,128)(2,1)S(1)}, bf16[72,2048]{1,0:T(8,128)(2,1)S(1)}, u32[]{:S(2)}, u32[]{:S(2)}) collective-permute-start(bf16[72,2048]{1,0:T(8,128)(2,1)S(1)} %get-tuple-element.79), channel_id=1, source_target_pairs={{0,12},{4,8},{8,4},{12,0},{1,13},{5,9},{9,5},{13,1},{2,14},{6,10},... | collective-permute-start | bytes 884744 | tf_op jit(solution)/shard_map/ppermute | solution.py:76
  111.9 24.4 %collective-permute-start.21 = (bf16[72,2048]{1,0:T(8,128)(2,1)S(1)}, bf16[72,2048]{1,0:T(8,128)(2,1)S(1)}, u32[]{:S(2)}, u32[]{:S(2)}) collective-permute-start(bf16[72,2048]{1,0:T(8,128)(2,1)S(1)} %get-tuple-element.92), channel_id=1, source_target_pairs={{4,0},{0,4},{12,8},{8,12},{5,1},{1,5},{13,9},{9,13},{6,2},{2,6},{1... | collective-permute-start | bytes 884744 | tf_op jit(solution)/shard_map/ppermute | solution.py:76
  116.7 20.0 %collective-permute-start.22 = (bf16[72,2048]{1,0:T(8,128)(2,1)S(1)}, bf16[72,2048]{1,0:T(8,128)(2,1)S(1)}, u32[]{:S(2)}, u32[]{:S(2)}) collective-permute-start(bf16[72,2048]{1,0:T(8,128)(2,1)S(1)} %get-tuple-element.93), channel_id=1, source_target_pairs={{8,0},{12,4},{0,8},{4,12},{9,1},{13,5},{1,9},{5,13},{10,2},{14,6},... | collective-permute-start | bytes 884744 | tf_op jit(solution)/shard_map/ppermute | solution.py:76
  118.2 36.5 %collective-permute-start.35 = (bf16[128,2048]{1,0:T(8,128)(2,1)S(1)}, bf16[128,2048]{1,0:T(8,128)(2,1)S(1)}, u32[]{:S(2)}, u32[]{:S(2)}) collective-permute-start(bf16[128,2048]{1,0:T(8,128)(2,1)S(1)} %combine.4), channel_id=1, source_target_pairs={{0,3},{1,0},{2,1},{3,2},{4,7},{5,4},{6,5},{7,6},{8,11},{9,8},{10,9... | collective-permute-start | bytes 1572872 | tf_op jit(solution)/shard_map/ppermute | solution.py:30
  124.1 17.9 %collective-permute-start.23 = (bf16[72,2048]{1,0:T(8,128)(2,1)S(1)}, bf16[72,2048]{1,0:T(8,128)(2,1)S(1)}, u32[]{:S(2)}, u32[]{:S(2)}) collective-permute-start(bf16[72,2048]{1,0:T(8,128)(2,1)S(1)} %get-tuple-element.94), channel_id=1, source_target_pairs={{12,0},{8,4},{4,8},{0,12},{13,1},{9,5},{5,9},{1,13},{14,2},{10,6},... | collective-permute-start | bytes 884744 | tf_op jit(solution)/shard_map/ppermute | solution.py:76
  136.3 13.1 %collective-permute-start.26 = (bf16[72,2048]{1,0:T(8,128)(2,1)S(1)}, bf16[72,2048]{1,0:T(8,128)(2,1)S(1)}, u32[]{:S(2)}, u32[]{:S(2)}) collective-permute-start(bf16[72,2048]{1,0:T(8,128)(2,1)S(1)} %get-tuple-element.97), channel_id=1, source_target_pairs={{8,0},{12,4},{0,8},{4,12},{9,1},{13,5},{1,9},{5,13},{10,2},{14,6},... | collective-permute-start | bytes 884744 | tf_op jit(solution)/shard_map/ppermute | solution.py:76
  136.8 17.9 %collective-permute-start.27 = (bf16[72,2048]{1,0:T(8,128)(2,1)S(1)}, bf16[72,2048]{1,0:T(8,128)(2,1)S(1)}, u32[]{:S(2)}, u32[]{:S(2)}) collective-permute-start(bf16[72,2048]{1,0:T(8,128)(2,1)S(1)} %get-tuple-element.98), channel_id=1, source_target_pairs={{12,0},{8,4},{4,8},{0,12},{13,1},{9,5},{5,9},{1,13},{14,2},{10,6},... | collective-permute-start | bytes 884744 | tf_op jit(solution)/shard_map/ppermute | solution.py:76
  142.8 27.9 %collective-permute-start.24 = (bf16[128,2048]{1,0:T(8,128)(2,1)S(1)}, bf16[128,2048]{1,0:T(8,128)(2,1)S(1)}, u32[]{:S(2)}, u32[]{:S(2)}) collective-permute-start(bf16[128,2048]{1,0:T(8,128)(2,1)S(1)} %combine.3), channel_id=1, source_target_pairs={{0,1},{1,2},{2,3},{3,0},{4,5},{5,6},{6,7},{7,4},{8,9},{9,10},{10,1... | collective-permute-start | bytes 1572872 | tf_op jit(solution)/shard_map/ppermute | solution.py:30
  155.4 15.3 %collective-permute-start.36 = (bf16[128,2048]{1,0:T(8,128)(2,1)S(1)}, bf16[128,2048]{1,0:T(8,128)(2,1)S(1)}, u32[]{:S(2)}, u32[]{:S(2)}) collective-permute-start(bf16[128,2048]{1,0:T(8,128)(2,1)S(1)} %combine.5), channel_id=1, source_target_pairs={{0,3},{1,0},{2,1},{3,2},{4,7},{5,4},{6,5},{7,6},{8,11},{9,8},{10,9... | collective-permute-start | bytes 1572872 | tf_op jit(solution)/shard_map/ppermute | solution.py:30
  156.2 9.9 %collective-permute-start.15 = (bf16[72,2048]{1,0:T(8,128)(2,1)S(1)}, bf16[72,2048]{1,0:T(8,128)(2,1)S(1)}, u32[]{:S(2)}, u32[]{:S(2)}) collective-permute-start(bf16[72,2048]{1,0:T(8,128)(2,1)S(1)} %get-tuple-element.85), channel_id=1, source_target_pairs={{8,0},{12,4},{0,8},{4,12},{9,1},{13,5},{1,9},{5,13},{10,2},{14,6},... | collective-permute-start | bytes 884744 | tf_op jit(solution)/shard_map/ppermute | solution.py:76
  156.5 14.1 %collective-permute-start.16 = (bf16[72,2048]{1,0:T(8,128)(2,1)S(1)}, bf16[72,2048]{1,0:T(8,128)(2,1)S(1)}, u32[]{:S(2)}, u32[]{:S(2)}) collective-permute-start(bf16[72,2048]{1,0:T(8,128)(2,1)S(1)} %get-tuple-element.86), channel_id=1, source_target_pairs={{12,0},{8,4},{4,8},{0,12},{13,1},{9,5},{5,9},{1,13},{14,2},{10,6},... | collective-permute-start | bytes 884744 | tf_op jit(solution)/shard_map/ppermute | solution.py:76
  (13 other events, 70.3 us)

commit v4 on v3

--- a/solution.py
+++ b/solution.py
@@ -97,9 +97,11 @@
 
 
 LOAD_LIMIT = 28
-
-
-def load(*weights):
+EARLY_LIMIT = 55
+CUT_LIMIT = 60
+
+
+def load(*weights, limit=LOAD_LIMIT):
     count = sum(w.shape[0] if w.ndim == 3 else 1 for w in weights)
     return pl.pallas_call(
         load_body,
@@ -107,7 +109,7 @@
         out_specs=[IN_VMEM] * len(weights),
         out_shape=[pltpu.VMEM(w.shape, w.dtype) for w in weights],
         scratch_shapes=[pltpu.SemaphoreType.DMA((count,))],
-        compiler_params=pltpu.CompilerParams(vmem_limit_bytes=LOAD_LIMIT << 20),
+        compiler_params=pltpu.CompilerParams(vmem_limit_bytes=limit << 20),
         name="load",
     )(*weights)
 
@@ -379,35 +381,45 @@
 AHEAD = 16
 
 
-def cut_body(place, x, routes, weights, *outs):
-    chunks, tail = outs[:-1], outs[-1]
-    n_tp, rows = len(chunks), routes.shape[0]
-    top = routes.shape[1]
-    lane = lax.broadcasted_iota(jnp.int32, (rows, rows), 1)
-    fields = jnp.zeros((rows, rows), jnp.float32)
-    for k in range(top):
-        fields = jnp.where(lane == k, routes[:, k : k + 1].astype(jnp.float32), fields)
-        fields = jnp.where(lane == top + k, weights[:, k : k + 1], fields)
-    fields = fields.T[:8].astype(jnp.bfloat16)
+def cut_body(place, x, routes, weights, *refs):
+    (own_routes, own_weights, done), (*chunks, tail) = refs[-3:], refs[:-3]
+    n_tp, (top, rows) = len(chunks), routes.shape
+    moves = [(routes, own_routes), (weights, own_weights)]
     for k, chunk in enumerate(chunks):
         first = (place[0] + k) % n_tp * rows
         before = pl.multiple_of(jnp.maximum(first - AHEAD, 0), AHEAD)
-        chunk[:AHEAD, :] = x[pl.ds(before, AHEAD), :]
-        chunk[AHEAD : AHEAD + rows, :] = x[pl.ds(pl.multiple_of(first, AHEAD), rows), :]
+        first = pl.multiple_of(first, AHEAD)
+        moves.append((x.at[pl.ds(first, rows), :], chunk.at[pl.ds(AHEAD, rows), :]))
+        moves.append((x.at[pl.ds(before, AHEAD), :], chunk.at[pl.ds(0, AHEAD), :]))
+    moves.append((x.at[pl.ds(x.shape[0] - AHEAD, AHEAD), :], tail))
+    copies = [pltpu.make_async_copy(a, b, done.at[i]) for i, (a, b) in enumerate(moves)]
+    for copy in copies:
+        copy.start()
+    for copy in copies:
+        copy.wait()
+    fields = [own_routes[...].astype(jnp.float32), own_weights[...]]
+    fields.append(jnp.zeros((8 - 2 * top, rows), jnp.float32))
+    fields = jnp.concatenate(fields, axis=0).astype(jnp.bfloat16)
+    for chunk in chunks:
         chunk[AHEAD + rows :, :] = jnp.zeros((8, chunk.shape[1]), jnp.bfloat16)
         chunk[AHEAD + rows :, :rows] = fields
-    tail[...] = x[x.shape[0] - AHEAD :, :]
 
 
 def cut(place, x, routes, weights, n_tp):
-    rows, channels = routes.shape[0], x.shape[1]
+    rows, channels = routes.shape[1], x.shape[1]
     chunk = jax.ShapeDtypeStruct((AHEAD + rows + 8, channels), x.dtype)
     return pl.pallas_call(
         cut_body,
-        in_specs=[IN_SMEM] + [IN_VMEM] * 3,
+        in_specs=[IN_SMEM] + [pl.BlockSpec(memory_space=pltpu.HBM)] * 3,
         out_specs=[IN_VMEM] * (n_tp + 1),
-        out_shape=[chunk] * n_tp + [jax.ShapeDtypeStruct((AHEAD, channels), x.dtype)],
-        compiler_params=pltpu.CompilerParams(vmem_limit_bytes=6 << 20),
+        out_shape=[pltpu.VMEM(chunk.shape, x.dtype)] * n_tp
+        + [pltpu.VMEM((AHEAD, channels), x.dtype)],
+        scratch_shapes=[
+            pltpu.VMEM(routes.shape, routes.dtype),
+            pltpu.VMEM(weights.shape, weights.dtype),
+            pltpu.SemaphoreType.DMA((2 * n_tp + 3,)),
+        ],
+        compiler_params=pltpu.CompilerParams(vmem_limit_bytes=CUT_LIMIT << 20),
         name="cut",
     )(place, x, routes, weights)
 
@@ -571,7 +583,7 @@
     slot_rows = local_experts * CAP
 
     place = jnp.stack([lax.axis_index("tp"), lax.axis_index("sp")]).astype(jnp.int32)
-    *chunks, tail = cut(place, pool_input, routes, route_weight, n_tp)
+    *chunks, tail = cut(place, pool_input, routes.T, route_weight.T, n_tp)
     halos = []
     for j in range(n_tp):
         pairs = [(s * n_tp + j, (s + 1) * n_tp) for s in range(n_sp - 1)]
@@ -579,7 +591,7 @@
     chunks = [rotated(x, "tp", k) if k else x for k, x in enumerate(chunks)]
     small = [x.reshape(1, -1) for x in (pool_scale, mix_gain, ffn_gain)]
     scale, mix_gain, ffn_gain, pool_weight, out_weight, resid_in = load(
-        *small, pool_weight, out_weight, resid_in
+        *small, pool_weight, out_weight, resid_in, limit=EARLY_LIMIT
     )
     residual, normed = mix_tokens(
         place, chunks, halos, pool_weight, scale, out_weight, mix_gain, ffn_gain, resid_in

time: 173 us -> 178 us (1.029)
  starting transfers between devices: 35.6 us -> 61.3 us
  waiting for transfers between devices: 91.7 us -> 75.9 us
  local copies, waits for them, and re-layouts: 8.87 us -> 0.62 us
  Pallas kernels: 36 us -> 38.6 us
    ppermute x9, starting transfers between devices: 16.7 us -> 39.5 us  [rotated(): return lax.ppermute(x, axis, [(i, (i + by) % size) for i in range(size)])]
    ppermute x24, waiting for transfers between devices: 57 us -> 42.8 us  [moved(): return lax.ppermute(x, axis, [(b, a) for a, b in pairs] if back else pairs)]
    unnamed x18 -> x4, local copies, waits for them, and re-layouts: 8.87 us -> 0.62 us
    ppermute x24, starting transfers between devices: 15.6 us -> 18.5 us  [moved(): return lax.ppermute(x, axis, [(b, a) for a, b in pairs] if back else pairs)]
  transfers between devices with their start and end apart: 37 -> 37, of which waited for: 18 -> 13; matrix products, arithmetic and copies ran while one was open for 0% -> 0% of each run, Pallas kernels for 18% -> 19%
where the time goes in v4:
time: 178 us; the launch traced here: 177 us
  waiting for transfers between devices  75.9 us (43%)
  starting transfers between devices  61.3 us (34%)
  Pallas kernels  38.6 us (22%)
    ppermute x24, waiting for transfers between devices, moved(): return lax.ppermute(x, axis, [(b, a) for a, b in pairs] if back else pairs)  42.8 us
    ppermute x9, starting transfers between devices, rotated(): return lax.ppermute(x, axis, [(i, (i + by) % size) for i in range(size)])  39.5 us
    ppermute x9, waiting for transfers between devices, rotated(): return lax.ppermute(x, axis, [(i, (i + by) % size) for i in range(size)])  33 us
    ppermute x24, starting transfers between devices, moved(): return lax.ppermute(x, axis, [(b, a) for a, b in pairs] if back else pairs)  18.5 us
    pallas_call x3, Pallas kernels, experts(): pl.pallas_call(lambda *refs: experts_body(n_src, *refs), in_specs=[IN_VME...  16.7 us
    pallas_call x2, Pallas kernels, load(): pl.pallas_call(load_body, in_specs=[pl.BlockSpec(memory_space=pltpu.HBM)]...  11.1 us
  transfers between devices with their start and end apart: 37, of which 13 were waited for; matrix products, arithmetic and copies ran while one was open for 0% of the time, Pallas kernels for 19%

profile of v4, /device:TPU:0, one launch (start us, length us, event | category | flops | bytes accessed | tf_op | source)
XLA Modules:
  0.0 177.4 jit_solution(6081708395895123928)
XLA Ops:
  0.6 1.8 %cut.1 = (bf16[152,256]{1,0:T(8,128)(2,1)S(1)}, bf16[152,256]{1,0:T(8,128)(2,1)S(1)}, bf16[152,256]{1,0:T(8,128)(2,1)S(1)}, bf16[152,256]{1,0:T(8,128)(2,1)S(1)}, bf16[16,256]{1,0:T(8,128)(2,1)S(1)}) custom-call(s32[2]{0:T(128)} %pad_add_fusion.place.refs_0_, bf16[512,256]{1,0:T(8,128)(2,1)} %x.1, s32[2,128]{1,0:T(2,128)} %bitcast.12, f32[2,128]{1,0:T(2,128)} %bitcast.13), custom_call_target="tpu_custom_call" | custom-call | tf_op jit(solution)/shard_map/cut/pallas_call | solution.py:411
  2.4 3.1 %collective-permute-start = (bf16[152,256]{1,0:T(8,128)(2,1)S(1)}, bf16[152,256]{1,0:T(8,128)(2,1)S(1)}, u32[]{:S(2)}, u32[]{:S(2)}) collective-permute-start(bf16[152,256]{1,0:T(8,128)(2,1)S(1)} %get-tuple-element.57), channel_id=1, source_target_pairs={{0,1},{1,2},{2,3},{3,0},{4,5},{5,6},{6,7},{7,4},{8,9},{9,10},{10,1... | collective-permute-start | bytes 233480 | tf_op jit(solution)/shard_map/ppermute | solution.py:30
  5.5 2.6 %collective-permute-start.1 = (bf16[152,256]{1,0:T(8,128)(2,1)S(1)}, bf16[152,256]{1,0:T(8,128)(2,1)S(1)}, u32[]{:S(2)}, u32[]{:S(2)}) collective-permute-start(bf16[152,256]{1,0:T(8,128)(2,1)S(1)} %get-tuple-element.58), channel_id=1, source_target_pairs={{0,2},{1,3},{2,0},{3,1},{4,6},{5,7},{6,4},{7,5},{8,10},{9,11},{10,... | collective-permute-start | bytes 233480 | tf_op jit(solution)/shard_map/ppermute | solution.py:30
  8.1 1.3 collective-permute-start.2
  12.9 2.7 %load.2 = (f32[1,1024]{1,0:T(1,128)S(1)}, f32[1,2048]{1,0:T(1,128)S(1)}, f32[1,2048]{1,0:T(1,128)S(1)}, bf16[4,256,256]{2,1,0:T(8,128)(2,1)S(1)}, bf16[1024,2048...) custom-call(f32[1,1024]{1,0:T(1,128)} %bitcast.11, f32[1,2048]{1,0:T(1,128)} %bitcast.9, f32[1,2048]{1,0:T(1,128)} %bitcast.10, ...), custom_call_target="tpu_custom_call" | custom-call | tf_op jit(solution)/shard_map/load/pallas_call | solution.py:106
  16.2 2.0 %mix.1 = (bf16[128,2048]{1,0:T(8,128)(2,1)S(1)}, bf16[128,2048]{1,0:T(8,128)(2,1)S(1)}) custom-call(s32[2]{0:T(128)S(1)} %copy-done.1, bf16[152,256]{1,0:T(8,128)(2,1)S(1)} %get-tuple-element.56.refs_1_, bf16[152,256]{1,0:T(8,128)(2,1)S(1)} %collective-permute-done.refs_2_, bf16[152,256]{1,0:T(8,128)(2,1)S(1)} %collective-permute-done.1.refs_3_, ...), custom_call_target="tpu_custom_call" | custom-call | tf_op jit(solution)/shard_map/mix/pallas_call | solution.py:486
  18.2 5.7 %collective-permute-start.10 = (bf16[128,2048]{1,0:T(8,128)(2,1)S(1)}, bf16[128,2048]{1,0:T(8,128)(2,1)S(1)}, u32[]{:S(2)}, u32[]{:S(2)}) collective-permute-start(bf16[128,2048]{1,0:T(8,128)(2,1)S(1)} %get-tuple-element.71.refs_1_), channel_id=1, source_target_pairs={{0,1},{1,2},{2,3},{3,0},{4,5},{5,6},{6,7},{7,4},{8,9},{9,10},{10,1... | collective-permute-start | bytes 1572872 | tf_op jit(solution)/shard_map/ppermute | solution.py:30
  23.9 16.0 %collective-permute-done.10.refs_1_ = bf16[128,2048]{1,0:T(8,128)(2,1)S(1)} collective-permute-done((bf16[128,2048]{1,0:T(8,128)(2,1)S(1)}, bf16[128,2048]{1,0:T(8,128)(2,1)S(1)}, u32[]{:S(2)}, u32[]{:S(2)}) %collective-permute-start.10) | collective-permute-done | bytes 524320 | tf_op jit(solution)/shard_map/ppermute | solution.py:30
  39.9 3.8 %collective-permute-start.17 = (bf16[128,2048]{1,0:T(8,128)(2,1)S(1)}, bf16[128,2048]{1,0:T(8,128)(2,1)S(1)}, u32[]{:S(2)}, u32[]{:S(2)}) collective-permute-start(bf16[128,2048]{1,0:T(8,128)(2,1)S(1)} %get-tuple-element.71.refs_1_), channel_id=1, source_target_pairs={{0,3},{1,0},{2,1},{3,2},{4,7},{5,4},{6,5},{7,6},{8,11},{9,8},{10,9... | collective-permute-start | bytes 1572872 | tf_op jit(solution)/shard_map/ppermute | solution.py:30
  44.7 11.5 %collective-permute-done.28.refs_1_ = bf16[128,2048]{1,0:T(8,128)(2,1)S(1)} collective-permute-done((bf16[128,2048]{1,0:T(8,128)(2,1)S(1)}, bf16[128,2048]{1,0:T(8,128)(2,1)S(1)}, u32[]{:S(2)}, u32[]{:S(2)}) %collective-permute-start.28) | collective-permute-done | bytes 524320 | tf_op jit(solution)/shard_map/ppermute | solution.py:30
  57.3 1.4 collective-permute-start.30
  60.0 5.5 %collective-permute-done.17.refs_1_ = bf16[128,2048]{1,0:T(8,128)(2,1)S(1)} collective-permute-done((bf16[128,2048]{1,0:T(8,128)(2,1)S(1)}, bf16[128,2048]{1,0:T(8,128)(2,1)S(1)}, u32[]{:S(2)}, u32[]{:S(2)}) %collective-permute-start.17) | collective-permute-done | bytes 524320 | tf_op jit(solution)/shard_map/ppermute | solution.py:30
  66.0 2.0 %collective-permute-start.9 = (bf16[72,2048]{1,0:T(8,128)(2,1)S(1)}, bf16[72,2048]{1,0:T(8,128)(2,1)S(1)}, u32[]{:S(2)}, u32[]{:S(2)}) collective-permute-start(bf16[72,2048]{1,0:T(8,128)(2,1)S(1)} %get-tuple-element.75), channel_id=1, source_target_pairs={{0,12},{4,8},{8,4},{12,0},{1,13},{5,9},{9,5},{13,1},{2,14},{6,10},... | collective-permute-start | bytes 884744 | tf_op jit(solution)/shard_map/ppermute | solution.py:76
  68.2 8.4 %load.3 = (bf16[8,2048,256]{2,1,0:T(8,128)(2,1)S(1)}, bf16[8,2048,256]{2,1,0:T(8,128)(2,1)S(1)}, bf16[8,256,2048]{2,1,0:T(8,128)(2,1)S(1)}) custom-call(bf16[8,2048,256]{2,1,0:T(8,128)(2,1)} %refs_0_.1, bf16[8,2048,256]{2,1,0:T(8,128)(2,1)} %refs_1_.1, bf16[8,256,2048]{2,1,0:T(8,128)(2,1)} %refs_2_.1), custom_call_target="tpu_custom_call" | custom-call | tf_op jit(solution)/shard_map/load/pallas_call | solution.py:106
  77.0 5.5 %experts.5 = (bf16[72,2048]{1,0:T(8,128)(2,1)S(1)}, bf16[72,2048]{1,0:T(8,128)(2,1)S(1)}, bf16[72,2048]{1,0:T(8,128)(2,1)S(1)}, bf16[72,2048]{1,0:T(8,128)(2,1)S(1)}) custom-call(bf16[72,2048]{1,0:T(8,128)(2,1)S(1)} %get-tuple-element.99.refs_0_, bf16[72,2048]{1,0:T(8,128)(2,1)S(1)} %collective-permute-done.29.refs_1_, ...), custom_call_target="tpu_custom_call" | custom-call | flops 905969664 | bytes 27525120 | tf_op jit(solution)/shard_map/experts/pallas_call | solution.py:265
  85.0 1.4 collective-permute-start.33
  87.8 4.7 %collective-permute-done.19.refs_2_ = bf16[72,2048]{1,0:T(8,128)(2,1)S(1)} collective-permute-done((bf16[72,2048]{1,0:T(8,128)(2,1)S(1)}, bf16[72,2048]{1,0:T(8,128)(2,1)S(1)}, u32[]{:S(2)}, u32[]{:S(2)}) %collective-permute-start.19) | collective-permute-done | bytes 294944 | tf_op jit(solution)/shard_map/ppermute | solution.py:76
  92.5 5.2 %collective-permute-done.20.refs_3_ = bf16[72,2048]{1,0:T(8,128)(2,1)S(1)} collective-permute-done((bf16[72,2048]{1,0:T(8,128)(2,1)S(1)}, bf16[72,2048]{1,0:T(8,128)(2,1)S(1)}, u32[]{:S(2)}, u32[]{:S(2)}) %collective-permute-start.20) | collective-permute-done | bytes 294944 | tf_op jit(solution)/shard_map/ppermute | solution.py:76
  97.7 1.4 collective-permute-start.12
  100.0 5.5 %experts.4 = (bf16[72,2048]{1,0:T(8,128)(2,1)S(1)}, bf16[72,2048]{1,0:T(8,128)(2,1)S(1)}, bf16[72,2048]{1,0:T(8,128)(2,1)S(1)}, bf16[72,2048]{1,0:T(8,128)(2,1)S(1)}) custom-call(bf16[72,2048]{1,0:T(8,128)(2,1)S(1)} %get-tuple-element.87.refs_0_, bf16[72,2048]{1,0:T(8,128)(2,1)S(1)} %collective-permute-done.18.refs_1_, ...), custom_call_target="tpu_custom_call" | custom-call | flops 905969664 | bytes 27525120 | tf_op jit(solution)/shard_map/experts/pallas_call | solution.py:265
  105.6 4.7 %collective-permute-done.34.refs_5_ = bf16[72,2048]{1,0:T(8,128)(2,1)S(1)} collective-permute-done((bf16[72,2048]{1,0:T(8,128)(2,1)S(1)}, bf16[72,2048]{1,0:T(8,128)(2,1)S(1)}, u32[]{:S(2)}, u32[]{:S(2)}) %collective-permute-start.34) | collective-permute-done | bytes 294944 | tf_op jit(solution)/shard_map/ppermute | solution.py:76
  110.3 1.4 collective-permute-start.22
  112.5 10.8 %collective-permute-start.35 = (bf16[128,2048]{1,0:T(8,128)(2,1)S(1)}, bf16[128,2048]{1,0:T(8,128)(2,1)S(1)}, u32[]{:S(2)}, u32[]{:S(2)}) collective-permute-start(bf16[128,2048]{1,0:T(8,128)(2,1)S(1)} %combine.4), channel_id=1, source_target_pairs={{0,3},{1,0},{2,1},{3,2},{4,7},{5,4},{6,5},{7,6},{8,11},{9,8},{10,9... | collective-permute-start | bytes 1572872 | tf_op jit(solution)/shard_map/ppermute | solution.py:30
  123.4 1.3 collective-permute-start.23
  124.7 5.7 %experts.3 = (bf16[72,2048]{1,0:T(8,128)(2,1)S(1)}, bf16[72,2048]{1,0:T(8,128)(2,1)S(1)}, bf16[72,2048]{1,0:T(8,128)(2,1)S(1)}, bf16[72,2048]{1,0:T(8,128)(2,1)S...) custom-call(bf16[72,2048]{1,0:T(8,128)(2,1)S(1)} %get-tuple-element., ...), custom_call_target="tpu_custom_call" | custom-call | flops 1811939328 | bytes 29884416 | tf_op jit(solution)/shard_map/experts/pallas_call | solution.py:265
  132.3 3.3 %collective-permute-done.23.refs_5_ = bf16[72,2048]{1,0:T(8,128)(2,1)S(1)} collective-permute-done((bf16[72,2048]{1,0:T(8,128)(2,1)S(1)}, bf16[72,2048]{1,0:T(8,128)(2,1)S(1)}, u32[]{:S(2)}, u32[]{:S(2)}) %collective-permute-start.23) | collective-permute-done | bytes 294944 | tf_op jit(solution)/shard_map/ppermute | solution.py:76
  136.5 6.6 %collective-permute-done.26.refs_4_ = bf16[72,2048]{1,0:T(8,128)(2,1)S(1)} collective-permute-done((bf16[72,2048]{1,0:T(8,128)(2,1)S(1)}, bf16[72,2048]{1,0:T(8,128)(2,1)S(1)}, u32[]{:S(2)}, u32[]{:S(2)}) %collective-permute-start.26) | collective-permute-done | bytes 294944 | tf_op jit(solution)/shard_map/ppermute | solution.py:76
  143.0 4.7 %collective-permute-done.27.refs_5_ = bf16[72,2048]{1,0:T(8,128)(2,1)S(1)} collective-permute-done((bf16[72,2048]{1,0:T(8,128)(2,1)S(1)}, bf16[72,2048]{1,0:T(8,128)(2,1)S(1)}, u32[]{:S(2)}, u32[]{:S(2)}) %collective-permute-start.27) | collective-permute-done | bytes 294944 | tf_op jit(solution)/shard_map/ppermute | solution.py:76
  148.5 12.1 %collective-permute-start.36 = (bf16[128,2048]{1,0:T(8,128)(2,1)S(1)}, bf16[128,2048]{1,0:T(8,128)(2,1)S(1)}, u32[]{:S(2)}, u32[]{:S(2)}) collective-permute-start(bf16[128,2048]{1,0:T(8,128)(2,1)S(1)} %combine.5), channel_id=1, source_target_pairs={{0,3},{1,0},{2,1},{3,2},{4,7},{5,4},{6,5},{7,6},{8,11},{9,8},{10,9... | collective-permute-start | bytes 1572872 | tf_op jit(solution)/shard_map/ppermute | solution.py:30
  162.5 8.4 %collective-permute-done.15.refs_6_ = bf16[72,2048]{1,0:T(8,128)(2,1)S(1)} collective-permute-done((bf16[72,2048]{1,0:T(8,128)(2,1)S(1)}, bf16[72,2048]{1,0:T(8,128)(2,1)S(1)}, u32[]{:S(2)}, u32[]{:S(2)}) %collective-permute-start.15) | collective-permute-done | bytes 294944 | tf_op jit(solution)/shard_map/ppermute | solution.py:76
  170.9 4.6 %collective-permute-done.16.refs_7_ = bf16[72,2048]{1,0:T(8,128)(2,1)S(1)} collective-permute-done((bf16[72,2048]{1,0:T(8,128)(2,1)S(1)}, bf16[72,2048]{1,0:T(8,128)(2,1)S(1)}, u32[]{:S(2)}, u32[]{:S(2)}) %collective-permute-start.16) | collective-permute-done | bytes 294944 | tf_op jit(solution)/shard_map/ppermute | solution.py:76
  175.5 1.8 %finish.1 = bf16[128,2048]{1,0:T(8,128)(2,1)} custom-call(s32[4,128,2]{2,1,0:T(8,128)S(1)} %get-tuple-element.60.refs_0_, f32[4,128,2]{2,1,0:T(8,128)S(1)} %get-tuple-element.61.refs_1_, bf16[128,2048]{1,0:T(8,128)(2,1)S(1)} %get-tuple-element.69.refs_2_, f32[1,2048]{1,0:T(1,128)S(1)} %bitcast.8, bf16[72,2048]{1,0:T(8,128)(2,1)S(1)} %get-tuple-element.83.refs_4_, ...), custom_call_target="tpu_custom_call" | custom-call | tf_op jit(solution)/shard_map/finish/pallas_call | solution.py:203
  (63 shorter events, 20.3 us)
Async XLA Ops:
  2.4 13.2 %collective-permute-start = (bf16[152,256]{1,0:T(8,128)(2,1)S(1)}, bf16[152,256]{1,0:T(8,128)(2,1)S(1)}, u32[]{:S(2)}, u32[]{:S(2)}) collective-permute-start(bf16[152,256]{1,0:T(8,128)(2,1)S(1)} %get-tuple-element.57), channel_id=1, source_target_pairs={{0,1},{1,2},{2,3},{3,0},{4,5},{5,6},{6,7},{7,4},{8,9},{9,10},{10,1... | collective-permute-start | bytes 233480 | tf_op jit(solution)/shard_map/ppermute | solution.py:30
  5.5 10.1 %collective-permute-start.1 = (bf16[152,256]{1,0:T(8,128)(2,1)S(1)}, bf16[152,256]{1,0:T(8,128)(2,1)S(1)}, u32[]{:S(2)}, u32[]{:S(2)}) collective-permute-start(bf16[152,256]{1,0:T(8,128)(2,1)S(1)} %get-tuple-element.58), channel_id=1, source_target_pairs={{0,2},{1,3},{2,0},{3,1},{4,6},{5,7},{6,4},{7,5},{8,10},{9,11},{10,... | collective-permute-start | bytes 233480 | tf_op jit(solution)/shard_map/ppermute | solution.py:30
  8.1 7.5 %collective-permute-start.2 = (bf16[152,256]{1,0:T(8,128)(2,1)S(1)}, bf16[152,256]{1,0:T(8,128)(2,1)S(1)}, u32[]{:S(2)}, u32[]{:S(2)}) collective-permute-start(bf16[152,256]{1,0:T(8,128)(2,1)S(1)} %get-tuple-element.59), channel_id=1, source_target_pairs={{0,3},{1,0},{2,1},{3,2},{4,7},{5,4},{6,5},{7,6},{8,11},{9,8},{10,9... | collective-permute-start | bytes 233480 | tf_op jit(solution)/shard_map/ppermute | solution.py:30
  18.2 21.7 %collective-permute-start.10 = (bf16[128,2048]{1,0:T(8,128)(2,1)S(1)}, bf16[128,2048]{1,0:T(8,128)(2,1)S(1)}, u32[]{:S(2)}, u32[]{:S(2)}) collective-permute-start(bf16[128,2048]{1,0:T(8,128)(2,1)S(1)} %get-tuple-element.71.refs_1_), channel_id=1, source_target_pairs={{0,1},{1,2},{2,3},{3,0},{4,5},{5,6},{6,7},{7,4},{8,9},{9,10},{10,1... | collective-permute-start | bytes 1572872 | tf_op jit(solution)/shard_map/ppermute | solution.py:30
  39.9 16.3 %collective-permute-start.28 = (bf16[128,2048]{1,0:T(8,128)(2,1)S(1)}, bf16[128,2048]{1,0:T(8,128)(2,1)S(1)}, u32[]{:S(2)}, u32[]{:S(2)}) collective-permute-start(bf16[128,2048]{1,0:T(8,128)(2,1)S(1)} %collective-permute-done.10.refs_1_), channel_id=1, source_target_pairs={{0,1},{1,2},{2,3},{3,0},{4,5},{5,6},{6,7},{7,4},{8,9},{9,10},{10,1... | collective-permute-start | bytes 1572872 | tf_op jit(solution)/shard_map/ppermute | solution.py:30
  39.9 25.6 %collective-permute-start.17 = (bf16[128,2048]{1,0:T(8,128)(2,1)S(1)}, bf16[128,2048]{1,0:T(8,128)(2,1)S(1)}, u32[]{:S(2)}, u32[]{:S(2)}) collective-permute-start(bf16[128,2048]{1,0:T(8,128)(2,1)S(1)} %get-tuple-element.71.refs_1_), channel_id=1, source_target_pairs={{0,3},{1,0},{2,1},{3,2},{4,7},{5,4},{6,5},{7,6},{8,11},{9,8},{10,9... | collective-permute-start | bytes 1572872 | tf_op jit(solution)/shard_map/ppermute | solution.py:30
  56.6 9.3 %collective-permute-start.29 = (bf16[72,2048]{1,0:T(8,128)(2,1)S(1)}, bf16[72,2048]{1,0:T(8,128)(2,1)S(1)}, u32[]{:S(2)}, u32[]{:S(2)}) collective-permute-start(bf16[72,2048]{1,0:T(8,128)(2,1)S(1)} %get-tuple-element.100), channel_id=1, source_target_pairs={{0,4},{4,0},{8,12},{12,8},{1,5},{5,1},{9,13},{13,9},{2,6},{6,2},{1... | collective-permute-start | bytes 884744 | tf_op jit(solution)/shard_map/ppermute | solution.py:76
  57.3 10.6 %collective-permute-start.30 = (bf16[72,2048]{1,0:T(8,128)(2,1)S(1)}, bf16[72,2048]{1,0:T(8,128)(2,1)S(1)}, u32[]{:S(2)}, u32[]{:S(2)}) collective-permute-start(bf16[72,2048]{1,0:T(8,128)(2,1)S(1)} %get-tuple-element.101), channel_id=1, source_target_pairs={{0,8},{4,12},{8,0},{12,4},{1,9},{5,13},{9,1},{13,5},{2,10},{6,14},... | collective-permute-start | bytes 884744 | tf_op jit(solution)/shard_map/ppermute | solution.py:76
  58.7 17.9 %collective-permute-start.31 = (bf16[72,2048]{1,0:T(8,128)(2,1)S(1)}, bf16[72,2048]{1,0:T(8,128)(2,1)S(1)}, u32[]{:S(2)}, u32[]{:S(2)}) collective-permute-start(bf16[72,2048]{1,0:T(8,128)(2,1)S(1)} %get-tuple-element.102), channel_id=1, source_target_pairs={{0,12},{4,8},{8,4},{12,0},{1,13},{5,9},{9,5},{13,1},{2,14},{6,10},... | collective-permute-start | bytes 884744 | tf_op jit(solution)/shard_map/ppermute | solution.py:76
  59.2 23.3 %collective-permute-start.7 = (bf16[72,2048]{1,0:T(8,128)(2,1)S(1)}, bf16[72,2048]{1,0:T(8,128)(2,1)S(1)}, u32[]{:S(2)}, u32[]{:S(2)}) collective-permute-start(bf16[72,2048]{1,0:T(8,128)(2,1)S(1)} %get-tuple-element.73), channel_id=1, source_target_pairs={{0,4},{4,0},{8,12},{12,8},{1,5},{5,1},{9,13},{13,9},{2,6},{6,2},{1... | collective-permute-start | bytes 884744 | tf_op jit(solution)/shard_map/ppermute | solution.py:76
  65.5 18.4 %collective-permute-start.8 = (bf16[72,2048]{1,0:T(8,128)(2,1)S(1)}, bf16[72,2048]{1,0:T(8,128)(2,1)S(1)}, u32[]{:S(2)}, u32[]{:S(2)}) collective-permute-start(bf16[72,2048]{1,0:T(8,128)(2,1)S(1)} %get-tuple-element.74), channel_id=1, source_target_pairs={{0,8},{4,12},{8,0},{12,4},{1,9},{5,13},{9,1},{13,5},{2,10},{6,14},... | collective-permute-start | bytes 884744 | tf_op jit(solution)/shard_map/ppermute | solution.py:76
  66.0 19.1 %collective-permute-start.9 = (bf16[72,2048]{1,0:T(8,128)(2,1)S(1)}, bf16[72,2048]{1,0:T(8,128)(2,1)S(1)}, u32[]{:S(2)}, u32[]{:S(2)}) collective-permute-start(bf16[72,2048]{1,0:T(8,128)(2,1)S(1)} %get-tuple-element.75), channel_id=1, source_target_pairs={{0,12},{4,8},{8,4},{12,0},{1,13},{5,9},{9,5},{13,1},{2,14},{6,10},... | collective-permute-start | bytes 884744 | tf_op jit(solution)/shard_map/ppermute | solution.py:76
  67.9 18.5 %collective-permute-start.18 = (bf16[72,2048]{1,0:T(8,128)(2,1)S(1)}, bf16[72,2048]{1,0:T(8,128)(2,1)S(1)}, u32[]{:S(2)}, u32[]{:S(2)}) collective-permute-start(bf16[72,2048]{1,0:T(8,128)(2,1)S(1)} %get-tuple-element.88), channel_id=1, source_target_pairs={{0,4},{4,0},{8,12},{12,8},{1,5},{5,1},{9,13},{13,9},{2,6},{6,2},{1... | collective-permute-start | bytes 884744 | tf_op jit(solution)/shard_map/ppermute | solution.py:76
  76.6 15.9 %collective-permute-start.19 = (bf16[72,2048]{1,0:T(8,128)(2,1)S(1)}, bf16[72,2048]{1,0:T(8,128)(2,1)S(1)}, u32[]{:S(2)}, u32[]{:S(2)}) collective-permute-start(bf16[72,2048]{1,0:T(8,128)(2,1)S(1)} %get-tuple-element.89), channel_id=1, source_target_pairs={{0,8},{4,12},{8,0},{12,4},{1,9},{5,13},{9,1},{13,5},{2,10},{6,14},... | collective-permute-start | bytes 884744 | tf_op jit(solution)/shard_map/ppermute | solution.py:76
  82.6 15.1 %collective-permute-start.20 = (bf16[72,2048]{1,0:T(8,128)(2,1)S(1)}, bf16[72,2048]{1,0:T(8,128)(2,1)S(1)}, u32[]{:S(2)}, u32[]{:S(2)}) collective-permute-start(bf16[72,2048]{1,0:T(8,128)(2,1)S(1)} %get-tuple-element.90), channel_id=1, source_target_pairs={{0,12},{4,8},{8,4},{12,0},{1,13},{5,9},{9,5},{13,1},{2,14},{6,10},... | collective-permute-start | bytes 884744 | tf_op jit(solution)/shard_map/ppermute | solution.py:76
  83.9 15.2 %collective-permute-start.32 = (bf16[72,2048]{1,0:T(8,128)(2,1)S(1)}, bf16[72,2048]{1,0:T(8,128)(2,1)S(1)}, u32[]{:S(2)}, u32[]{:S(2)}) collective-permute-start(bf16[72,2048]{1,0:T(8,128)(2,1)S(1)} %get-tuple-element.104), channel_id=1, source_target_pairs={{4,0},{0,4},{12,8},{8,12},{5,1},{1,5},{13,9},{9,13},{6,2},{2,6},{1... | collective-permute-start | bytes 884744 | tf_op jit(solution)/shard_map/ppermute | solution.py:76
  85.0 20.5 %collective-permute-start.33 = (bf16[72,2048]{1,0:T(8,128)(2,1)S(1)}, bf16[72,2048]{1,0:T(8,128)(2,1)S(1)}, u32[]{:S(2)}, u32[]{:S(2)}) collective-permute-start(bf16[72,2048]{1,0:T(8,128)(2,1)S(1)} %get-tuple-element.105), channel_id=1, source_target_pairs={{8,0},{12,4},{0,8},{4,12},{9,1},{13,5},{1,9},{5,13},{10,2},{14,6},... | collective-permute-start | bytes 884744 | tf_op jit(solution)/shard_map/ppermute | solution.py:76
  86.5 23.9 %collective-permute-start.34 = (bf16[72,2048]{1,0:T(8,128)(2,1)S(1)}, bf16[72,2048]{1,0:T(8,128)(2,1)S(1)}, u32[]{:S(2)}, u32[]{:S(2)}) collective-permute-start(bf16[72,2048]{1,0:T(8,128)(2,1)S(1)} %get-tuple-element.106), channel_id=1, source_target_pairs={{12,0},{8,4},{4,8},{0,12},{13,1},{9,5},{5,9},{1,13},{14,2},{10,6},... | collective-permute-start | bytes 884744 | tf_op jit(solution)/shard_map/ppermute | solution.py:76
  92.5 20.1 %collective-permute-start.11 = (bf16[72,2048]{1,0:T(8,128)(2,1)S(1)}, bf16[72,2048]{1,0:T(8,128)(2,1)S(1)}, u32[]{:S(2)}, u32[]{:S(2)}) collective-permute-start(bf16[72,2048]{1,0:T(8,128)(2,1)S(1)} %get-tuple-element.77), channel_id=1, source_target_pairs={{0,4},{4,0},{8,12},{12,8},{1,5},{5,1},{9,13},{13,9},{2,6},{6,2},{1... | collective-permute-start | bytes 884744 | tf_op jit(solution)/shard_map/ppermute | solution.py:76
  97.7 25.7 %collective-permute-start.12 = (bf16[72,2048]{1,0:T(8,128)(2,1)S(1)}, bf16[72,2048]{1,0:T(8,128)(2,1)S(1)}, u32[]{:S(2)}, u32[]{:S(2)}) collective-permute-start(bf16[72,2048]{1,0:T(8,128)(2,1)S(1)} %get-tuple-element.78), channel_id=1, source_target_pairs={{0,8},{4,12},{8,0},{12,4},{1,9},{5,13},{9,1},{13,5},{2,10},{6,14},... | collective-permute-start | bytes 884744 | tf_op jit(solution)/shard_map/ppermute | solution.py:76
  99.1 25.6 %collective-permute-start.13 = (bf16[72,2048]{1,0:T(8,128)(2,1)S(1)}, bf16[72,2048]{1,0:T(8,128)(2,1)S(1)}, u32[]{:S(2)}, u32[]{:S(2)}) collective-permute-start(bf16[72,2048]{1,0:T(8,128)(2,1)S(1)} %get-tuple-element.79), channel_id=1, source_target_pairs={{0,12},{4,8},{8,4},{12,0},{1,13},{5,9},{9,5},{13,1},{2,14},{6,10},... | collective-permute-start | bytes 884744 | tf_op jit(solution)/shard_map/ppermute | solution.py:76
  105.5 25.1 %collective-permute-start.21 = (bf16[72,2048]{1,0:T(8,128)(2,1)S(1)}, bf16[72,2048]{1,0:T(8,128)(2,1)S(1)}, u32[]{:S(2)}, u32[]{:S(2)}) collective-permute-start(bf16[72,2048]{1,0:T(8,128)(2,1)S(1)} %get-tuple-element.92), channel_id=1, source_target_pairs={{4,0},{0,4},{12,8},{8,12},{5,1},{1,5},{13,9},{9,13},{6,2},{2,6},{1... | collective-permute-start | bytes 884744 | tf_op jit(solution)/shard_map/ppermute | solution.py:76
  110.3 21.0 %collective-permute-start.22 = (bf16[72,2048]{1,0:T(8,128)(2,1)S(1)}, bf16[72,2048]{1,0:T(8,128)(2,1)S(1)}, u32[]{:S(2)}, u32[]{:S(2)}) collective-permute-start(bf16[72,2048]{1,0:T(8,128)(2,1)S(1)} %get-tuple-element.93), channel_id=1, source_target_pairs={{8,0},{12,4},{0,8},{4,12},{9,1},{13,5},{1,9},{5,13},{10,2},{14,6},... | collective-permute-start | bytes 884744 | tf_op jit(solution)/shard_map/ppermute | solution.py:76
  112.5 35.2 %collective-permute-start.35 = (bf16[128,2048]{1,0:T(8,128)(2,1)S(1)}, bf16[128,2048]{1,0:T(8,128)(2,1)S(1)}, u32[]{:S(2)}, u32[]{:S(2)}) collective-permute-start(bf16[128,2048]{1,0:T(8,128)(2,1)S(1)} %combine.4), channel_id=1, source_target_pairs={{0,3},{1,0},{2,1},{3,2},{4,7},{5,4},{6,5},{7,6},{8,11},{9,8},{10,9... | collective-permute-start | bytes 1572872 | tf_op jit(solution)/shard_map/ppermute | solution.py:30
  123.4 12.3 %collective-permute-start.23 = (bf16[72,2048]{1,0:T(8,128)(2,1)S(1)}, bf16[72,2048]{1,0:T(8,128)(2,1)S(1)}, u32[]{:S(2)}, u32[]{:S(2)}) collective-permute-start(bf16[72,2048]{1,0:T(8,128)(2,1)S(1)} %get-tuple-element.94), channel_id=1, source_target_pairs={{12,0},{8,4},{4,8},{0,12},{13,1},{9,5},{5,9},{1,13},{14,2},{10,6},... | collective-permute-start | bytes 884744 | tf_op jit(solution)/shard_map/ppermute | solution.py:76
  130.4 6.1 %collective-permute-start.25 = (bf16[72,2048]{1,0:T(8,128)(2,1)S(1)}, bf16[72,2048]{1,0:T(8,128)(2,1)S(1)}, u32[]{:S(2)}, u32[]{:S(2)}) collective-permute-start(bf16[72,2048]{1,0:T(8,128)(2,1)S(1)} %get-tuple-element.96), channel_id=1, source_target_pairs={{4,0},{0,4},{12,8},{8,12},{5,1},{1,5},{13,9},{9,13},{6,2},{2,6},{1... | collective-permute-start | bytes 884744 | tf_op jit(solution)/shard_map/ppermute | solution.py:76
  130.6 12.4 %collective-permute-start.26 = (bf16[72,2048]{1,0:T(8,128)(2,1)S(1)}, bf16[72,2048]{1,0:T(8,128)(2,1)S(1)}, u32[]{:S(2)}, u32[]{:S(2)}) collective-permute-start(bf16[72,2048]{1,0:T(8,128)(2,1)S(1)} %get-tuple-element.97), channel_id=1, source_target_pairs={{8,0},{12,4},{0,8},{4,12},{9,1},{13,5},{1,9},{5,13},{10,2},{14,6},... | collective-permute-start | bytes 884744 | tf_op jit(solution)/shard_map/ppermute | solution.py:76
  131.3 16.4 %collective-permute-start.27 = (bf16[72,2048]{1,0:T(8,128)(2,1)S(1)}, bf16[72,2048]{1,0:T(8,128)(2,1)S(1)}, u32[]{:S(2)}, u32[]{:S(2)}) collective-permute-start(bf16[72,2048]{1,0:T(8,128)(2,1)S(1)} %get-tuple-element.98), channel_id=1, source_target_pairs={{12,0},{8,4},{4,8},{0,12},{13,1},{9,5},{5,9},{1,13},{14,2},{10,6},... | collective-permute-start | bytes 884744 | tf_op jit(solution)/shard_map/ppermute | solution.py:76
  136.4 39.1 %collective-permute-start.24 = (bf16[128,2048]{1,0:T(8,128)(2,1)S(1)}, bf16[128,2048]{1,0:T(8,128)(2,1)S(1)}, u32[]{:S(2)}, u32[]{:S(2)}) collective-permute-start(bf16[128,2048]{1,0:T(8,128)(2,1)S(1)} %combine.3), channel_id=1, source_target_pairs={{0,1},{1,2},{2,3},{3,0},{4,5},{5,6},{6,7},{7,4},{8,9},{9,10},{10,1... | collective-permute-start | bytes 1572872 | tf_op jit(solution)/shard_map/ppermute | solution.py:30
  148.5 27.0 %collective-permute-start.36 = (bf16[128,2048]{1,0:T(8,128)(2,1)S(1)}, bf16[128,2048]{1,0:T(8,128)(2,1)S(1)}, u32[]{:S(2)}, u32[]{:S(2)}) collective-permute-start(bf16[128,2048]{1,0:T(8,128)(2,1)S(1)} %combine.5), channel_id=1, source_target_pairs={{0,3},{1,0},{2,1},{3,2},{4,7},{5,4},{6,5},{7,6},{8,11},{9,8},{10,9... | collective-permute-start | bytes 1572872 | tf_op jit(solution)/shard_map/ppermute | solution.py:30
  161.0 9.9 %collective-permute-start.15 = (bf16[72,2048]{1,0:T(8,128)(2,1)S(1)}, bf16[72,2048]{1,0:T(8,128)(2,1)S(1)}, u32[]{:S(2)}, u32[]{:S(2)}) collective-permute-start(bf16[72,2048]{1,0:T(8,128)(2,1)S(1)} %get-tuple-element.85), channel_id=1, source_target_pairs={{8,0},{12,4},{0,8},{4,12},{9,1},{13,5},{1,9},{5,13},{10,2},{14,6},... | collective-permute-start | bytes 884744 | tf_op jit(solution)/shard_map/ppermute | solution.py:76
  161.3 14.2 %collective-permute-start.16 = (bf16[72,2048]{1,0:T(8,128)(2,1)S(1)}, bf16[72,2048]{1,0:T(8,128)(2,1)S(1)}, u32[]{:S(2)}, u32[]{:S(2)}) collective-permute-start(bf16[72,2048]{1,0:T(8,128)(2,1)S(1)} %get-tuple-element.86), channel_id=1, source_target_pairs={{12,0},{8,4},{4,8},{0,12},{13,1},{9,5},{5,9},{1,13},{14,2},{10,6},... | collective-permute-start | bytes 884744 | tf_op jit(solution)/shard_map/ppermute | solution.py:76
  (7 other events, 64.3 us)

commit v5 on v4

--- a/solution.py
+++ b/solution.py
@@ -177,18 +177,22 @@
 
 
 def finish_body(at, n_back, slot, weight, resid, gain, *refs):
-    backs, parts, (out, mix) = refs[:n_back], refs[n_back:-2], refs[-2:]
+    backs, apart = refs[:n_back], refs[n_back : 2 * n_back]
+    parts, (out, mix) = refs[2 * n_back : -2], refs[-2:]
     rows, width = backs[0].shape[0], out.shape[1]
+    apart_from = backs[0].shape[1]
     share = [shares_of(at, slot, weight, d, rows) for d in range(n_back)]
     square = jnp.zeros((out.shape[0], LANES), jnp.float32)
     for j in range(0, width, 2 * LANES):
-        cols = slice(j, j + 2 * LANES)
-        total = parts[0][:, cols].astype(jnp.float32) if parts else 0.0
-        for part in parts[1:]:
+        near = j < apart_from
+        first = j if near else j - apart_from
+        cols = slice(first, first + 2 * LANES)
+        total = jnp.zeros((out.shape[0], 2 * LANES), jnp.float32)
+        for part in parts if near else ():
             total = total + part[:, cols].astype(jnp.float32)
-        for d, back in enumerate(backs):
+        for d, back in enumerate(backs if near else apart):
             total = total + jnp.dot(share[d], back[:, cols], preferred_element_type=jnp.float32)
-        mix[:, cols] = total
+        mix[:, j : j + 2 * LANES] = total
         square = square + total[:, :LANES] * total[:, :LANES]
         square = square + total[:, LANES:] * total[:, LANES:]
     mean = jnp.sum(square, axis=1, keepdims=True) / width
@@ -199,23 +203,24 @@
         out[:, cols] = (resid[:, cols].astype(jnp.float32) + scaled).astype(out.dtype)
 
 
-def finish(at, slot, weight, resid, gain, backs, parts):
+def finish(at, slot, weight, resid, gain, backs, apart, parts):
     return pl.pallas_call(
         lambda *refs: finish_body(at, len(backs), *refs),
-        in_specs=[IN_VMEM] * (4 + len(backs) + len(parts)),
+        in_specs=[IN_VMEM] * (4 + 2 * len(backs) + len(parts)),
         out_specs=IN_VMEM,
         out_shape=jax.ShapeDtypeStruct(resid.shape, resid.dtype),
         scratch_shapes=[pltpu.VMEM(resid.shape, jnp.float32)],
         compiler_params=pltpu.CompilerParams(vmem_limit_bytes=6 << 20),
         name="finish",
-    )(slot, weight, resid, gain.reshape(1, -1), *backs, *parts)
-
-
-def experts_body(n_src, *refs):
+    )(slot, weight, resid, gain.reshape(1, -1), *backs, *apart, *parts)
+
+
+def experts_body(n_src, n_sp, *refs):
     xs, (wg, wu, wd) = refs[:n_src], refs[n_src : n_src + 3]
-    outs, (into, outof) = refs[n_src + 3 : 2 * n_src + 3], refs[2 * n_src + 3 :]
-    count, width = wg.shape[0], xs[0].shape[1]
-    tiles, left = divmod(xs[0].shape[0] // count, 8)
+    outs, sums, (into, outof) = refs[n_src + 3 : 2 * n_src + 3], refs[2 * n_src + 3 : -2], refs[-2:]
+    count, (rows, width) = wg.shape[0], xs[0].shape
+    apart_from = outs[0].shape[1]
+    tiles, left = divmod(rows // count, 8)
     whole = count * tiles * 8
     for s, x in enumerate(xs):
         for j in range(width // LANES):
@@ -225,9 +230,9 @@
             )
 
     def one(e, carry):
-        own = [pl.ds(pl.multiple_of((e * tiles + i) * 8, 8), 8) for i in range(tiles)]
+        starts = [pl.multiple_of((e * tiles + i) * 8, 8) for i in range(tiles)]
         apart = pl.ds(e, n_src * left, stride=count)
-        taken = [x[at, :].astype(jnp.float32) for x in xs for at in own]
+        taken = [x[pl.ds(at, 8), :].astype(jnp.float32) for x in xs for at in starts]
         taken.append(jnp.concatenate([into[j, apart, :] for j in range(width // LANES)], axis=1))
         taken = jnp.concatenate(taken, axis=0).astype(jnp.bfloat16)
         gate_pre = jnp.dot(taken, wg[e], preferred_element_type=jnp.float32)
@@ -235,9 +240,12 @@
         activated = clamped_unit(gate_pre, upward).astype(jnp.bfloat16)
         result = jnp.dot(activated, wd[e], preferred_element_type=jnp.float32)
         row = 0
-        for out in outs:
-            for at in own:
-                out[at, :] = result[row : row + 8].astype(out.dtype)
+        for s, out in enumerate(outs):
+            block, d = divmod(s, n_sp)
+            for at in starts:
+                part = result[row : row + 8].astype(out.dtype)
+                out[pl.ds(at, 8), :] = part[:, :apart_from]
+                sums[block][pl.ds(pl.multiple_of(d * rows + at, 8), 8), :] = part[:, apart_from:]
                 row += 8
         for j in range(width // LANES):
             outof[j, apart, :] = result[row:, j * LANES : (j + 1) * LANES]
@@ -245,33 +253,63 @@
 
     lax.fori_loop(0, count, one, 0, unroll=EXPERT_UNROLL)
     for s, out in enumerate(outs):
+        block, d = divmod(s, n_sp)
         for j in range(width // LANES):
-            cols = slice(j * LANES, (j + 1) * LANES)
-            out[whole:, cols] = outof[j, s * left * count : (s + 1) * left * count, :].astype(
-                out.dtype
-            )
+            part = outof[j, s * left * count : (s + 1) * left * count, :].astype(out.dtype)
+            first = j * LANES
+            if first < apart_from:
+                out[whole:, first : first + LANES] = part
+            else:
+                first -= apart_from
+                sums[block][d * rows + whole : (d + 1) * rows, first : first + LANES] = part
 
 
 EXPERT_UNROLL = 2
 
 
-def experts(xs, w_gate, w_up, w_down):
+def experts(xs, w_gate, w_up, w_down, n_sp, apart_from):
     count, width, hidden = w_gate.shape
     rows, n_src = xs[0].shape[0], len(xs)
+    blocks = n_src // n_sp
     left = rows // count % 8
     scratch = pltpu.VMEM((width // LANES, n_src * left * count, LANES), jnp.float32)
+    out = jax.ShapeDtypeStruct((rows, apart_from), jnp.bfloat16)
+    summed = jax.ShapeDtypeStruct((n_sp * rows, width - apart_from), jnp.bfloat16)
     flops = 6 * n_src * rows * width * hidden
     moved_bytes = 3 * count * width * hidden * 2 + 4 * n_src * rows * width
-    return pl.pallas_call(
-        lambda *refs: experts_body(n_src, *refs),
+    cost = pl.CostEstimate(flops=flops, bytes_accessed=moved_bytes, transcendentals=0)
+    outs = pl.pallas_call(
+        lambda *refs: experts_body(n_src, n_sp, *refs),
         in_specs=[IN_VMEM] * (n_src + 3),
-        out_specs=[IN_VMEM] * n_src,
-        out_shape=[jax.ShapeDtypeStruct((rows, width), jnp.bfloat16)] * n_src,
+        out_specs=[IN_VMEM] * (n_src + blocks),
+        out_shape=[out] * n_src + [summed] * blocks,
         scratch_shapes=[scratch, scratch],
-        cost_estimate=pl.CostEstimate(flops=flops, bytes_accessed=moved_bytes, transcendentals=0),
+        cost_estimate=cost,
         compiler_params=pltpu.CompilerParams(vmem_limit_bytes=6 << 20),
         name="experts",
     )(*xs, w_gate, w_up, w_down)
+    return outs[:n_src], outs[n_src:]
+
+
+def join_body(n_in, *refs):
+    total = sum(x[...].astype(jnp.float32) for x in refs[:n_in])
+    outs = refs[n_in:]
+    rows = outs[0].shape[0]
+    for i, out in enumerate(outs):
+        out[...] = total[i * rows : (i + 1) * rows].astype(out.dtype)
+
+
+def join(arrays, pieces=1):
+    rows, width = arrays[0].shape
+    out = jax.ShapeDtypeStruct((rows // pieces, width), arrays[0].dtype)
+    return pl.pallas_call(
+        lambda *refs: join_body(len(arrays), *refs),
+        in_specs=[IN_VMEM] * len(arrays),
+        out_specs=[IN_VMEM] * pieces,
+        out_shape=[out] * pieces,
+        compiler_params=pltpu.CompilerParams(vmem_limit_bytes=6 << 20),
+        name="join",
+    )(*arrays)
 
 
 def plain_path(
@@ -613,12 +651,25 @@
     for at, k in enumerate(order):
         rows = pick(at, slot, blocks[k], n_sp, slot_rows)
         arrived.append([moved(x, "sp", d) if d else x for d, x in enumerate(rows)])
+    apart_from = apart_column(resid_in.shape[1])
+    sums = []
     for first, stop in groups_of(n_tp):
         group = arrived[first:stop]
-        terms = experts([x for xs in group for x in xs], *weights)
+        xs = [x for xs in group for x in xs]
+        terms, summed = experts(xs, *weights, n_sp, apart_from)
+        sums += summed
         for at in range(first, stop):
             back = terms[(at - first) * n_sp : (at - first + 1) * n_sp]
             backs[at] = [moved(x, "sp", d, True) if d else x for d, x in enumerate(back)]
+    passed = {}
+    for at in return_order(n_tp)[:-1]:
+        k = order[at]
+        by = -1 if k <= far else 1
+        inner = k < far or k > far + 1
+        part = join([sums[at], passed.pop(k - by)])[0] if inner else sums[at]
+        passed[k] = rotated(part, "tp", by)
+    apart = join([sums[0], *passed.values()], n_sp)
+    apart = [moved(x, "sp", d, True) if d else x for d, x in enumerate(apart)]
     for at in return_order(n_tp)[:-1]:
         k = order[at]
         by = -1 if k <= far else 1
@@ -626,7 +677,9 @@
         joined = [parts.pop(k - by)] if inner else []
         part = combine(at, by_row, weight, backs[at], joined)
         parts[k] = rotated(part, "tp", by)
-    return finish(0, by_row, weight, residual, post_gain, backs[0], list(parts.values()))
+    return finish(
+        0, by_row, weight, residual, post_gain, backs[0], apart, list(parts.values())
+    )
 
 
 def per_device(*args):
@@ -640,6 +693,14 @@
 def groups_of(n_tp):
     first = min(2, n_tp)
     return [(0, first)] + [(at, at + 1) for at in range(first, n_tp)]
+
+
+def apart_column(width):
+    step = 2 * LANES
+    return width - width // (APART * step) * step
+
+
+APART = 4
 
 
 def return_order(n_tp):

time: 178 us -> 169 us (0.949)
  starting transfers between devices: 61.3 us -> 56.2 us
  waiting for transfers between devices: 75.9 us -> 72.2 us
    ppermute x24 -> x27, waiting for transfers between devices: 42.8 us -> 21.6 us  [moved(): return lax.ppermute(x, axis, [(b, a) for a, b in pairs] if back else pairs)]
    ppermute x9 -> x12, waiting for transfers between devices: 33 us -> 50.5 us  [rotated(): return lax.ppermute(x, axis, [(i, (i + by) % size) for i in range(size)])]
    ppermute x9 -> x12, starting transfers between devices: 39.5 us -> 34.1 us  [rotated(): return lax.ppermute(x, axis, [(i, (i + by) % size) for i in range(size)])]
    ppermute x24 -> x27, starting transfers between devices: 18.5 us -> 18.9 us  [moved(): return lax.ppermute(x, axis, [(b, a) for a, b in pairs] if back else pairs)]
    pallas_call x3 -> x5, Pallas kernels: 16.7 us -> 16.9 us  [the longest x3 16.7 us: experts(): pl.pallas_call(lambda *refs: experts_body(n_src, n_sp, *refs), in_specs=[...]
  transfers between devices with their start and end apart: 37 -> 43, of which waited for: 13 -> 15; matrix products, arithmetic and copies ran while one was open for 0% -> 0% of each run, Pallas kernels for 19% -> 19%
where the time goes in v5:
time: 169 us; the launch traced here: 168 us
  waiting for transfers between devices  72.2 us (43%)
  starting transfers between devices  56.2 us (33%)
  Pallas kernels  38.4 us (23%)
    ppermute x12, waiting for transfers between devices, rotated(): return lax.ppermute(x, axis, [(i, (i + by) % size) for i in range(size)])  50.5 us
    ppermute x12, starting transfers between devices, rotated(): return lax.ppermute(x, axis, [(i, (i + by) % size) for i in range(size)])  34.1 us
    ppermute x27, waiting for transfers between devices, moved(): return lax.ppermute(x, axis, [(b, a) for a, b in pairs] if back else pairs)  21.6 us
    ppermute x27, starting transfers between devices, moved(): return lax.ppermute(x, axis, [(b, a) for a, b in pairs] if back else pairs)  18.9 us
    pallas_call x3, Pallas kernels, experts(): pl.pallas_call(lambda *refs: experts_body(n_src, n_sp, *refs), in_specs=[...  16.7 us
    pallas_call x2, Pallas kernels, load(): pl.pallas_call(load_body, in_specs=[pl.BlockSpec(memory_space=pltpu.HBM)]...  11.1 us
  transfers between devices with their start and end apart: 43, of which 15 were waited for; matrix products, arithmetic and copies ran while one was open for 0% of the time, Pallas kernels for 19%

profile of v5, /device:TPU:0, one launch (start us, length us, event | category | flops | bytes accessed | tf_op | source)
XLA Modules:
  0.0 168.5 jit_solution(6658835517704814501)
XLA Ops:
  0.6 1.8 %cut.1 = (bf16[152,256]{1,0:T(8,128)(2,1)S(1)}, bf16[152,256]{1,0:T(8,128)(2,1)S(1)}, bf16[152,256]{1,0:T(8,128)(2,1)S(1)}, bf16[152,256]{1,0:T(8,128)(2,1)S(1)}, bf16[16,256]{1,0:T(8,128)(2,1)S(1)}) custom-call(s32[2]{0:T(128)} %pad_add_fusion.place.refs_0_, bf16[512,256]{1,0:T(8,128)(2,1)} %x.1, s32[2,128]{1,0:T(2,128)} %bitcast.12, f32[2,128]{1,0:T(2,128)} %bitcast.13), custom_call_target="tpu_custom_call" | custom-call | tf_op jit(solution)/shard_map/cut/pallas_call | solution.py:449
  2.4 3.1 %collective-permute-start = (bf16[152,256]{1,0:T(8,128)(2,1)S(1)}, bf16[152,256]{1,0:T(8,128)(2,1)S(1)}, u32[]{:S(2)}, u32[]{:S(2)}) collective-permute-start(bf16[152,256]{1,0:T(8,128)(2,1)S(1)} %get-tuple-element.65), channel_id=1, source_target_pairs={{0,1},{1,2},{2,3},{3,0},{4,5},{5,6},{6,7},{7,4},{8,9},{9,10},{10,1... | collective-permute-start | bytes 233480 | tf_op jit(solution)/shard_map/ppermute | solution.py:30
  5.5 2.6 %collective-permute-start.1 = (bf16[152,256]{1,0:T(8,128)(2,1)S(1)}, bf16[152,256]{1,0:T(8,128)(2,1)S(1)}, u32[]{:S(2)}, u32[]{:S(2)}) collective-permute-start(bf16[152,256]{1,0:T(8,128)(2,1)S(1)} %get-tuple-element.66), channel_id=1, source_target_pairs={{0,2},{1,3},{2,0},{3,1},{4,6},{5,7},{6,4},{7,5},{8,10},{9,11},{10,... | collective-permute-start | bytes 233480 | tf_op jit(solution)/shard_map/ppermute | solution.py:30
  12.9 2.7 %load.2 = (f32[1,1024]{1,0:T(1,128)S(1)}, f32[1,2048]{1,0:T(1,128)S(1)}, f32[1,2048]{1,0:T(1,128)S(1)}, bf16[4,256,256]{2,1,0:T(8,128)(2,1)S(1)}, bf16[1024,2048...) custom-call(f32[1,1024]{1,0:T(1,128)} %bitcast.11, f32[1,2048]{1,0:T(1,128)} %bitcast.9, f32[1,2048]{1,0:T(1,128)} %bitcast.10, ...), custom_call_target="tpu_custom_call" | custom-call | tf_op jit(solution)/shard_map/load/pallas_call | solution.py:106
  16.3 2.0 %mix.1 = (bf16[128,2048]{1,0:T(8,128)(2,1)S(1)}, bf16[128,2048]{1,0:T(8,128)(2,1)S(1)}) custom-call(s32[2]{0:T(128)S(1)} %copy-done.1, bf16[152,256]{1,0:T(8,128)(2,1)S(1)} %get-tuple-element.64.refs_1_, bf16[152,256]{1,0:T(8,128)(2,1)S(1)} %collective-permute-done.refs_2_, bf16[152,256]{1,0:T(8,128)(2,1)S(1)} %collective-permute-done.1.refs_3_, ...), custom_call_target="tpu_custom_call" | custom-call | tf_op jit(solution)/shard_map/mix/pallas_call | solution.py:524
  18.3 5.7 %collective-permute-start.10 = (bf16[128,2048]{1,0:T(8,128)(2,1)S(1)}, bf16[128,2048]{1,0:T(8,128)(2,1)S(1)}, u32[]{:S(2)}, u32[]{:S(2)}) collective-permute-start(bf16[128,2048]{1,0:T(8,128)(2,1)S(1)} %get-tuple-element.79.refs_1_), channel_id=1, source_target_pairs={{0,1},{1,2},{2,3},{3,0},{4,5},{5,6},{6,7},{7,4},{8,9},{9,10},{10,1... | collective-permute-start | bytes 1572872 | tf_op jit(solution)/shard_map/ppermute | solution.py:30
  24.0 15.9 %collective-permute-done.10.refs_1_ = bf16[128,2048]{1,0:T(8,128)(2,1)S(1)} collective-permute-done((bf16[128,2048]{1,0:T(8,128)(2,1)S(1)}, bf16[128,2048]{1,0:T(8,128)(2,1)S(1)}, u32[]{:S(2)}, u32[]{:S(2)}) %collective-permute-start.10) | collective-permute-done | bytes 524320 | tf_op jit(solution)/shard_map/ppermute | solution.py:30
  39.9 3.8 %collective-permute-start.17 = (bf16[128,2048]{1,0:T(8,128)(2,1)S(1)}, bf16[128,2048]{1,0:T(8,128)(2,1)S(1)}, u32[]{:S(2)}, u32[]{:S(2)}) collective-permute-start(bf16[128,2048]{1,0:T(8,128)(2,1)S(1)} %get-tuple-element.79.refs_1_), channel_id=1, source_target_pairs={{0,3},{1,0},{2,1},{3,2},{4,7},{5,4},{6,5},{7,6},{8,11},{9,8},{10,9... | collective-permute-start | bytes 1572872 | tf_op jit(solution)/shard_map/ppermute | solution.py:30
  48.0 8.2 %collective-permute-done.22.refs_1_ = bf16[128,2048]{1,0:T(8,128)(2,1)S(1)} collective-permute-done((bf16[128,2048]{1,0:T(8,128)(2,1)S(1)}, bf16[128,2048]{1,0:T(8,128)(2,1)S(1)}, u32[]{:S(2)}, u32[]{:S(2)}) %collective-permute-start.22) | collective-permute-done | bytes 524320 | tf_op jit(solution)/shard_map/ppermute | solution.py:30
  57.4 1.8 %collective-permute-start.24 = (bf16[72,2048]{1,0:T(8,128)(2,1)S(1)}, bf16[72,2048]{1,0:T(8,128)(2,1)S(1)}, u32[]{:S(2)}, u32[]{:S(2)}) collective-permute-start(bf16[72,2048]{1,0:T(8,128)(2,1)S(1)} %get-tuple-element.104), channel_id=1, source_target_pairs={{0,8},{4,12},{8,0},{12,4},{1,9},{5,13},{9,1},{13,5},{2,10},{6,14},... | collective-permute-start | bytes 884744 | tf_op jit(solution)/shard_map/ppermute | solution.py:76
  59.1 6.4 %collective-permute-done.17.refs_1_ = bf16[128,2048]{1,0:T(8,128)(2,1)S(1)} collective-permute-done((bf16[128,2048]{1,0:T(8,128)(2,1)S(1)}, bf16[128,2048]{1,0:T(8,128)(2,1)S(1)}, u32[]{:S(2)}, u32[]{:S(2)}) %collective-permute-start.17) | collective-permute-done | bytes 524320 | tf_op jit(solution)/shard_map/ppermute | solution.py:30
  66.6 1.7 %collective-permute-start.19 = (bf16[72,2048]{1,0:T(8,128)(2,1)S(1)}, bf16[72,2048]{1,0:T(8,128)(2,1)S(1)}, u32[]{:S(2)}, u32[]{:S(2)}) collective-permute-start(bf16[72,2048]{1,0:T(8,128)(2,1)S(1)} %get-tuple-element.98), channel_id=1, source_target_pairs={{0,8},{4,12},{8,0},{12,4},{1,9},{5,13},{9,1},{13,5},{2,10},{6,14},... | collective-permute-start | bytes 884744 | tf_op jit(solution)/shard_map/ppermute | solution.py:76
  68.4 1.7 collective-permute-start.12
  70.1 8.4 %load.3 = (bf16[8,2048,256]{2,1,0:T(8,128)(2,1)S(1)}, bf16[8,2048,256]{2,1,0:T(8,128)(2,1)S(1)}, bf16[8,256,2048]{2,1,0:T(8,128)(2,1)S(1)}) custom-call(bf16[8,2048,256]{2,1,0:T(8,128)(2,1)} %refs_0_.1, bf16[8,2048,256]{2,1,0:T(8,128)(2,1)} %refs_1_.1, bf16[8,256,2048]{2,1,0:T(8,128)(2,1)} %refs_2_.1), custom_call_target="tpu_custom_call" | custom-call | tf_op jit(solution)/shard_map/load/pallas_call | solution.py:106
  78.6 5.5 %experts.5 = (bf16[72,1536]{1,0:T(8,128)(2,1)S(1)}, bf16[72,1536]{1,0:T(8,128)(2,1)S(1)}, bf16[72,1536]{1,0:T(8,128)(2,1)S(1)}, bf16[72,1536]{1,0:T(8,128)(2,1)S(1)}, bf16[288,512]{1,0:T(8,128)(2,1)S(1)}) custom-call(bf16[72,2048]{1,0:T(8,128)(2,1)S(1)} %get-tuple-element.102.refs_0_, bf16[72,2048]{1,0:T(8,128)(2,1)S(1)} %collective-permute-done.23.refs_1_, ...), custom_call_target="tpu_custom_call" | custom-call | flops 905969664 | bytes 27525120 | tf_op jit(solution)/shard_map/experts/pallas_call | solution.py:281
  84.6 1.7 collective-permute-start.39
  87.5 5.5 %experts.4 = (bf16[72,1536]{1,0:T(8,128)(2,1)S(1)}, bf16[72,1536]{1,0:T(8,128)(2,1)S(1)}, bf16[72,1536]{1,0:T(8,128)(2,1)S(1)}, bf16[72,1536]{1,0:T(8,128)(2,1)S(1)}, bf16[288,512]{1,0:T(8,128)(2,1)S(1)}) custom-call(bf16[72,2048]{1,0:T(8,128)(2,1)S(1)} %get-tuple-element.96.refs_0_, bf16[72,2048]{1,0:T(8,128)(2,1)S(1)} %collective-permute-done.18.refs_1_, ...), custom_call_target="tpu_custom_call" | custom-call | flops 905969664 | bytes 27525120 | tf_op jit(solution)/shard_map/experts/pallas_call | solution.py:281
  94.5 4.9 %collective-permute-done.13.refs_7_ = bf16[72,2048]{1,0:T(8,128)(2,1)S(1)} collective-permute-done((bf16[72,2048]{1,0:T(8,128)(2,1)S(1)}, bf16[72,2048]{1,0:T(8,128)(2,1)S(1)}, u32[]{:S(2)}, u32[]{:S(2)}) %collective-permute-start.13) | collective-permute-done | bytes 294944 | tf_op jit(solution)/shard_map/ppermute | solution.py:76
  102.0 3.6 %collective-permute-done.39.refs_4_ = bf16[72,1536]{1,0:T(8,128)(2,1)S(1)} collective-permute-done((bf16[72,1536]{1,0:T(8,128)(2,1)S(1)}, bf16[72,1536]{1,0:T(8,128)(2,1)S(1)}, u32[]{:S(2)}, u32[]{:S(2)}) %collective-permute-start.39) | collective-permute-done | bytes 221216 | tf_op jit(solution)/shard_map/ppermute | solution.py:76
  105.6 9.9 %collective-permute-start.26 = (bf16[288,512]{1,0:T(8,128)(2,1)S(1)}, bf16[288,512]{1,0:T(8,128)(2,1)S(1)}, u32[]{:S(2)}, u32[]{:S(2)}) collective-permute-start(bf16[288,512]{1,0:T(8,128)(2,1)S(1)} %get-tuple-element.106), channel_id=1, source_target_pairs={{0,3},{1,0},{2,1},{3,2},{4,7},{5,4},{6,5},{7,6},{8,11},{9,8},{10,9... | collective-permute-start | bytes 884744 | tf_op jit(solution)/shard_map/ppermute | solution.py:30
  115.5 5.7 %experts.3 = (bf16[72,1536]{1,0:T(8,128)(2,1)S(1)}, bf16[72,1536]{1,0:T(8,128)(2,1)S(1)}, bf16[72,1536]{1,0:T(8,128)(2,1)S(1)}, bf16[72,1536]{1,0:T(8,128)(2,1)S...) custom-call(bf16[72,2048]{1,0:T(8,128)(2,1)S(1)} %get-tuple-element., ...), custom_call_target="tpu_custom_call" | custom-call | flops 1811939328 | bytes 29884416 | tf_op jit(solution)/shard_map/experts/pallas_call | solution.py:281
  122.2 1.8 %collective-permute-start.37 = (bf16[72,1536]{1,0:T(8,128)(2,1)S(1)}, bf16[72,1536]{1,0:T(8,128)(2,1)S(1)}, u32[]{:S(2)}, u32[]{:S(2)}) collective-permute-start(bf16[72,1536]{1,0:T(8,128)(2,1)S(1)} %get-tuple-element.118), channel_id=1, source_target_pairs={{12,0},{8,4},{4,8},{0,12},{13,1},{9,5},{5,9},{1,13},{14,2},{10,6},... | collective-permute-start | bytes 663560 | tf_op jit(solution)/shard_map/ppermute | solution.py:76
  124.0 1.7 collective-permute-start.21
  125.7 3.9 %collective-permute-start.27 = (bf16[288,512]{1,0:T(8,128)(2,1)S(1)}, bf16[288,512]{1,0:T(8,128)(2,1)S(1)}, u32[]{:S(2)}, u32[]{:S(2)}) collective-permute-start(bf16[288,512]{1,0:T(8,128)(2,1)S(1)} %join.2), channel_id=1, source_target_pairs={{0,3},{1,0},{2,1},{3,2},{4,7},{5,4},{6,5},{7,6},{8,11},{9,8},{10,9... | collective-permute-start | bytes 884744 | tf_op jit(solution)/shard_map/ppermute | solution.py:30
  130.4 1.9 %collective-permute-start.34 = (bf16[128,1536]{1,0:T(8,128)(2,1)S(1)}, bf16[128,1536]{1,0:T(8,128)(2,1)S(1)}, u32[]{:S(2)}, u32[]{:S(2)}) collective-permute-start(bf16[128,1536]{1,0:T(8,128)(2,1)S(1)} %combine.3), channel_id=1, source_target_pairs={{0,1},{1,2},{2,3},{3,0},{4,5},{5,6},{6,7},{7,4},{8,9},{9,10},{10,1... | collective-permute-start | bytes 1179656 | tf_op jit(solution)/shard_map/ppermute | solution.py:30
  132.4 1.8 %collective-permute-done.37.refs_5_ = bf16[72,1536]{1,0:T(8,128)(2,1)S(1)} collective-permute-done((bf16[72,1536]{1,0:T(8,128)(2,1)S(1)}, bf16[72,1536]{1,0:T(8,128)(2,1)S(1)}, u32[]{:S(2)}, u32[]{:S(2)}) %collective-permute-start.37) | collective-permute-done | bytes 221216 | tf_op jit(solution)/shard_map/ppermute | solution.py:76
  134.2 6.1 %collective-permute-done.41.refs_6_ = bf16[128,1536]{1,0:T(8,128)(2,1)S(1)} collective-permute-done((bf16[128,1536]{1,0:T(8,128)(2,1)S(1)}, bf16[128,1536]{1,0:T(8,128)(2,1)S(1)}, u32[]{:S(2)}, u32[]{:S(2)}) %collective-permute-start.41) | collective-permute-done | bytes 393248 | tf_op jit(solution)/shard_map/ppermute | solution.py:30
  141.3 13.8 %collective-permute-done.27.refs_2_ = bf16[288,512]{1,0:T(8,128)(2,1)S(1)} collective-permute-done((bf16[288,512]{1,0:T(8,128)(2,1)S(1)}, bf16[288,512]{1,0:T(8,128)(2,1)S(1)}, u32[]{:S(2)}, u32[]{:S(2)}) %collective-permute-start.27) | collective-permute-done | bytes 294944 | tf_op jit(solution)/shard_map/ppermute | solution.py:30
  155.4 2.0 %collective-permute-start.29 = (bf16[72,512]{1,0:T(8,128)(2,1)S(1)}, bf16[72,512]{1,0:T(8,128)(2,1)S(1)}, u32[]{:S(2)}, u32[]{:S(2)}) collective-permute-start(bf16[72,512]{1,0:T(8,128)(2,1)S(1)} %get-tuple-element.109), channel_id=1, source_target_pairs={{8,0},{12,4},{0,8},{4,12},{9,1},{13,5},{1,9},{5,13},{10,2},{14,6},... | collective-permute-start | bytes 221192 | tf_op jit(solution)/shard_map/ppermute | solution.py:76
  157.4 5.4 %collective-permute-done.16.refs_7_ = bf16[72,1536]{1,0:T(8,128)(2,1)S(1)} collective-permute-done((bf16[72,1536]{1,0:T(8,128)(2,1)S(1)}, bf16[72,1536]{1,0:T(8,128)(2,1)S(1)}, u32[]{:S(2)}, u32[]{:S(2)}) %collective-permute-start.16) | collective-permute-done | bytes 221216 | tf_op jit(solution)/shard_map/ppermute | solution.py:76
  163.1 3.5 %collective-permute-done.30.refs_11_ = bf16[72,512]{1,0:T(8,128)(2,1)S(1)} collective-permute-done((bf16[72,512]{1,0:T(8,128)(2,1)S(1)}, bf16[72,512]{1,0:T(8,128)(2,1)S(1)}, u32[]{:S(2)}, u32[]{:S(2)}) %collective-permute-start.30) | collective-permute-done | bytes 73760 | tf_op jit(solution)/shard_map/ppermute | solution.py:76
  166.6 1.8 %finish.1 = bf16[128,2048]{1,0:T(8,128)(2,1)} custom-call(s32[4,128,2]{2,1,0:T(8,128)S(1)} %get-tuple-element.68.refs_0_, f32[4,128,2]{2,1,0:T(8,128)S(1)} %get-tuple-element.69.refs_1_, bf16[128,2048]{1,0:T(8,128)(2,1)S(1)} %get-tuple-element.77.refs_2_, f32[1,2048]{1,0:T(1,128)S(1)} %bitcast.8, bf16[72,1536]{1,0:T(8,128)(2,1)S(1)} %get-tuple-element.91.refs_4_, ...), custom_call_target="tpu_custom_call" | custom-call | tf_op jit(solution)/shard_map/finish/pallas_call | solution.py:207
  (77 shorter events, 21.7 us)
Async XLA Ops:
  2.4 13.2 %collective-permute-start = (bf16[152,256]{1,0:T(8,128)(2,1)S(1)}, bf16[152,256]{1,0:T(8,128)(2,1)S(1)}, u32[]{:S(2)}, u32[]{:S(2)}) collective-permute-start(bf16[152,256]{1,0:T(8,128)(2,1)S(1)} %get-tuple-element.65), channel_id=1, source_target_pairs={{0,1},{1,2},{2,3},{3,0},{4,5},{5,6},{6,7},{7,4},{8,9},{9,10},{10,1... | collective-permute-start | bytes 233480 | tf_op jit(solution)/shard_map/ppermute | solution.py:30
  5.5 10.1 %collective-permute-start.1 = (bf16[152,256]{1,0:T(8,128)(2,1)S(1)}, bf16[152,256]{1,0:T(8,128)(2,1)S(1)}, u32[]{:S(2)}, u32[]{:S(2)}) collective-permute-start(bf16[152,256]{1,0:T(8,128)(2,1)S(1)} %get-tuple-element.66), channel_id=1, source_target_pairs={{0,2},{1,3},{2,0},{3,1},{4,6},{5,7},{6,4},{7,5},{8,10},{9,11},{10,... | collective-permute-start | bytes 233480 | tf_op jit(solution)/shard_map/ppermute | solution.py:30
  18.3 21.7 %collective-permute-start.10 = (bf16[128,2048]{1,0:T(8,128)(2,1)S(1)}, bf16[128,2048]{1,0:T(8,128)(2,1)S(1)}, u32[]{:S(2)}, u32[]{:S(2)}) collective-permute-start(bf16[128,2048]{1,0:T(8,128)(2,1)S(1)} %get-tuple-element.79.refs_1_), channel_id=1, source_target_pairs={{0,1},{1,2},{2,3},{3,0},{4,5},{5,6},{6,7},{7,4},{8,9},{9,10},{10,1... | collective-permute-start | bytes 1572872 | tf_op jit(solution)/shard_map/ppermute | solution.py:30
  39.9 16.3 %collective-permute-start.22 = (bf16[128,2048]{1,0:T(8,128)(2,1)S(1)}, bf16[128,2048]{1,0:T(8,128)(2,1)S(1)}, u32[]{:S(2)}, u32[]{:S(2)}) collective-permute-start(bf16[128,2048]{1,0:T(8,128)(2,1)S(1)} %collective-permute-done.10.refs_1_), channel_id=1, source_target_pairs={{0,1},{1,2},{2,3},{3,0},{4,5},{5,6},{6,7},{7,4},{8,9},{9,10},{10,1... | collective-permute-start | bytes 1572872 | tf_op jit(solution)/shard_map/ppermute | solution.py:30
  39.9 25.6 %collective-permute-start.17 = (bf16[128,2048]{1,0:T(8,128)(2,1)S(1)}, bf16[128,2048]{1,0:T(8,128)(2,1)S(1)}, u32[]{:S(2)}, u32[]{:S(2)}) collective-permute-start(bf16[128,2048]{1,0:T(8,128)(2,1)S(1)} %get-tuple-element.79.refs_1_), channel_id=1, source_target_pairs={{0,3},{1,0},{2,1},{3,2},{4,7},{5,4},{6,5},{7,6},{8,11},{9,8},{10,9... | collective-permute-start | bytes 1572872 | tf_op jit(solution)/shard_map/ppermute | solution.py:30
  45.2 12.1 %collective-permute-start.7 = (bf16[72,2048]{1,0:T(8,128)(2,1)S(1)}, bf16[72,2048]{1,0:T(8,128)(2,1)S(1)}, u32[]{:S(2)}, u32[]{:S(2)}) collective-permute-start(bf16[72,2048]{1,0:T(8,128)(2,1)S(1)} %get-tuple-element.81), channel_id=1, source_target_pairs={{0,4},{4,0},{8,12},{12,8},{1,5},{5,1},{9,13},{13,9},{2,6},{6,2},{1... | collective-permute-start | bytes 884744 | tf_op jit(solution)/shard_map/ppermute | solution.py:76
  46.1 11.3 %collective-permute-start.8 = (bf16[72,2048]{1,0:T(8,128)(2,1)S(1)}, bf16[72,2048]{1,0:T(8,128)(2,1)S(1)}, u32[]{:S(2)}, u32[]{:S(2)}) collective-permute-start(bf16[72,2048]{1,0:T(8,128)(2,1)S(1)} %get-tuple-element.82), channel_id=1, source_target_pairs={{0,8},{4,12},{8,0},{12,4},{1,9},{5,13},{9,1},{13,5},{2,10},{6,14},... | collective-permute-start | bytes 884744 | tf_op jit(solution)/shard_map/ppermute | solution.py:76
  46.9 19.1 %collective-permute-start.9 = (bf16[72,2048]{1,0:T(8,128)(2,1)S(1)}, bf16[72,2048]{1,0:T(8,128)(2,1)S(1)}, u32[]{:S(2)}, u32[]{:S(2)}) collective-permute-start(bf16[72,2048]{1,0:T(8,128)(2,1)S(1)} %get-tuple-element.83), channel_id=1, source_target_pairs={{0,12},{4,8},{8,4},{12,0},{1,13},{5,9},{9,5},{13,1},{2,14},{6,10},... | collective-permute-start | bytes 884744 | tf_op jit(solution)/shard_map/ppermute | solution.py:76
  56.2 10.4 %collective-permute-start.11 = (bf16[72,2048]{1,0:T(8,128)(2,1)S(1)}, bf16[72,2048]{1,0:T(8,128)(2,1)S(1)}, u32[]{:S(2)}, u32[]{:S(2)}) collective-permute-start(bf16[72,2048]{1,0:T(8,128)(2,1)S(1)} %get-tuple-element.85), channel_id=1, source_target_pairs={{0,4},{4,0},{8,12},{12,8},{1,5},{5,1},{9,13},{13,9},{2,6},{6,2},{1... | collective-permute-start | bytes 884744 | tf_op jit(solution)/shard_map/ppermute | solution.py:76
  57.3 11.0 %collective-permute-start.23 = (bf16[72,2048]{1,0:T(8,128)(2,1)S(1)}, bf16[72,2048]{1,0:T(8,128)(2,1)S(1)}, u32[]{:S(2)}, u32[]{:S(2)}) collective-permute-start(bf16[72,2048]{1,0:T(8,128)(2,1)S(1)} %get-tuple-element.103), channel_id=1, source_target_pairs={{0,4},{4,0},{8,12},{12,8},{1,5},{5,1},{9,13},{13,9},{2,6},{6,2},{1... | collective-permute-start | bytes 884744 | tf_op jit(solution)/shard_map/ppermute | solution.py:76
  57.4 11.1 %collective-permute-start.24 = (bf16[72,2048]{1,0:T(8,128)(2,1)S(1)}, bf16[72,2048]{1,0:T(8,128)(2,1)S(1)}, u32[]{:S(2)}, u32[]{:S(2)}) collective-permute-start(bf16[72,2048]{1,0:T(8,128)(2,1)S(1)} %get-tuple-element.104), channel_id=1, source_target_pairs={{0,8},{4,12},{8,0},{12,4},{1,9},{5,13},{9,1},{13,5},{2,10},{6,14},... | collective-permute-start | bytes 884744 | tf_op jit(solution)/shard_map/ppermute | solution.py:76
  65.5 13.0 %collective-permute-start.25 = (bf16[72,2048]{1,0:T(8,128)(2,1)S(1)}, bf16[72,2048]{1,0:T(8,128)(2,1)S(1)}, u32[]{:S(2)}, u32[]{:S(2)}) collective-permute-start(bf16[72,2048]{1,0:T(8,128)(2,1)S(1)} %get-tuple-element.105), channel_id=1, source_target_pairs={{0,12},{4,8},{8,4},{12,0},{1,13},{5,9},{9,5},{13,1},{2,14},{6,10},... | collective-permute-start | bytes 884744 | tf_op jit(solution)/shard_map/ppermute | solution.py:76
  66.0 18.1 %collective-permute-start.18 = (bf16[72,2048]{1,0:T(8,128)(2,1)S(1)}, bf16[72,2048]{1,0:T(8,128)(2,1)S(1)}, u32[]{:S(2)}, u32[]{:S(2)}) collective-permute-start(bf16[72,2048]{1,0:T(8,128)(2,1)S(1)} %get-tuple-element.97), channel_id=1, source_target_pairs={{0,4},{4,0},{8,12},{12,8},{1,5},{5,1},{9,13},{13,9},{2,6},{6,2},{1... | collective-permute-start | bytes 884744 | tf_op jit(solution)/shard_map/ppermute | solution.py:76
  66.6 18.0 %collective-permute-start.19 = (bf16[72,2048]{1,0:T(8,128)(2,1)S(1)}, bf16[72,2048]{1,0:T(8,128)(2,1)S(1)}, u32[]{:S(2)}, u32[]{:S(2)}) collective-permute-start(bf16[72,2048]{1,0:T(8,128)(2,1)S(1)} %get-tuple-element.98), channel_id=1, source_target_pairs={{0,8},{4,12},{8,0},{12,4},{1,9},{5,13},{9,1},{13,5},{2,10},{6,14},... | collective-permute-start | bytes 884744 | tf_op jit(solution)/shard_map/ppermute | solution.py:76
  68.3 18.4 %collective-permute-start.20 = (bf16[72,2048]{1,0:T(8,128)(2,1)S(1)}, bf16[72,2048]{1,0:T(8,128)(2,1)S(1)}, u32[]{:S(2)}, u32[]{:S(2)}) collective-permute-start(bf16[72,2048]{1,0:T(8,128)(2,1)S(1)} %get-tuple-element.99), channel_id=1, source_target_pairs={{0,12},{4,8},{8,4},{12,0},{1,13},{5,9},{9,5},{13,1},{2,14},{6,10},... | collective-permute-start | bytes 884744 | tf_op jit(solution)/shard_map/ppermute | solution.py:76
  68.4 26.1 %collective-permute-start.12 = (bf16[72,2048]{1,0:T(8,128)(2,1)S(1)}, bf16[72,2048]{1,0:T(8,128)(2,1)S(1)}, u32[]{:S(2)}, u32[]{:S(2)}) collective-permute-start(bf16[72,2048]{1,0:T(8,128)(2,1)S(1)} %get-tuple-element.86), channel_id=1, source_target_pairs={{0,8},{4,12},{8,0},{12,4},{1,9},{5,13},{9,1},{13,5},{2,10},{6,14},... | collective-permute-start | bytes 884744 | tf_op jit(solution)/shard_map/ppermute | solution.py:76
  78.5 20.9 %collective-permute-start.13 = (bf16[72,2048]{1,0:T(8,128)(2,1)S(1)}, bf16[72,2048]{1,0:T(8,128)(2,1)S(1)}, u32[]{:S(2)}, u32[]{:S(2)}) collective-permute-start(bf16[72,2048]{1,0:T(8,128)(2,1)S(1)} %get-tuple-element.87), channel_id=1, source_target_pairs={{0,12},{4,8},{8,4},{12,0},{1,13},{5,9},{9,5},{13,1},{2,14},{6,10},... | collective-permute-start | bytes 884744 | tf_op jit(solution)/shard_map/ppermute | solution.py:76
  84.1 16.3 %collective-permute-start.38 = (bf16[72,1536]{1,0:T(8,128)(2,1)S(1)}, bf16[72,1536]{1,0:T(8,128)(2,1)S(1)}, u32[]{:S(2)}, u32[]{:S(2)}) collective-permute-start(bf16[72,1536]{1,0:T(8,128)(2,1)S(1)} %get-tuple-element.120), channel_id=1, source_target_pairs={{4,0},{0,4},{12,8},{8,12},{5,1},{1,5},{13,9},{9,13},{6,2},{2,6},{1... | collective-permute-start | bytes 663560 | tf_op jit(solution)/shard_map/ppermute | solution.py:76
  84.6 20.9 %collective-permute-start.39 = (bf16[72,1536]{1,0:T(8,128)(2,1)S(1)}, bf16[72,1536]{1,0:T(8,128)(2,1)S(1)}, u32[]{:S(2)}, u32[]{:S(2)}) collective-permute-start(bf16[72,1536]{1,0:T(8,128)(2,1)S(1)} %get-tuple-element.121), channel_id=1, source_target_pairs={{8,0},{12,4},{0,8},{4,12},{9,1},{13,5},{1,9},{5,13},{10,2},{14,6},... | collective-permute-start | bytes 663560 | tf_op jit(solution)/shard_map/ppermute | solution.py:76
  86.7 34.5 %collective-permute-start.40 = (bf16[72,1536]{1,0:T(8,128)(2,1)S(1)}, bf16[72,1536]{1,0:T(8,128)(2,1)S(1)}, u32[]{:S(2)}, u32[]{:S(2)}) collective-permute-start(bf16[72,1536]{1,0:T(8,128)(2,1)S(1)} %get-tuple-element.122), channel_id=1, source_target_pairs={{12,0},{8,4},{4,8},{0,12},{13,1},{9,5},{5,9},{1,13},{14,2},{10,6},... | collective-permute-start | bytes 663560 | tf_op jit(solution)/shard_map/ppermute | solution.py:76
  94.5 27.5 %collective-permute-start.31 = (bf16[72,1536]{1,0:T(8,128)(2,1)S(1)}, bf16[72,1536]{1,0:T(8,128)(2,1)S(1)}, u32[]{:S(2)}, u32[]{:S(2)}) collective-permute-start(bf16[72,1536]{1,0:T(8,128)(2,1)S(1)} %get-tuple-element.112), channel_id=1, source_target_pairs={{4,0},{0,4},{12,8},{8,12},{5,1},{1,5},{13,9},{9,13},{6,2},{2,6},{1... | collective-permute-start | bytes 663560 | tf_op jit(solution)/shard_map/ppermute | solution.py:76
  99.4 22.7 %collective-permute-start.32 = (bf16[72,1536]{1,0:T(8,128)(2,1)S(1)}, bf16[72,1536]{1,0:T(8,128)(2,1)S(1)}, u32[]{:S(2)}, u32[]{:S(2)}) collective-permute-start(bf16[72,1536]{1,0:T(8,128)(2,1)S(1)} %get-tuple-element.113), channel_id=1, source_target_pairs={{8,0},{12,4},{0,8},{4,12},{9,1},{13,5},{1,9},{5,13},{10,2},{14,6},... | collective-permute-start | bytes 663560 | tf_op jit(solution)/shard_map/ppermute | solution.py:76
  100.4 21.7 %collective-permute-start.33 = (bf16[72,1536]{1,0:T(8,128)(2,1)S(1)}, bf16[72,1536]{1,0:T(8,128)(2,1)S(1)}, u32[]{:S(2)}, u32[]{:S(2)}) collective-permute-start(bf16[72,1536]{1,0:T(8,128)(2,1)S(1)} %get-tuple-element.114), channel_id=1, source_target_pairs={{12,0},{8,4},{4,8},{0,12},{13,1},{9,5},{5,9},{1,13},{14,2},{10,6},... | collective-permute-start | bytes 663560 | tf_op jit(solution)/shard_map/ppermute | solution.py:76
  105.6 18.4 %collective-permute-start.26 = (bf16[288,512]{1,0:T(8,128)(2,1)S(1)}, bf16[288,512]{1,0:T(8,128)(2,1)S(1)}, u32[]{:S(2)}, u32[]{:S(2)}) collective-permute-start(bf16[288,512]{1,0:T(8,128)(2,1)S(1)} %get-tuple-element.106), channel_id=1, source_target_pairs={{0,3},{1,0},{2,1},{3,2},{4,7},{5,4},{6,5},{7,6},{8,11},{9,8},{10,9... | collective-permute-start | bytes 884744 | tf_op jit(solution)/shard_map/ppermute | solution.py:30
  122.0 18.4 %collective-permute-start.41 = (bf16[128,1536]{1,0:T(8,128)(2,1)S(1)}, bf16[128,1536]{1,0:T(8,128)(2,1)S(1)}, u32[]{:S(2)}, u32[]{:S(2)}) collective-permute-start(bf16[128,1536]{1,0:T(8,128)(2,1)S(1)} %combine.4), channel_id=1, source_target_pairs={{0,3},{1,0},{2,1},{3,2},{4,7},{5,4},{6,5},{7,6},{8,11},{9,8},{10,9... | collective-permute-start | bytes 1179656 | tf_op jit(solution)/shard_map/ppermute | solution.py:30
  122.2 12.1 %collective-permute-start.37 = (bf16[72,1536]{1,0:T(8,128)(2,1)S(1)}, bf16[72,1536]{1,0:T(8,128)(2,1)S(1)}, u32[]{:S(2)}, u32[]{:S(2)}) collective-permute-start(bf16[72,1536]{1,0:T(8,128)(2,1)S(1)} %get-tuple-element.118), channel_id=1, source_target_pairs={{12,0},{8,4},{4,8},{0,12},{13,1},{9,5},{5,9},{1,13},{14,2},{10,6},... | collective-permute-start | bytes 663560 | tf_op jit(solution)/shard_map/ppermute | solution.py:76
  124.0 17.2 %collective-permute-start.21 = (bf16[288,512]{1,0:T(8,128)(2,1)S(1)}, bf16[288,512]{1,0:T(8,128)(2,1)S(1)}, u32[]{:S(2)}, u32[]{:S(2)}) collective-permute-start(bf16[288,512]{1,0:T(8,128)(2,1)S(1)} %get-tuple-element.100), channel_id=1, source_target_pairs={{0,1},{1,2},{2,3},{3,0},{4,5},{5,6},{6,7},{7,4},{8,9},{9,10},{10,1... | collective-permute-start | bytes 884744 | tf_op jit(solution)/shard_map/ppermute | solution.py:30
  125.7 29.4 %collective-permute-start.27 = (bf16[288,512]{1,0:T(8,128)(2,1)S(1)}, bf16[288,512]{1,0:T(8,128)(2,1)S(1)}, u32[]{:S(2)}, u32[]{:S(2)}) collective-permute-start(bf16[288,512]{1,0:T(8,128)(2,1)S(1)} %join.2), channel_id=1, source_target_pairs={{0,3},{1,0},{2,1},{3,2},{4,7},{5,4},{6,5},{7,6},{8,11},{9,8},{10,9... | collective-permute-start | bytes 884744 | tf_op jit(solution)/shard_map/ppermute | solution.py:30
  130.4 32.4 %collective-permute-start.34 = (bf16[128,1536]{1,0:T(8,128)(2,1)S(1)}, bf16[128,1536]{1,0:T(8,128)(2,1)S(1)}, u32[]{:S(2)}, u32[]{:S(2)}) collective-permute-start(bf16[128,1536]{1,0:T(8,128)(2,1)S(1)} %combine.3), channel_id=1, source_target_pairs={{0,1},{1,2},{2,3},{3,0},{4,5},{5,6},{6,7},{7,4},{8,9},{9,10},{10,1... | collective-permute-start | bytes 1179656 | tf_op jit(solution)/shard_map/ppermute | solution.py:30
  141.0 25.6 %collective-permute-start.42 = (bf16[128,1536]{1,0:T(8,128)(2,1)S(1)}, bf16[128,1536]{1,0:T(8,128)(2,1)S(1)}, u32[]{:S(2)}, u32[]{:S(2)}) collective-permute-start(bf16[128,1536]{1,0:T(8,128)(2,1)S(1)} %combine.5), channel_id=1, source_target_pairs={{0,3},{1,0},{2,1},{3,2},{4,7},{5,4},{6,5},{7,6},{8,11},{9,8},{10,9... | collective-permute-start | bytes 1179656 | tf_op jit(solution)/shard_map/ppermute | solution.py:30
  141.1 14.1 %collective-permute-start.14 = (bf16[72,1536]{1,0:T(8,128)(2,1)S(1)}, bf16[72,1536]{1,0:T(8,128)(2,1)S(1)}, u32[]{:S(2)}, u32[]{:S(2)}) collective-permute-start(bf16[72,1536]{1,0:T(8,128)(2,1)S(1)} %get-tuple-element.92), channel_id=1, source_target_pairs={{4,0},{0,4},{12,8},{8,12},{5,1},{1,5},{13,9},{9,13},{6,2},{2,6},{1... | collective-permute-start | bytes 663560 | tf_op jit(solution)/shard_map/ppermute | solution.py:76
  141.2 14.2 %collective-permute-start.15 = (bf16[72,1536]{1,0:T(8,128)(2,1)S(1)}, bf16[72,1536]{1,0:T(8,128)(2,1)S(1)}, u32[]{:S(2)}, u32[]{:S(2)}) collective-permute-start(bf16[72,1536]{1,0:T(8,128)(2,1)S(1)} %get-tuple-element.93), channel_id=1, source_target_pairs={{8,0},{12,4},{0,8},{4,12},{9,1},{13,5},{1,9},{5,13},{10,2},{14,6},... | collective-permute-start | bytes 663560 | tf_op jit(solution)/shard_map/ppermute | solution.py:76
  (13 other events, 109.9 us)

commit v6 on v5

--- a/solution.py
+++ b/solution.py
@@ -424,7 +424,7 @@
     n_tp, (top, rows) = len(chunks), routes.shape
     moves = [(routes, own_routes), (weights, own_weights)]
     for k, chunk in enumerate(chunks):
-        first = (place[0] + k) % n_tp * rows
+        first = (place[0] % n_tp + k) % n_tp * rows
         before = pl.multiple_of(jnp.maximum(first - AHEAD, 0), AHEAD)
         first = pl.multiple_of(first, AHEAD)
         moves.append((x.at[pl.ds(first, rows), :], chunk.at[pl.ds(AHEAD, rows), :]))
@@ -468,7 +468,7 @@
     residual, normed, raw, pooled, mix = refs[2 * n_tp + 6 :]
     rows, width = resid.shape
     channels = chunks[0].shape[1]
-    tp, sp = place[0], place[1]
+    tp, sp = place[0] % n_tp, place[0] // n_tp
     for k, chunk in enumerate(chunks):
         source = (tp - k + n_tp) % n_tp
         cols = pl.ds(pl.multiple_of(source * channels, LANES), channels)
@@ -571,7 +571,7 @@
                 (expert // local).astype(jnp.float32) * hit, axis=0, keepdims=True
             ).astype(jnp.int32)
             inside = route.astype(jnp.int32) - owner * local
-            owner = offset_to(owner, place[1], n_sp)
+            owner = offset_to(owner, place[0] // len(chunks), n_sp)
             in_tile = inside * whole + mine
             apart = local * whole + (mine - whole) * local + inside
             found.append(owner * local * CAP + jnp.where(mine < whole, in_tile, apart))
@@ -620,7 +620,7 @@
     local_experts = w_gate.shape[0]
     slot_rows = local_experts * CAP
 
-    place = jnp.stack([lax.axis_index("tp"), lax.axis_index("sp")]).astype(jnp.int32)
+    place = (lax.axis_index("sp") * n_tp + lax.axis_index("tp")).reshape(1)
     *chunks, tail = cut(place, pool_input, routes.T, route_weight.T, n_tp)
     halos = []
     for j in range(n_tp):
@@ -697,15 +697,15 @@
 
 def apart_column(width):
     step = 2 * LANES
-    return width - width // (APART * step) * step
-
-
-APART = 4
+    return width - width * APART // (8 * step) * step
+
+
+APART = 3
 
 
 def return_order(n_tp):
     far = n_tp // 2
-    return list(range(far, 1, -1)) + list(range(n_tp - 1, far, -1)) + list(range(min(2, n_tp)))[::-1]
+    return list(range(far, 0, -1)) + list(range(far + 1, n_tp)) + [0]
 
 
 def solution(mesh):

time: 169 us -> 160 us (0.947)
  waiting for transfers between devices: 72.2 us -> 55.3 us
  starting transfers between devices: 56.2 us -> 67.1 us
  Pallas kernels: 38.4 us -> 36.6 us
    ppermute x12, waiting for transfers between devices: 50.5 us -> 35.9 us  [rotated(): return lax.ppermute(x, axis, [(i, (i + by) % size) for i in range(size)])]
    ppermute x27, starting transfers between devices: 18.9 us -> 25.1 us  [moved(): return lax.ppermute(x, axis, [(b, a) for a, b in pairs] if back else pairs)]
    ppermute x12, starting transfers between devices: 34.1 us -> 38.7 us  [rotated(): return lax.ppermute(x, axis, [(i, (i + by) % size) for i in range(size)])]
    ppermute x27, waiting for transfers between devices: 21.6 us -> 19.2 us  [moved(): return lax.ppermute(x, axis, [(b, a) for a, b in pairs] if back else pairs)]
  transfers between devices with their start and end apart: 43 -> 43, of which waited for: 15 -> 15; matrix products, arithmetic and copies ran while one was open for 0% -> 0% of each run, Pallas kernels for 19% -> 20%
where the time goes in v6:
time: 160 us; the launch traced here: 159 us
  starting transfers between devices  67.1 us (42%)
  waiting for transfers between devices  55.3 us (35%)
  Pallas kernels  36.6 us (23%)
    ppermute x12, starting transfers between devices, rotated(): return lax.ppermute(x, axis, [(i, (i + by) % size) for i in range(size)])  38.7 us
    ppermute x12, waiting for transfers between devices, rotated(): return lax.ppermute(x, axis, [(i, (i + by) % size) for i in range(size)])  35.9 us
    ppermute x27, starting transfers between devices, moved(): return lax.ppermute(x, axis, [(b, a) for a, b in pairs] if back else pairs)  25.1 us
    ppermute x27, waiting for transfers between devices, moved(): return lax.ppermute(x, axis, [(b, a) for a, b in pairs] if back else pairs)  19.2 us
    pallas_call x3, Pallas kernels, experts(): pl.pallas_call(lambda *refs: experts_body(n_src, n_sp, *refs), in_specs=[...  16.7 us
    pallas_call x2, Pallas kernels, load(): pl.pallas_call(load_body, in_specs=[pl.BlockSpec(memory_space=pltpu.HBM)]...  11.1 us
    ppermute x4, starting transfers between devices, kernel_path(): halos.append(lax.ppermute(tail, ('sp', 'tp'), pairs))  3.25 us
  transfers between devices with their start and end apart: 43, of which 15 were waited for; matrix products, arithmetic and copies ran while one was open for 0% of the time, Pallas kernels for 20%

profile of v6, /device:TPU:0, one launch (start us, length us, event | category | flops | bytes accessed | tf_op | source)
XLA Modules:
  0.0 159.3 jit_solution(947951278775234214)
XLA Ops:
  1.1 3.1 %collective-permute-start = (bf16[152,256]{1,0:T(8,128)(2,1)S(1)}, bf16[152,256]{1,0:T(8,128)(2,1)S(1)}, u32[]{:S(2)}, u32[]{:S(2)}) collective-permute-start(bf16[152,256]{1,0:T(8,128)(2,1)S(1)} %get-tuple-element.65), channel_id=1, source_target_pairs={{0,1},{1,2},{2,3},{3,0},{4,5},{5,6},{6,7},{7,4},{8,9},{9,10},{10,1... | collective-permute-start | bytes 233480 | tf_op jit(solution)/shard_map/ppermute | solution.py:30
  4.2 2.6 %collective-permute-start.1 = (bf16[152,256]{1,0:T(8,128)(2,1)S(1)}, bf16[152,256]{1,0:T(8,128)(2,1)S(1)}, u32[]{:S(2)}, u32[]{:S(2)}) collective-permute-start(bf16[152,256]{1,0:T(8,128)(2,1)S(1)} %get-tuple-element.66), channel_id=1, source_target_pairs={{0,2},{1,3},{2,0},{3,1},{4,6},{5,7},{6,4},{7,5},{8,10},{9,11},{10,... | collective-permute-start | bytes 233480 | tf_op jit(solution)/shard_map/ppermute | solution.py:30
  11.6 2.7 %load.2 = (f32[1,1024]{1,0:T(1,128)S(1)}, f32[1,2048]{1,0:T(1,128)S(1)}, f32[1,2048]{1,0:T(1,128)S(1)}, bf16[4,256,256]{2,1,0:T(8,128)(2,1)S(1)}, bf16[1024,2048...) custom-call(f32[1,1024]{1,0:T(1,128)} %bitcast.10, f32[1,2048]{1,0:T(1,128)} %bitcast.8, f32[1,2048]{1,0:T(1,128)} %bitcast.9, ...), custom_call_target="tpu_custom_call" | custom-call | tf_op jit(solution)/shard_map/load/pallas_call | solution.py:106
  15.8 5.7 %collective-permute-start.10 = (bf16[128,2048]{1,0:T(8,128)(2,1)S(1)}, bf16[128,2048]{1,0:T(8,128)(2,1)S(1)}, u32[]{:S(2)}, u32[]{:S(2)}) collective-permute-start(bf16[128,2048]{1,0:T(8,128)(2,1)S(1)} %get-tuple-element.79.refs_1_), channel_id=1, source_target_pairs={{0,1},{1,2},{2,3},{3,0},{4,5},{5,6},{6,7},{7,4},{8,9},{9,10},{10,1... | collective-permute-start | bytes 1572872 | tf_op jit(solution)/shard_map/ppermute | solution.py:30
  21.5 16.0 %collective-permute-done.10.refs_1_ = bf16[128,2048]{1,0:T(8,128)(2,1)S(1)} collective-permute-done((bf16[128,2048]{1,0:T(8,128)(2,1)S(1)}, bf16[128,2048]{1,0:T(8,128)(2,1)S(1)}, u32[]{:S(2)}, u32[]{:S(2)}) %collective-permute-start.10) | collective-permute-done | bytes 524320 | tf_op jit(solution)/shard_map/ppermute | solution.py:30
  37.5 3.8 %collective-permute-start.23 = (bf16[128,2048]{1,0:T(8,128)(2,1)S(1)}, bf16[128,2048]{1,0:T(8,128)(2,1)S(1)}, u32[]{:S(2)}, u32[]{:S(2)}) collective-permute-start(bf16[128,2048]{1,0:T(8,128)(2,1)S(1)} %get-tuple-element.79.refs_1_), channel_id=1, source_target_pairs={{0,3},{1,0},{2,1},{3,2},{4,7},{5,4},{6,5},{7,6},{8,11},{9,8},{10,9... | collective-permute-start | bytes 1572872 | tf_op jit(solution)/shard_map/ppermute | solution.py:30
  45.0 8.7 %collective-permute-done.17.refs_1_ = bf16[128,2048]{1,0:T(8,128)(2,1)S(1)} collective-permute-done((bf16[128,2048]{1,0:T(8,128)(2,1)S(1)}, bf16[128,2048]{1,0:T(8,128)(2,1)S(1)}, u32[]{:S(2)}, u32[]{:S(2)}) %collective-permute-start.17) | collective-permute-done | bytes 524320 | tf_op jit(solution)/shard_map/ppermute | solution.py:30
  54.9 1.8 %collective-permute-start.19 = (bf16[72,2048]{1,0:T(8,128)(2,1)S(1)}, bf16[72,2048]{1,0:T(8,128)(2,1)S(1)}, u32[]{:S(2)}, u32[]{:S(2)}) collective-permute-start(bf16[72,2048]{1,0:T(8,128)(2,1)S(1)} %get-tuple-element.99), channel_id=1, source_target_pairs={{0,8},{4,12},{8,0},{12,4},{1,9},{5,13},{9,1},{13,5},{2,10},{6,14},... | collective-permute-start | bytes 884744 | tf_op jit(solution)/shard_map/ppermute | solution.py:76
  57.5 2.0 %collective-permute-start.20 = (bf16[72,2048]{1,0:T(8,128)(2,1)S(1)}, bf16[72,2048]{1,0:T(8,128)(2,1)S(1)}, u32[]{:S(2)}, u32[]{:S(2)}) collective-permute-start(bf16[72,2048]{1,0:T(8,128)(2,1)S(1)} %get-tuple-element.100), channel_id=1, source_target_pairs={{0,12},{4,8},{8,4},{12,0},{1,13},{5,9},{9,5},{13,1},{2,14},{6,10},... | collective-permute-start | bytes 884744 | tf_op jit(solution)/shard_map/ppermute | solution.py:76
  59.5 3.6 %collective-permute-done.23.refs_1_ = bf16[128,2048]{1,0:T(8,128)(2,1)S(1)} collective-permute-done((bf16[128,2048]{1,0:T(8,128)(2,1)S(1)}, bf16[128,2048]{1,0:T(8,128)(2,1)S(1)}, u32[]{:S(2)}, u32[]{:S(2)}) %collective-permute-start.23) | collective-permute-done | bytes 524320 | tf_op jit(solution)/shard_map/ppermute | solution.py:30
  63.1 1.9 %collective-permute-start.13 = (bf16[72,2048]{1,0:T(8,128)(2,1)S(1)}, bf16[72,2048]{1,0:T(8,128)(2,1)S(1)}, u32[]{:S(2)}, u32[]{:S(2)}) collective-permute-start(bf16[72,2048]{1,0:T(8,128)(2,1)S(1)} %get-tuple-element.87), channel_id=1, source_target_pairs={{0,12},{4,8},{8,4},{12,0},{1,13},{5,9},{9,5},{13,1},{2,14},{6,10},... | collective-permute-start | bytes 884744 | tf_op jit(solution)/shard_map/ppermute | solution.py:76
  65.0 8.4 %load.3 = (bf16[8,2048,256]{2,1,0:T(8,128)(2,1)S(1)}, bf16[8,2048,256]{2,1,0:T(8,128)(2,1)S(1)}, bf16[8,256,2048]{2,1,0:T(8,128)(2,1)S(1)}) custom-call(bf16[8,2048,256]{2,1,0:T(8,128)(2,1)} %refs_0_.1, bf16[8,2048,256]{2,1,0:T(8,128)(2,1)} %refs_1_.1, bf16[8,256,2048]{2,1,0:T(8,128)(2,1)} %refs_2_.1), custom_call_target="tpu_custom_call" | custom-call | tf_op jit(solution)/shard_map/load/pallas_call | solution.py:106
  75.8 5.5 %experts.4 = (bf16[72,1280]{1,0:T(8,128)(2,1)S(1)}, bf16[72,1280]{1,0:T(8,128)(2,1)S(1)}, bf16[72,1280]{1,0:T(8,128)(2,1)S(1)}, bf16[72,1280]{1,0:T(8,128)(2,1)S(1)}, bf16[288,768]{1,0:T(8,128)(2,1)S(1)}) custom-call(bf16[72,2048]{1,0:T(8,128)(2,1)S(1)} %get-tuple-element.97.refs_0_, bf16[72,2048]{1,0:T(8,128)(2,1)S(1)} %collective-permute-done.18.refs_1_, ...), custom_call_target="tpu_custom_call" | custom-call | flops 905969664 | bytes 27525120 | tf_op jit(solution)/shard_map/experts/pallas_call | solution.py:281
  81.3 8.0 %collective-permute-start.21 = (bf16[288,768]{1,0:T(8,128)(2,1)S(1)}, bf16[288,768]{1,0:T(8,128)(2,1)S(1)}, u32[]{:S(2)}, u32[]{:S(2)}) collective-permute-start(bf16[288,768]{1,0:T(8,128)(2,1)S(1)} %get-tuple-element.101), channel_id=1, source_target_pairs={{0,3},{1,0},{2,1},{3,2},{4,7},{5,4},{6,5},{7,6},{8,11},{9,8},{10,9... | collective-permute-start | bytes 1327112 | tf_op jit(solution)/shard_map/ppermute | solution.py:30
  89.4 5.7 %experts.3 = (bf16[72,1280]{1,0:T(8,128)(2,1)S(1)}, bf16[72,1280]{1,0:T(8,128)(2,1)S(1)}, bf16[72,1280]{1,0:T(8,128)(2,1)S(1)}, bf16[72,1280]{1,0:T(8,128)(2,1)S...) custom-call(bf16[72,2048]{1,0:T(8,128)(2,1)S(1)} %get-tuple-element., ...), custom_call_target="tpu_custom_call" | custom-call | flops 1811939328 | bytes 29884416 | tf_op jit(solution)/shard_map/experts/pallas_call | solution.py:281
  97.1 5.5 %experts.5 = (bf16[72,1280]{1,0:T(8,128)(2,1)S(1)}, bf16[72,1280]{1,0:T(8,128)(2,1)S(1)}, bf16[72,1280]{1,0:T(8,128)(2,1)S(1)}, bf16[72,1280]{1,0:T(8,128)(2,1)S(1)}, bf16[288,768]{1,0:T(8,128)(2,1)S(1)}) custom-call(bf16[72,2048]{1,0:T(8,128)(2,1)S(1)} %get-tuple-element.102.refs_0_, bf16[72,2048]{1,0:T(8,128)(2,1)S(1)} %collective-permute-done.24.refs_1_, ...), custom_call_target="tpu_custom_call" | custom-call | flops 905969664 | bytes 27525120 | tf_op jit(solution)/shard_map/experts/pallas_call | solution.py:281
  103.5 10.4 %collective-permute-start.22 = (bf16[288,768]{1,0:T(8,128)(2,1)S(1)}, bf16[288,768]{1,0:T(8,128)(2,1)S(1)}, u32[]{:S(2)}, u32[]{:S(2)}) collective-permute-start(bf16[288,768]{1,0:T(8,128)(2,1)S(1)} %join.2), channel_id=1, source_target_pairs={{0,3},{1,0},{2,1},{3,2},{4,7},{5,4},{6,5},{7,6},{8,11},{9,8},{10,9... | collective-permute-start | bytes 1327112 | tf_op jit(solution)/shard_map/ppermute | solution.py:30
  113.9 1.7 %collective-permute-start.40 = (bf16[72,1280]{1,0:T(8,128)(2,1)S(1)}, bf16[72,1280]{1,0:T(8,128)(2,1)S(1)}, u32[]{:S(2)}, u32[]{:S(2)}) collective-permute-start(bf16[72,1280]{1,0:T(8,128)(2,1)S(1)} %get-tuple-element.121), channel_id=1, source_target_pairs={{8,0},{12,4},{0,8},{4,12},{9,1},{13,5},{1,9},{5,13},{10,2},{14,6},... | collective-permute-start | bytes 552968 | tf_op jit(solution)/shard_map/ppermute | solution.py:76
  116.3 2.1 %collective-permute-start.37 = (bf16[128,1280]{1,0:T(8,128)(2,1)S(1)}, bf16[128,1280]{1,0:T(8,128)(2,1)S(1)}, u32[]{:S(2)}, u32[]{:S(2)}) collective-permute-start(bf16[128,1280]{1,0:T(8,128)(2,1)S(1)} %combine.3), channel_id=1, source_target_pairs={{0,3},{1,0},{2,1},{3,2},{4,7},{5,4},{6,5},{7,6},{8,11},{9,8},{10,9... | collective-permute-start | bytes 983048 | tf_op jit(solution)/shard_map/ppermute | solution.py:30
  118.3 3.1 %collective-permute-done.40.refs_4_ = bf16[72,1280]{1,0:T(8,128)(2,1)S(1)} collective-permute-done((bf16[72,1280]{1,0:T(8,128)(2,1)S(1)}, bf16[72,1280]{1,0:T(8,128)(2,1)S(1)}, u32[]{:S(2)}, u32[]{:S(2)}) %collective-permute-start.40) | collective-permute-done | bytes 184352 | tf_op jit(solution)/shard_map/ppermute | solution.py:76
  121.4 1.7 %collective-permute-start.32 = (bf16[72,1280]{1,0:T(8,128)(2,1)S(1)}, bf16[72,1280]{1,0:T(8,128)(2,1)S(1)}, u32[]{:S(2)}, u32[]{:S(2)}) collective-permute-start(bf16[72,1280]{1,0:T(8,128)(2,1)S(1)} %get-tuple-element.113), channel_id=1, source_target_pairs={{8,0},{12,4},{0,8},{4,12},{9,1},{13,5},{1,9},{5,13},{10,2},{14,6},... | collective-permute-start | bytes 552968 | tf_op jit(solution)/shard_map/ppermute | solution.py:76
  123.2 1.5 collective-permute-done.41.refs_5_
  124.6 2.2 %collective-permute-start.33 = (bf16[72,1280]{1,0:T(8,128)(2,1)S(1)}, bf16[72,1280]{1,0:T(8,128)(2,1)S(1)}, u32[]{:S(2)}, u32[]{:S(2)}) collective-permute-start(bf16[72,1280]{1,0:T(8,128)(2,1)S(1)} %get-tuple-element.114), channel_id=1, source_target_pairs={{12,0},{8,4},{4,8},{0,12},{13,1},{9,5},{5,9},{1,13},{14,2},{10,6},... | collective-permute-start | bytes 552968 | tf_op jit(solution)/shard_map/ppermute | solution.py:76
  128.9 3.1 %collective-permute-done.33.refs_5_ = bf16[72,1280]{1,0:T(8,128)(2,1)S(1)} collective-permute-done((bf16[72,1280]{1,0:T(8,128)(2,1)S(1)}, bf16[72,1280]{1,0:T(8,128)(2,1)S(1)}, u32[]{:S(2)}, u32[]{:S(2)}) %collective-permute-start.33) | collective-permute-done | bytes 184352 | tf_op jit(solution)/shard_map/ppermute | solution.py:76
  132.0 7.2 %collective-permute-done.37.refs_6_ = bf16[128,1280]{1,0:T(8,128)(2,1)S(1)} collective-permute-done((bf16[128,1280]{1,0:T(8,128)(2,1)S(1)}, bf16[128,1280]{1,0:T(8,128)(2,1)S(1)}, u32[]{:S(2)}, u32[]{:S(2)}) %collective-permute-start.37) | collective-permute-done | bytes 327712 | tf_op jit(solution)/shard_map/ppermute | solution.py:30
  139.9 1.6 %collective-permute-start.38 = (bf16[128,1280]{1,0:T(8,128)(2,1)S(1)}, bf16[128,1280]{1,0:T(8,128)(2,1)S(1)}, u32[]{:S(2)}, u32[]{:S(2)}) collective-permute-start(bf16[128,1280]{1,0:T(8,128)(2,1)S(1)} %combine.4), channel_id=1, source_target_pairs={{0,3},{1,0},{2,1},{3,2},{4,7},{5,4},{6,5},{7,6},{8,11},{9,8},{10,9... | collective-permute-start | bytes 983048 | tf_op jit(solution)/shard_map/ppermute | solution.py:30
  141.5 1.7 %collective-permute-start.15 = (bf16[72,1280]{1,0:T(8,128)(2,1)S(1)}, bf16[72,1280]{1,0:T(8,128)(2,1)S(1)}, u32[]{:S(2)}, u32[]{:S(2)}) collective-permute-start(bf16[72,1280]{1,0:T(8,128)(2,1)S(1)} %get-tuple-element.93), channel_id=1, source_target_pairs={{8,0},{12,4},{0,8},{4,12},{9,1},{13,5},{1,9},{5,13},{10,2},{14,6},... | collective-permute-start | bytes 552968 | tf_op jit(solution)/shard_map/ppermute | solution.py:76
  143.9 5.1 %collective-permute-done.15.refs_6_ = bf16[72,1280]{1,0:T(8,128)(2,1)S(1)} collective-permute-done((bf16[72,1280]{1,0:T(8,128)(2,1)S(1)}, bf16[72,1280]{1,0:T(8,128)(2,1)S(1)}, u32[]{:S(2)}, u32[]{:S(2)}) %collective-permute-start.15) | collective-permute-done | bytes 184352 | tf_op jit(solution)/shard_map/ppermute | solution.py:76
  149.0 1.7 %collective-permute-start.29 = (bf16[72,768]{1,0:T(8,128)(2,1)S(1)}, bf16[72,768]{1,0:T(8,128)(2,1)S(1)}, u32[]{:S(2)}, u32[]{:S(2)}) collective-permute-start(bf16[72,768]{1,0:T(8,128)(2,1)S(1)} %get-tuple-element.109), channel_id=1, source_target_pairs={{8,0},{12,4},{0,8},{4,12},{9,1},{13,5},{1,9},{5,13},{10,2},{14,6},... | collective-permute-start | bytes 331784 | tf_op jit(solution)/shard_map/ppermute | solution.py:76
  152.2 2.2 %collective-permute-start.30 = (bf16[72,768]{1,0:T(8,128)(2,1)S(1)}, bf16[72,768]{1,0:T(8,128)(2,1)S(1)}, u32[]{:S(2)}, u32[]{:S(2)}) collective-permute-start(bf16[72,768]{1,0:T(8,128)(2,1)S(1)} %get-tuple-element.110), channel_id=1, source_target_pairs={{12,0},{8,4},{4,8},{0,12},{13,1},{9,5},{5,9},{1,13},{14,2},{10,6},... | collective-permute-start | bytes 331784 | tf_op jit(solution)/shard_map/ppermute | solution.py:76
  154.9 2.5 %collective-permute-done.30.refs_11_ = bf16[72,768]{1,0:T(8,128)(2,1)S(1)} collective-permute-done((bf16[72,768]{1,0:T(8,128)(2,1)S(1)}, bf16[72,768]{1,0:T(8,128)(2,1)S(1)}, u32[]{:S(2)}, u32[]{:S(2)}) %collective-permute-start.30) | collective-permute-done | bytes 110624 | tf_op jit(solution)/shard_map/ppermute | solution.py:76
  157.4 1.9 %finish.1 = bf16[128,2048]{1,0:T(8,128)(2,1)} custom-call(s32[4,128,2]{2,1,0:T(8,128)S(1)} %get-tuple-element.68.refs_0_, f32[4,128,2]{2,1,0:T(8,128)S(1)} %get-tuple-element.69.refs_1_, bf16[128,2048]{1,0:T(8,128)(2,1)S(1)} %get-tuple-element.77.refs_2_, f32[1,2048]{1,0:T(1,128)S(1)} %bitcast.7, bf16[72,1280]{1,0:T(8,128)(2,1)S(1)} %get-tuple-element.91.refs_4_, ...), custom_call_target="tpu_custom_call" | custom-call | tf_op jit(solution)/shard_map/finish/pallas_call | solution.py:207
  (74 shorter events, 24.2 us)
Async XLA Ops:
  1.1 13.2 %collective-permute-start = (bf16[152,256]{1,0:T(8,128)(2,1)S(1)}, bf16[152,256]{1,0:T(8,128)(2,1)S(1)}, u32[]{:S(2)}, u32[]{:S(2)}) collective-permute-start(bf16[152,256]{1,0:T(8,128)(2,1)S(1)} %get-tuple-element.65), channel_id=1, source_target_pairs={{0,1},{1,2},{2,3},{3,0},{4,5},{5,6},{6,7},{7,4},{8,9},{9,10},{10,1... | collective-permute-start | bytes 233480 | tf_op jit(solution)/shard_map/ppermute | solution.py:30
  4.2 10.1 %collective-permute-start.1 = (bf16[152,256]{1,0:T(8,128)(2,1)S(1)}, bf16[152,256]{1,0:T(8,128)(2,1)S(1)}, u32[]{:S(2)}, u32[]{:S(2)}) collective-permute-start(bf16[152,256]{1,0:T(8,128)(2,1)S(1)} %get-tuple-element.66), channel_id=1, source_target_pairs={{0,2},{1,3},{2,0},{3,1},{4,6},{5,7},{6,4},{7,5},{8,10},{9,11},{10,... | collective-permute-start | bytes 233480 | tf_op jit(solution)/shard_map/ppermute | solution.py:30
  6.8 7.5 %collective-permute-start.2 = (bf16[152,256]{1,0:T(8,128)(2,1)S(1)}, bf16[152,256]{1,0:T(8,128)(2,1)S(1)}, u32[]{:S(2)}, u32[]{:S(2)}) collective-permute-start(bf16[152,256]{1,0:T(8,128)(2,1)S(1)} %get-tuple-element.67), channel_id=1, source_target_pairs={{0,3},{1,0},{2,1},{3,2},{4,7},{5,4},{6,5},{7,6},{8,11},{9,8},{10,9... | collective-permute-start | bytes 233480 | tf_op jit(solution)/shard_map/ppermute | solution.py:30
  15.8 21.7 %collective-permute-start.10 = (bf16[128,2048]{1,0:T(8,128)(2,1)S(1)}, bf16[128,2048]{1,0:T(8,128)(2,1)S(1)}, u32[]{:S(2)}, u32[]{:S(2)}) collective-permute-start(bf16[128,2048]{1,0:T(8,128)(2,1)S(1)} %get-tuple-element.79.refs_1_), channel_id=1, source_target_pairs={{0,1},{1,2},{2,3},{3,0},{4,5},{5,6},{6,7},{7,4},{8,9},{9,10},{10,1... | collective-permute-start | bytes 1572872 | tf_op jit(solution)/shard_map/ppermute | solution.py:30
  37.5 16.3 %collective-permute-start.17 = (bf16[128,2048]{1,0:T(8,128)(2,1)S(1)}, bf16[128,2048]{1,0:T(8,128)(2,1)S(1)}, u32[]{:S(2)}, u32[]{:S(2)}) collective-permute-start(bf16[128,2048]{1,0:T(8,128)(2,1)S(1)} %collective-permute-done.10.refs_1_), channel_id=1, source_target_pairs={{0,1},{1,2},{2,3},{3,0},{4,5},{5,6},{6,7},{7,4},{8,9},{9,10},{10,1... | collective-permute-start | bytes 1572872 | tf_op jit(solution)/shard_map/ppermute | solution.py:30
  37.5 25.6 %collective-permute-start.23 = (bf16[128,2048]{1,0:T(8,128)(2,1)S(1)}, bf16[128,2048]{1,0:T(8,128)(2,1)S(1)}, u32[]{:S(2)}, u32[]{:S(2)}) collective-permute-start(bf16[128,2048]{1,0:T(8,128)(2,1)S(1)} %get-tuple-element.79.refs_1_), channel_id=1, source_target_pairs={{0,3},{1,0},{2,1},{3,2},{4,7},{5,4},{6,5},{7,6},{8,11},{9,8},{10,9... | collective-permute-start | bytes 1572872 | tf_op jit(solution)/shard_map/ppermute | solution.py:30
  42.2 12.6 %collective-permute-start.7 = (bf16[72,2048]{1,0:T(8,128)(2,1)S(1)}, bf16[72,2048]{1,0:T(8,128)(2,1)S(1)}, u32[]{:S(2)}, u32[]{:S(2)}) collective-permute-start(bf16[72,2048]{1,0:T(8,128)(2,1)S(1)} %get-tuple-element.81), channel_id=1, source_target_pairs={{0,4},{4,0},{8,12},{12,8},{1,5},{5,1},{9,13},{13,9},{2,6},{6,2},{1... | collective-permute-start | bytes 884744 | tf_op jit(solution)/shard_map/ppermute | solution.py:76
  43.1 11.8 %collective-permute-start.8 = (bf16[72,2048]{1,0:T(8,128)(2,1)S(1)}, bf16[72,2048]{1,0:T(8,128)(2,1)S(1)}, u32[]{:S(2)}, u32[]{:S(2)}) collective-permute-start(bf16[72,2048]{1,0:T(8,128)(2,1)S(1)} %get-tuple-element.82), channel_id=1, source_target_pairs={{0,8},{4,12},{8,0},{12,4},{1,9},{5,13},{9,1},{13,5},{2,10},{6,14},... | collective-permute-start | bytes 884744 | tf_op jit(solution)/shard_map/ppermute | solution.py:76
  43.9 13.6 %collective-permute-start.9 = (bf16[72,2048]{1,0:T(8,128)(2,1)S(1)}, bf16[72,2048]{1,0:T(8,128)(2,1)S(1)}, u32[]{:S(2)}, u32[]{:S(2)}) collective-permute-start(bf16[72,2048]{1,0:T(8,128)(2,1)S(1)} %get-tuple-element.83), channel_id=1, source_target_pairs={{0,12},{4,8},{8,4},{12,0},{1,13},{5,9},{9,5},{13,1},{2,14},{6,10},... | collective-permute-start | bytes 884744 | tf_op jit(solution)/shard_map/ppermute | solution.py:76
  53.8 9.3 %collective-permute-start.11 = (bf16[72,2048]{1,0:T(8,128)(2,1)S(1)}, bf16[72,2048]{1,0:T(8,128)(2,1)S(1)}, u32[]{:S(2)}, u32[]{:S(2)}) collective-permute-start(bf16[72,2048]{1,0:T(8,128)(2,1)S(1)} %get-tuple-element.85), channel_id=1, source_target_pairs={{0,4},{4,0},{8,12},{12,8},{1,5},{5,1},{9,13},{13,9},{2,6},{6,2},{1... | collective-permute-start | bytes 884744 | tf_op jit(solution)/shard_map/ppermute | solution.py:76
  54.9 19.0 %collective-permute-start.18 = (bf16[72,2048]{1,0:T(8,128)(2,1)S(1)}, bf16[72,2048]{1,0:T(8,128)(2,1)S(1)}, u32[]{:S(2)}, u32[]{:S(2)}) collective-permute-start(bf16[72,2048]{1,0:T(8,128)(2,1)S(1)} %get-tuple-element.98), channel_id=1, source_target_pairs={{0,4},{4,0},{8,12},{12,8},{1,5},{5,1},{9,13},{13,9},{2,6},{6,2},{1... | collective-permute-start | bytes 884744 | tf_op jit(solution)/shard_map/ppermute | solution.py:76
  54.9 19.2 %collective-permute-start.19 = (bf16[72,2048]{1,0:T(8,128)(2,1)S(1)}, bf16[72,2048]{1,0:T(8,128)(2,1)S(1)}, u32[]{:S(2)}, u32[]{:S(2)}) collective-permute-start(bf16[72,2048]{1,0:T(8,128)(2,1)S(1)} %get-tuple-element.99), channel_id=1, source_target_pairs={{0,8},{4,12},{8,0},{12,4},{1,9},{5,13},{9,1},{13,5},{2,10},{6,14},... | collective-permute-start | bytes 884744 | tf_op jit(solution)/shard_map/ppermute | solution.py:76
  57.5 16.8 %collective-permute-start.20 = (bf16[72,2048]{1,0:T(8,128)(2,1)S(1)}, bf16[72,2048]{1,0:T(8,128)(2,1)S(1)}, u32[]{:S(2)}, u32[]{:S(2)}) collective-permute-start(bf16[72,2048]{1,0:T(8,128)(2,1)S(1)} %get-tuple-element.100), channel_id=1, source_target_pairs={{0,12},{4,8},{8,4},{12,0},{1,13},{5,9},{9,5},{13,1},{2,14},{6,10},... | collective-permute-start | bytes 884744 | tf_op jit(solution)/shard_map/ppermute | solution.py:76
  63.1 18.2 %collective-permute-start.12 = (bf16[72,2048]{1,0:T(8,128)(2,1)S(1)}, bf16[72,2048]{1,0:T(8,128)(2,1)S(1)}, u32[]{:S(2)}, u32[]{:S(2)}) collective-permute-start(bf16[72,2048]{1,0:T(8,128)(2,1)S(1)} %get-tuple-element.86), channel_id=1, source_target_pairs={{0,8},{4,12},{8,0},{12,4},{1,9},{5,13},{9,1},{13,5},{2,10},{6,14},... | collective-permute-start | bytes 884744 | tf_op jit(solution)/shard_map/ppermute | solution.py:76
  63.1 26.3 %collective-permute-start.13 = (bf16[72,2048]{1,0:T(8,128)(2,1)S(1)}, bf16[72,2048]{1,0:T(8,128)(2,1)S(1)}, u32[]{:S(2)}, u32[]{:S(2)}) collective-permute-start(bf16[72,2048]{1,0:T(8,128)(2,1)S(1)} %get-tuple-element.87), channel_id=1, source_target_pairs={{0,12},{4,8},{8,4},{12,0},{1,13},{5,9},{9,5},{13,1},{2,14},{6,10},... | collective-permute-start | bytes 884744 | tf_op jit(solution)/shard_map/ppermute | solution.py:76
  73.9 21.3 %collective-permute-start.24 = (bf16[72,2048]{1,0:T(8,128)(2,1)S(1)}, bf16[72,2048]{1,0:T(8,128)(2,1)S(1)}, u32[]{:S(2)}, u32[]{:S(2)}) collective-permute-start(bf16[72,2048]{1,0:T(8,128)(2,1)S(1)} %get-tuple-element.103), channel_id=1, source_target_pairs={{0,4},{4,0},{8,12},{12,8},{1,5},{5,1},{9,13},{13,9},{2,6},{6,2},{1... | collective-permute-start | bytes 884744 | tf_op jit(solution)/shard_map/ppermute | solution.py:76
  74.2 21.5 %collective-permute-start.25 = (bf16[72,2048]{1,0:T(8,128)(2,1)S(1)}, bf16[72,2048]{1,0:T(8,128)(2,1)S(1)}, u32[]{:S(2)}, u32[]{:S(2)}) collective-permute-start(bf16[72,2048]{1,0:T(8,128)(2,1)S(1)} %get-tuple-element.104), channel_id=1, source_target_pairs={{0,8},{4,12},{8,0},{12,4},{1,9},{5,13},{9,1},{13,5},{2,10},{6,14},... | collective-permute-start | bytes 884744 | tf_op jit(solution)/shard_map/ppermute | solution.py:76
  74.3 22.0 %collective-permute-start.26 = (bf16[72,2048]{1,0:T(8,128)(2,1)S(1)}, bf16[72,2048]{1,0:T(8,128)(2,1)S(1)}, u32[]{:S(2)}, u32[]{:S(2)}) collective-permute-start(bf16[72,2048]{1,0:T(8,128)(2,1)S(1)} %get-tuple-element.105), channel_id=1, source_target_pairs={{0,12},{4,8},{8,4},{12,0},{1,13},{5,9},{9,5},{13,1},{2,14},{6,10},... | collective-permute-start | bytes 884744 | tf_op jit(solution)/shard_map/ppermute | solution.py:76
  81.3 22.1 %collective-permute-start.21 = (bf16[288,768]{1,0:T(8,128)(2,1)S(1)}, bf16[288,768]{1,0:T(8,128)(2,1)S(1)}, u32[]{:S(2)}, u32[]{:S(2)}) collective-permute-start(bf16[288,768]{1,0:T(8,128)(2,1)S(1)} %get-tuple-element.101), channel_id=1, source_target_pairs={{0,3},{1,0},{2,1},{3,2},{4,7},{5,4},{6,5},{7,6},{8,11},{9,8},{10,9... | collective-permute-start | bytes 1327112 | tf_op jit(solution)/shard_map/ppermute | solution.py:30
  95.1 7.5 %collective-permute-start.31 = (bf16[72,1280]{1,0:T(8,128)(2,1)S(1)}, bf16[72,1280]{1,0:T(8,128)(2,1)S(1)}, u32[]{:S(2)}, u32[]{:S(2)}) collective-permute-start(bf16[72,1280]{1,0:T(8,128)(2,1)S(1)} %get-tuple-element.112), channel_id=1, source_target_pairs={{4,0},{0,4},{12,8},{8,12},{5,1},{1,5},{13,9},{9,13},{6,2},{2,6},{1... | collective-permute-start | bytes 552968 | tf_op jit(solution)/shard_map/ppermute | solution.py:76
  95.2 8.4 %collective-permute-start.34 = (bf16[72,1280]{1,0:T(8,128)(2,1)S(1)}, bf16[72,1280]{1,0:T(8,128)(2,1)S(1)}, u32[]{:S(2)}, u32[]{:S(2)}) collective-permute-start(bf16[72,1280]{1,0:T(8,128)(2,1)S(1)} %get-tuple-element.116), channel_id=1, source_target_pairs={{4,0},{0,4},{12,8},{8,12},{5,1},{1,5},{13,9},{9,13},{6,2},{2,6},{1... | collective-permute-start | bytes 552968 | tf_op jit(solution)/shard_map/ppermute | solution.py:76
  95.7 18.3 %collective-permute-start.35 = (bf16[72,1280]{1,0:T(8,128)(2,1)S(1)}, bf16[72,1280]{1,0:T(8,128)(2,1)S(1)}, u32[]{:S(2)}, u32[]{:S(2)}) collective-permute-start(bf16[72,1280]{1,0:T(8,128)(2,1)S(1)} %get-tuple-element.117), channel_id=1, source_target_pairs={{8,0},{12,4},{0,8},{4,12},{9,1},{13,5},{1,9},{5,13},{10,2},{14,6},... | collective-permute-start | bytes 552968 | tf_op jit(solution)/shard_map/ppermute | solution.py:76
  96.4 19.3 %collective-permute-start.36 = (bf16[72,1280]{1,0:T(8,128)(2,1)S(1)}, bf16[72,1280]{1,0:T(8,128)(2,1)S(1)}, u32[]{:S(2)}, u32[]{:S(2)}) collective-permute-start(bf16[72,1280]{1,0:T(8,128)(2,1)S(1)} %get-tuple-element.118), channel_id=1, source_target_pairs={{12,0},{8,4},{4,8},{0,12},{13,1},{9,5},{5,9},{1,13},{14,2},{10,6},... | collective-permute-start | bytes 552968 | tf_op jit(solution)/shard_map/ppermute | solution.py:76
  102.6 13.6 %collective-permute-start.39 = (bf16[72,1280]{1,0:T(8,128)(2,1)S(1)}, bf16[72,1280]{1,0:T(8,128)(2,1)S(1)}, u32[]{:S(2)}, u32[]{:S(2)}) collective-permute-start(bf16[72,1280]{1,0:T(8,128)(2,1)S(1)} %get-tuple-element.120), channel_id=1, source_target_pairs={{4,0},{0,4},{12,8},{8,12},{5,1},{1,5},{13,9},{9,13},{6,2},{2,6},{1... | collective-permute-start | bytes 552968 | tf_op jit(solution)/shard_map/ppermute | solution.py:76
  103.4 38.1 %collective-permute-start.27 = (bf16[288,768]{1,0:T(8,128)(2,1)S(1)}, bf16[288,768]{1,0:T(8,128)(2,1)S(1)}, u32[]{:S(2)}, u32[]{:S(2)}) collective-permute-start(bf16[288,768]{1,0:T(8,128)(2,1)S(1)} %get-tuple-element.106), channel_id=1, source_target_pairs={{0,1},{1,2},{2,3},{3,0},{4,5},{5,6},{6,7},{7,4},{8,9},{9,10},{10,1... | collective-permute-start | bytes 1327112 | tf_op jit(solution)/shard_map/ppermute | solution.py:30
  103.5 39.7 %collective-permute-start.22 = (bf16[288,768]{1,0:T(8,128)(2,1)S(1)}, bf16[288,768]{1,0:T(8,128)(2,1)S(1)}, u32[]{:S(2)}, u32[]{:S(2)}) collective-permute-start(bf16[288,768]{1,0:T(8,128)(2,1)S(1)} %join.2), channel_id=1, source_target_pairs={{0,3},{1,0},{2,1},{3,2},{4,7},{5,4},{6,5},{7,6},{8,11},{9,8},{10,9... | collective-permute-start | bytes 1327112 | tf_op jit(solution)/shard_map/ppermute | solution.py:30
  115.7 9.0 %collective-permute-start.41 = (bf16[72,1280]{1,0:T(8,128)(2,1)S(1)}, bf16[72,1280]{1,0:T(8,128)(2,1)S(1)}, u32[]{:S(2)}, u32[]{:S(2)}) collective-permute-start(bf16[72,1280]{1,0:T(8,128)(2,1)S(1)} %get-tuple-element.122), channel_id=1, source_target_pairs={{12,0},{8,4},{4,8},{0,12},{13,1},{9,5},{5,9},{1,13},{14,2},{10,6},... | collective-permute-start | bytes 552968 | tf_op jit(solution)/shard_map/ppermute | solution.py:76
  116.3 23.0 %collective-permute-start.37 = (bf16[128,1280]{1,0:T(8,128)(2,1)S(1)}, bf16[128,1280]{1,0:T(8,128)(2,1)S(1)}, u32[]{:S(2)}, u32[]{:S(2)}) collective-permute-start(bf16[128,1280]{1,0:T(8,128)(2,1)S(1)} %combine.3), channel_id=1, source_target_pairs={{0,3},{1,0},{2,1},{3,2},{4,7},{5,4},{6,5},{7,6},{8,11},{9,8},{10,9... | collective-permute-start | bytes 983048 | tf_op jit(solution)/shard_map/ppermute | solution.py:30
  128.9 25.5 %collective-permute-start.42 = (bf16[128,1280]{1,0:T(8,128)(2,1)S(1)}, bf16[128,1280]{1,0:T(8,128)(2,1)S(1)}, u32[]{:S(2)}, u32[]{:S(2)}) collective-permute-start(bf16[128,1280]{1,0:T(8,128)(2,1)S(1)} %combine.5), channel_id=1, source_target_pairs={{0,1},{1,2},{2,3},{3,0},{4,5},{5,6},{6,7},{7,4},{8,9},{9,10},{10,1... | collective-permute-start | bytes 983048 | tf_op jit(solution)/shard_map/ppermute | solution.py:30
  139.9 14.9 %collective-permute-start.38 = (bf16[128,1280]{1,0:T(8,128)(2,1)S(1)}, bf16[128,1280]{1,0:T(8,128)(2,1)S(1)}, u32[]{:S(2)}, u32[]{:S(2)}) collective-permute-start(bf16[128,1280]{1,0:T(8,128)(2,1)S(1)} %combine.4), channel_id=1, source_target_pairs={{0,3},{1,0},{2,1},{3,2},{4,7},{5,4},{6,5},{7,6},{8,11},{9,8},{10,9... | collective-permute-start | bytes 983048 | tf_op jit(solution)/shard_map/ppermute | solution.py:30
  143.2 9.0 %collective-permute-start.16 = (bf16[72,1280]{1,0:T(8,128)(2,1)S(1)}, bf16[72,1280]{1,0:T(8,128)(2,1)S(1)}, u32[]{:S(2)}, u32[]{:S(2)}) collective-permute-start(bf16[72,1280]{1,0:T(8,128)(2,1)S(1)} %get-tuple-element.94), channel_id=1, source_target_pairs={{12,0},{8,4},{4,8},{0,12},{13,1},{9,5},{5,9},{1,13},{14,2},{10,6},... | collective-permute-start | bytes 552968 | tf_op jit(solution)/shard_map/ppermute | solution.py:76
  143.6 11.2 %collective-permute-start.28 = (bf16[72,768]{1,0:T(8,128)(2,1)S(1)}, bf16[72,768]{1,0:T(8,128)(2,1)S(1)}, u32[]{:S(2)}, u32[]{:S(2)}) collective-permute-start(bf16[72,768]{1,0:T(8,128)(2,1)S(1)} %get-tuple-element.108), channel_id=1, source_target_pairs={{4,0},{0,4},{12,8},{8,12},{5,1},{1,5},{13,9},{9,13},{6,2},{2,6},{1... | collective-permute-start | bytes 331784 | tf_op jit(solution)/shard_map/ppermute | solution.py:76
  (12 other events, 114.3 us)
